TPU v7x, 512 devices: a whole 4x4x16 slice. The times are simulated.
512 devices in a mesh: ep: 32 (over z, core), tp: 16 (over y, x).
Axes of the slice: x: 4, y: 4, z: 16, core: 2. Of those that a mesh axis runs over, the one named last changes fastest.
Arguments:
- tokens: bfloat16 [1536, 2048], P('ep'), may hold values from -6 to 6
- retention_state: float32 [1536, 16, 64, 64], P('ep', 'tp'), may hold values from -1.5 to 1.5
- lengths: int32 [1536], P('ep'), may hold values from 1024 to 16383
- query_weight: bfloat16 [2048, 1024], P(None, 'tp'), may hold values from -0.125 to 0.125
- key_weight: bfloat16 [2048, 1024], P(None, 'tp'), may hold values from -0.125 to 0.125
- value_weight: bfloat16 [2048, 1024], P(None, 'tp'), may hold values from -0.125 to 0.125
- gate_weight: bfloat16 [2048, 1024], P(None, 'tp'), may hold values from -0.125 to 0.125
- out_weight: bfloat16 [1024, 2048], P(None, 'tp'), may hold values from -0.1875 to 0.1875
- first_gain: float32 [2048], replicated, may hold values from 0.1 to 1.9
- routing: int32 [1536, 4], P('ep'), may hold values from 0 to 127, all different within a row; in each aligned block of 48 rows (0 to 47, 48 to 95, ...) at most 5 rows name the same one
- route_weight: float32 [1536, 4], P('ep'), may hold values from 0.1 to 1
- expert_gate: bfloat16 [128, 2048, 512], P('ep', None, 'tp'), may hold values from -0.125 to 0.125
- expert_up: bfloat16 [128, 2048, 512], P('ep', None, 'tp'), may hold values from -0.125 to 0.125
- expert_down: bfloat16 [128, 512, 2048], P('ep', None, 'tp'), may hold values from -0.25 to 0.25
- shared_gate: bfloat16 [2048, 512], P(None, 'tp'), may hold values from -0.125 to 0.125
- shared_up: bfloat16 [2048, 512], P(None, 'tp'), may hold values from -0.125 to 0.125
- shared_down: bfloat16 [512, 2048], P(None, 'tp'), may hold values from -0.25 to 0.25
- side_gate: bfloat16 [2048, 256], P('ep', 'tp'), may hold values from -0.125 to 0.125
- side_up: bfloat16 [2048, 256], P('ep', 'tp'), may hold values from -0.125 to 0.125
- side_down: bfloat16 [256, 2048], P(None, 'tp'), may hold values from -0.375 to 0.375
- side_switch: bfloat16 [2048], replicated, may hold values from -0.125 to 0.125
- second_gain: float32 [2048], P('tp'), may hold values from 0.1 to 1.9
Outputs:
- output: bfloat16 [1536, 2048], P('ep', 'tp')
- new_state: float32 [1536, 16, 64, 64], P('ep', 'tp')
Inputs may be any that keep to these rules, and one draw needn't show every extreme that they name: `routing`: each row names 4 different experts. Among the rows of one ep index (aligned blocks of 48 rows) no expert is named by more than 5 rows, a bound that some block reaches.
All inputs are finite; a program needn't handle non-finite values.
Results may differ from a plain program's by a relative error of at most 0.013.
Values may be sent and summed in bfloat16 or wider, within the bound.
No kernel may reach another device: no remote copies, remote signals or barrier semaphores. Data moves between devices by JAX's collectives and lax.ppermute only.
A program may use at most 64 MiB of HBM per device.

v0:
```python
import functools

import jax
import jax.numpy as jnp
from jax import lax
from jax.sharding import Mesh
from jax.sharding import PartitionSpec as P

HEADS = 16
TP = ("tp_0", "tp_1")


RESIDUAL_SCALE = 2.0**0.25
NORM_EPS = 1e-05
GROUP_EPS = 1e-06
ROPE_BASE = 10000.0


def from_everyone(shard, axis):
    length = lax.axis_size(axis)
    return lax.all_to_all(
        jnp.broadcast_to(shard[None], (length, *shard.shape)), axis, 0, 0, tiled=True
    )


def in_order(parts, dim):
    parts = jnp.moveaxis(parts, 0, dim)
    dims = parts.shape
    return parts.reshape(*dims[:dim], dims[dim] * dims[dim + 1], *dims[dim + 2 :])


def collect(shard, axis, dim):
    parts = from_everyone(shard, axis)
    return in_order(parts, dim)


def in_one_piece(arrays, axis, dim, along):
    both = jnp.concatenate(arrays, axis=along)
    filled, at, finished = (lax.all_gather(both, axis, axis=dim, tiled=True), 0, [])
    for a in arrays:
        finished.append(lax.slice_in_dim(filled, at, at + a.shape[along], axis=along))
        at += a.shape[along]
    return tuple(finished)


def one_gather(arrays, axis, dims):
    line = jnp.concatenate([a.reshape(-1) for a in arrays])
    lines, at, finished = (lax.all_gather(line, axis), 0, [])
    for a, dim in zip(arrays, dims):
        parts = lines[:, at : at + a.size].reshape(-1, *a.shape)
        finished.append(in_order(parts, dim))
        at += a.size
    return tuple(finished)


def by_axis(shard, axes):
    return functools.reduce(lax.psum, axes, shard)


def rotate(vector, positions):
    half_width = vector.shape[-1] // 2
    frequency = ROPE_BASE ** (-jnp.arange(half_width, dtype=jnp.float32) / half_width)
    angles = positions.astype(jnp.float32)[:, None, None] * frequency[None, None, :]
    cosine = jnp.cos(angles)
    sine_part = jnp.sin(angles)
    first_half = vector[..., :half_width]
    second_half = vector[..., half_width:]
    return jnp.concatenate(
        [
            first_half * cosine - second_half * sine_part,
            second_half * cosine + first_half * sine_part,
        ],
        -1,
    )


def retain(
    tokens,
    retention_state,
    lengths,
    query_weight,
    key_weight,
    value_weight,
    gate_weight,
    first_head,
):
    row_count = tokens.shape[0]
    head_count = retention_state.shape[1]
    head_width = retention_state.shape[2]

    def project(weight):
        rounded = jnp.dot(tokens, weight, preferred_element_type=jnp.float32).astype(jnp.bfloat16)
        return lax.optimization_barrier(rounded).astype(jnp.float32)

    queries = rotate(project(query_weight).reshape(row_count, head_count, head_width), lengths)
    key_rows = rotate(
        project(key_weight).reshape(row_count, head_count, head_width), lengths
    ) * head_width ** (-0.5)
    values = project(value_weight).reshape(row_count, head_count, head_width)
    gate_act = project(gate_weight)
    head_index = (first_head + jnp.arange(head_count)).astype(jnp.float32)
    decays = 1.0 - 2.0 ** (-5.0 - 7.0 * head_index / (HEADS - 1))
    own_term = jnp.sum(queries * key_rows, -1, keepdims=True) * values
    carried = decays[None, :, None] * jnp.einsum("bhd,bhde->bhe", queries, retention_state)
    result = own_term + carried
    new_state = (
        decays[None, :, None, None] * retention_state
        + key_rows[:, :, :, None] * values[:, :, None, :]
    )
    normed = result * lax.rsqrt(jnp.mean(result * result, -1, keepdims=True) + GROUP_EPS)
    mixed_heads = (
        normed.reshape(row_count, head_count * head_width) * jax.nn.silu(gate_act)
    ).astype(jnp.bfloat16)
    return (mixed_heads, new_state)


def slot_numbers(route_ids, expert_count, capacity):
    onehot = (route_ids[..., None] == jnp.arange(expert_count, dtype=jnp.int32)).astype(jnp.int32)
    position = jnp.sum(jnp.cumsum(onehot, -2) * onehot, -1) - 1
    return route_ids * capacity + position


def on_device(
    tokens,
    retention_state,
    lengths,
    query_weight,
    key_weight,
    value_weight,
    gate_weight,
    out_weight,
    first_gain,
    routing,
    route_weight,
    expert_gate,
    expert_up,
    expert_down,
    shared_gate,
    shared_up,
    shared_down,
    side_gate,
    side_up,
    side_down,
    side_switch,
    second_gain,
):
    seq_rows = tokens.shape[0]
    model_width = tokens.shape[1]
    head_count = retention_state.shape[1]
    col_count = out_weight.shape[1]
    ep_count = lax.axis_size("ep")
    tp_rank = lax.axis_index(TP)
    col_start = tp_rank * col_count
    mixed_heads, new_state = retain(
        tokens,
        retention_state,
        lengths,
        query_weight,
        key_weight,
        value_weight,
        gate_weight,
        tp_rank * head_count,
    )
    mixing = jnp.dot(collect(mixed_heads, TP, 1), out_weight, preferred_element_type=jnp.float32)
    own_cols = lax.dynamic_slice_in_dim(tokens, col_start, col_count, 1).astype(jnp.float32)
    pre_first = RESIDUAL_SCALE * own_cols + mixing
    whole_rows = collect(pre_first, TP, 1)
    row_mean = jnp.mean(whole_rows, -1, keepdims=True)
    square = jnp.mean(whole_rows * whole_rows, -1, keepdims=True)
    normed_full = (
        (whole_rows - row_mean) * lax.rsqrt(square - row_mean * row_mean + NORM_EPS) * first_gain
    ).astype(jnp.bfloat16)
    normed_cols = lax.dynamic_slice_in_dim(normed_full, col_start, col_count, 1)
    portion = in_one_piece((side_gate, side_up), "ep", 0, 1)
    side_pre = jnp.dot(normed_full, portion[0], preferred_element_type=jnp.float32)
    side_lift = jnp.dot(normed_full, portion[1], preferred_element_type=jnp.float32)
    side_hidden = (jax.nn.silu(side_pre) * side_lift).astype(jnp.bfloat16)
    shared_hidden = (
        jax.nn.silu(jnp.dot(normed_full, shared_gate, preferred_element_type=jnp.float32))
        * jnp.dot(normed_full, shared_up, preferred_element_type=jnp.float32)
    ).astype(jnp.bfloat16)
    shared_all, side_all = one_gather((shared_hidden, side_hidden), TP, (1, 1))
    shared_out = jnp.dot(shared_all, shared_down, preferred_element_type=jnp.float32)
    side_out = jnp.dot(side_all, side_down, preferred_element_type=jnp.float32)
    switch = jax.nn.sigmoid(jnp.dot(normed_full, side_switch, preferred_element_type=jnp.float32))
    top_count = routing.shape[1]
    local_experts = expert_gate.shape[0]
    expert_count = local_experts * ep_count
    capacity = (3 * seq_rows * top_count + expert_count - 1) // expert_count
    assigned = seq_rows * top_count
    slot_ids = slot_numbers(routing.reshape(assigned), expert_count, capacity)
    slot_hot = (
        slot_ids[:, None] == jnp.arange(expert_count * capacity, dtype=jnp.int32)[None, :]
    ).astype(jnp.bfloat16)
    token_hot = (
        (jnp.arange(assigned, dtype=jnp.int32) // top_count)[:, None]
        == jnp.arange(seq_rows, dtype=jnp.int32)[None, :]
    ).astype(jnp.bfloat16)
    table = jnp.einsum("as,at->st", slot_hot, token_hot, preferred_element_type=jnp.float32).astype(
        jnp.bfloat16
    )
    outgoing = jnp.dot(table, normed_cols, preferred_element_type=jnp.float32).astype(jnp.bfloat16)
    slot_rows = collect(
        lax.all_to_all(
            outgoing.reshape(expert_count, capacity, col_count),
            "ep",
            split_axis=0,
            concat_axis=0,
            tiled=True,
        ),
        TP,
        2,
    )
    slot_count = slot_rows.shape[1]
    grouped = slot_rows.reshape(ep_count, local_experts, slot_count, slot_rows.shape[2])
    gate_part = jnp.einsum(
        "sjcd,jdf->sjcf", grouped, expert_gate, preferred_element_type=jnp.float32
    )
    up_part = jnp.einsum("sjcd,jdf->sjcf", grouped, expert_up, preferred_element_type=jnp.float32)
    hidden = (jax.nn.silu(gate_part) * up_part).astype(jnp.bfloat16)
    hidden_all = collect(hidden, TP, 3)
    result = jnp.einsum(
        "sjcf,jfd->sjcd", hidden_all, expert_down, preferred_element_type=jnp.float32
    ).astype(jnp.bfloat16)
    returned = lax.all_to_all(
        result.reshape(ep_count * local_experts, slot_count, col_count),
        "ep",
        split_axis=0,
        concat_axis=0,
        tiled=True,
    )
    picked = jnp.dot(
        slot_hot,
        returned.reshape(expert_count * capacity, col_count),
        preferred_element_type=jnp.float32,
    ).reshape(seq_rows, top_count, col_count)
    routed = jnp.sum(picked * route_weight[:, :, None], 1)
    pre_second = (
        RESIDUAL_SCALE * normed_cols.astype(jnp.float32)
        + routed
        + shared_out
        + switch[:, None] * side_out
    )
    totals_second = (
        by_axis(jnp.sum(pre_second, -1), TP),
        by_axis(jnp.sum(pre_second * pre_second, -1), TP),
    )
    mean_second = totals_second[0][:, None] / model_width
    square_second = totals_second[1][:, None] / model_width
    output = (
        (pre_second - mean_second)
        * lax.rsqrt(square_second - mean_second * mean_second + NORM_EPS)
        * second_gain
    ).astype(jnp.bfloat16)
    return (output, new_state)


def solution(mesh):
    finer = Mesh(mesh.devices.reshape(mesh.shape["ep"], 4, 4), ("ep", "tp_0", "tp_1"))
    return jax.shard_map(
        on_device,
        mesh=finer,
        in_specs=(
            P("ep", None),
            P("ep", TP, None, None),
            P("ep"),
            P(None, TP),
            P(None, TP),
            P(None, TP),
            P(None, TP),
            P(None, TP),
            P(),
            P("ep", None),
            P("ep", None),
            P("ep", None, TP),
            P("ep", None, TP),
            P("ep", None, TP),
            P(None, TP),
            P(None, TP),
            P(None, TP),
            P("ep", TP),
            P("ep", TP),
            P(None, TP),
            P(),
            P(TP),
        ),
        out_specs=(P("ep", TP), P("ep", TP, None, None)),
        check_vma=False,
    )
```

profile of v0, /device:TPU:32, one launch (start us, length us, event | category | flops | bytes accessed | tf_op | source)
XLA Modules:
  0.0 213.5 jit_solution(11035793085490469563)
XLA Ops:
  0.7 1.4 convolution_convert_fusion.6
  2.1 1.3 convolution_convert_fusion.5
  3.4 0.7 convert_element_type.70
  4.1 1.3 convolution_convert_fusion.4
  5.7 0.3 fusion.70
  6.3 0.2 convolution_convert_fusion.3
  6.7 0.8 reshape.417
  7.5 7.0 %all-to-all-start = ((bf16[16,2,1536]{2,1,0:T(2,128)(2,1)}), bf16[16,2,1536]{2,1,0:T(2,128)(2,1)S(1)}, u32[]{:S(2)}, u32[]{:S(2)}) async-start(bf16[16,2,1536]{2,1,0:T(2,128)(2,1)} %reshape.417), calls=%async_computation | async-start | bytes 196608 | tf_op jit(solution)/shard_map/all_to_all | solution.py:21
  15.1 7.3 %all-to-all-done = bf16[16,2,1536]{2,1,0:T(2,128)(2,1)S(1)} async-done(((bf16[16,2,1536]{2,1,0:T(2,128)(2,1)}), bf16[16,2,1536]{2,1,0:T(2,128)(2,1)S(1)}, u32[]{:S(2)}, u32[]{:S(2)}) %all-to-all-start) | async-done | bytes 98336 | tf_op jit(solution)/shard_map/all_to_all | solution.py:21
  22.9 0.8 broadcast_in_dim.9
  23.7 3.6 %all-to-all-start.1 = ((f32[16,48,128]{2,1,0:T(8,128)}), f32[16,48,128]{2,1,0:T(8,128)S(1)}, u32[]{:S(2)}, u32[]{:S(2)}) async-start(f32[16,48,128]{2,1,0:T(8,128)} %broadcast_in_dim.9), calls=%async_computation.1 | async-start | bytes 786432 | tf_op jit(solution)/shard_map/all_to_all | solution.py:21
  27.5 9.1 %all-to-all-done.1 = f32[16,48,128]{2,1,0:T(8,128)S(1)} async-done(((f32[16,48,128]{2,1,0:T(8,128)}), f32[16,48,128]{2,1,0:T(8,128)S(1)}, u32[]{:S(2)}, u32[]{:S(2)}) %all-to-all-start.1) | async-done | bytes 393248 | tf_op jit(solution)/shard_map/all_to_all | solution.py:21
  37.0 0.5 convolution_convert_fusion.1
  37.6 36.1 %all_to_all.30 = bf16[128,5,128]{2,1,0:T(8,128)(2,1)S(1)} all-to-all(bf16[128,5,128]{2,1,0:T(8,128)(2,1)S(1)} %reshape.384), channel_id=1, replica_groups=mesh['ep'=32,'tp_0'=4,'tp_1'=4] {'ep'}, dimensions={0} | all-to-all | bytes 327680 | tf_op jit(solution)/shard_map/all_to_all | solution.py:204
  73.8 2.1 %broadcast_in_dim.10 = bf16[16,128,5,128]{3,1,2,0:T(8,128)(2,1)} broadcast(bf16[128,5,128]{2,0,1:T(8,128)(2,1)S(1)} %copy.66), dimensions={1,2,3} | broadcast | bytes 2785280 | tf_op jit(solution)/shard_map/broadcast_in_dim | solution.py:22
  75.9 3.9 %all-to-all-start.3 = ((bf16[16,128,5,128]{3,1,2,0:T(8,128)(2,1)}), bf16[16,128,5,128]{3,1,2,0:T(8,128)(2,1)S(1)}, u32[]{:S(2)}, u32[]{:S(2)}) async-start(bf16[16,128,5,128]{3,1,2,0:T(8,128)(2,1)} %broadcast_in_dim.10), calls=%async_computation.3 | async-start | bytes 5242880 | tf_op jit(solution)/shard_map/all_to_all | solution.py:21
  79.9 0.7 copy.65
  80.6 29.6 %all-gather.1 = bf16[32,64,32]{1,2,0:T(8,128)(2,1)S(1)} all-gather(bf16[1,64,32]{1,2,0:T(8,128)(2,1)S(1)} %maximum_bitcast_fusion), channel_id=1, replica_groups=mesh['ep'=32,'tp_0'=4,'tp_1'=4] {'ep'}, dimensions={0}, use_global_device_ids=true | all-gather | bytes 135168 | tf_op jit(solution)/shard_map/all_gather | solution.py:39
  110.2 0.8 copy.74
  111.0 1.2 reshape.404
  112.2 0.7 reshape.414
  113.0 3.0 %multiply_add_fusion = f32[48,1,64,64]{3,2,1,0:T(8,128)} fusion(f32[48,1,64,64]{3,2,1,0:T(8,128)} %param.23, f32[48,64]{1,0:T(8,128)S(1)} %convert_element_type.73, f32[48,64]{1,0:T(8,128)S(1)} %maximum_multiply_fusion.1, f32[]{:T(128)S(6)} %sub.66), kind=kLoop, calls=%fused_computation.6 | loop fusion | flops 589824 | bytes 1597444 | tf_op jit(solution)/shard_map/add | solution.py:107
  116.0 2.3 %all-to-all-done.3 = bf16[16,128,5,128]{3,1,2,0:T(8,128)(2,1)S(1)} async-done(((bf16[16,128,5,128]{3,1,2,0:T(8,128)(2,1)}), bf16[16,128,5,128]{3,1,2,0:T(8,128)(2,1)S(1)}, u32[]{:S(2)}, u32[]{:S(2)}) %all-to-all-start.3) | async-done | bytes 2621472 | tf_op jit(solution)/shard_map/all_to_all | solution.py:21
  118.3 3.2 %copy.67 = bf16[128,5,16,128]{3,2,0,1:T(8,128)(2,1)} copy(bf16[128,5,16,128]{3,0,1,2:T(8,128)(2,1)S(1)} %bitcast.140) | data formatting | bytes 5242880 | tf_op jit(solution)/shard_map/transpose | solution.py:27
  121.5 3.5 %reshape_reshape.3 = bf16[32,4,5,2048]{3,1,0,2:T(4,128)(2,1)S(1)} reshape(bf16[128,5,16,128]{3,2,0,1:T(8,128)(2,1)} %copy.67) | data formatting | bytes 5242880 | tf_op jit(solution)/shard_map/reshape;reshape | solution.py:215
  125.0 2.6 %fusion.6 = f32[32,4,5,32]{3,0,2,1:T(8,128)S(1)} fusion(bf16[32,4,5,2048]{3,1,0,2:T(4,128)(2,1)S(1)} %reshape_reshape.3, bf16[4,2048,32]{1,2,0:T(8,128)(2,1)} %param.33), kind=kOutput, calls=%fused_computation.7 | convolution fusion | flops 83886080 | bytes 3227648 | tf_op jit(solution)/shard_map/sjcd,jdf->sjcf/dot_general | solution.py:216
  127.7 1.6 fusion.15
  129.3 0.5 broadcast_bitcast_fusion
  129.9 3.2 %reshape.419 = bf16[16,2,10240]{2,1,0:T(2,128)(2,1)} reshape(bf16[16,4,5,32,32]{4,3,2,1,0:T(8,128)(2,1)S(1)} %broadcast_bitcast_fusion) | data formatting | bytes 1310720
  133.0 5.0 %all-to-all-start.4 = ((bf16[16,2,10240]{2,1,0:T(2,128)(2,1)}), bf16[16,2,10240]{2,1,0:T(2,128)(2,1)}, u32[]{:S(2)}, u32[]{:S(2)}) async-start(bf16[16,2,10240]{2,1,0:T(2,128)(2,1)} %reshape.419), calls=%async_computation.4 | async-start | bytes 1310720 | tf_op jit(solution)/shard_map/all_to_all | solution.py:21
  138.0 1.1 fusion.73
  139.1 1.1 fusion.21
  140.2 11.3 %all-to-all-done.4 = bf16[16,2,10240]{2,1,0:T(2,128)(2,1)} async-done(((bf16[16,2,10240]{2,1,0:T(2,128)(2,1)}), bf16[16,2,10240]{2,1,0:T(2,128)(2,1)}, u32[]{:S(2)}, u32[]{:S(2)}) %all-to-all-start.4) | async-done | bytes 655392 | tf_op jit(solution)/shard_map/all_to_all | solution.py:21
  151.5 3.6 %reshape.420 = bf16[16,4,5,32,32]{4,3,2,1,0:T(8,128)(2,1)S(1)} reshape(bf16[16,2,10240]{2,1,0:T(2,128)(2,1)} %all-to-all-done.4) | data formatting | bytes 1310720
  155.1 0.5 bitcast_bitcast_fusion
  155.6 1.7 copy.70
  157.3 3.3 %reshape.385 = bf16[32,4,5,512]{3,0,2,1:T(8,128)(2,1)} reshape(bf16[32,4,5,16,32]{4,3,0,2,1:T(8,128)(2,1)S(1)} %copy.70) | data formatting | bytes 1310720 | tf_op jit(solution)/shard_map/reshape | solution.py:29
  160.6 1.4 fusion.18
  162.1 0.8 copy.72
  162.9 6.9 %all-to-all-start.5 = ((bf16[128,5,128]{2,1,0:T(8,128)(2,1)}), bf16[128,5,128]{2,1,0:T(8,128)(2,1)S(1)}, u32[]{:S(2)}, u32[]{:S(2)}) async-start(bf16[128,5,128]{2,1,0:T(8,128)(2,1)} %copy.72), calls=%async_computation.5 | async-start | bytes 524288 | tf_op jit(solution)/shard_map/all_to_all | solution.py:225
  170.6 21.7 %all-gather.2 = bf16[16,1,2304]{2,1,0:T(2,128)(2,1)S(1)} all-gather(bf16[1,1,2304]{2,1,0:T(2,128)(2,1)S(1)} %reshape.405), channel_id=2, replica_groups=mesh['ep'=32,'tp_0'=4,'tp_1'=4] {'tp_0','tp_1'}, dimensions={0}, use_global_device_ids=true | all-gather | bytes 78336 | tf_op jit(solution)/shard_map/all_gather | solution.py:48
  192.5 0.2 reshape.391
  192.7 0.2 reshape.392
  193.3 0.3 fusion.19
  193.8 0.3 fusion.68
  194.1 10.0 %all-reduce.2 = (f32[48]{0:T(128)S(1)}, f32[48]{0:T(128)S(1)}) all-reduce(f32[48]{0:T(128)S(1)} %get-tuple-element.3, f32[48]{0:T(128)S(1)} %get-tuple-element.2), channel_id=1, replica_groups=mesh['ep'=32,'tp_0'=4,'tp_1'=4] {'tp_0'}, use_global_device_ids=true, to_apply=%region_12.13 | all-reduce | flops 96 | bytes 768 | tf_op jit(solution)/shard_map/psum | solution.py:57
  204.1 8.7 %all-reduce.1 = (f32[48]{0:T(128)S(1)}, f32[48]{0:T(128)S(1)}) all-reduce(f32[48]{0:T(128)S(1)} %get-tuple-element.6, f32[48]{0:T(128)S(1)} %get-tuple-element.7), channel_id=1, replica_groups=mesh['ep'=32,'tp_0'=4,'tp_1'=4] {'tp_1'}, use_global_device_ids=true, to_apply=%region_13.14 | all-reduce | flops 96 | bytes 768 | tf_op jit(solution)/shard_map/psum | solution.py:57
  212.8 0.7 multiply_convert_fusion
  (88 shorter events, 4.3 us)
Async XLA Ops:
  0.6 159.9 %copy-start = (bf16[4,512,128]{2,1,0:T(8,128)(2,1)S(1)}, bf16[4,512,128]{2,1,0:T(8,128)(2,1)}, u32[]{:S(2)}) copy-start(bf16[4,512,128]{2,1,0:T(8,128)(2,1)} %param.35) | copy-start | bytes 1572868
  0.6 5.7 %copy-start.2 = (bf16[48,2048]{1,0:T(8,128)(2,1)S(1)}, bf16[48,2048]{1,0:T(8,128)(2,1)}, u32[]{:S(2)}) copy-start(bf16[48,2048]{1,0:T(8,128)(2,1)} %param.22) | copy-start | bytes 589828
  0.7 5.1 %copy-start.1 = (f32[48,1,64,64]{3,2,1,0:T(8,128)S(1)}, f32[48,1,64,64]{3,2,1,0:T(8,128)}, u32[]{:S(2)}) copy-start(f32[48,1,64,64]{3,2,1,0:T(8,128)} %param.23) | copy-start | bytes 2359300
  0.7 5.7 %copy-start.3 = (bf16[2048,64]{0,1:T(8,128)(2,1)S(1)}, bf16[2048,64]{0,1:T(8,128)(2,1)}, u32[]{:S(2)}) copy-start(bf16[2048,64]{0,1:T(8,128)(2,1)} %param.28) | copy-start | bytes 786436
  0.7 13.9 %copy-start.8 = (s32[48,4]{0,1:T(4,128)S(1)}, s32[48,4]{0,1:T(4,128)}, u32[]{:S(2)}) copy-start(s32[48,4]{0,1:T(4,128)} %param.31) | copy-start | bytes 2308
  4.1 18.7 %copy-start.4 = (bf16[1024,128]{1,0:T(8,128)(2,1)S(1)}, bf16[1024,128]{1,0:T(8,128)(2,1)}, u32[]{:S(2)}) copy-start(bf16[1024,128]{1,0:T(8,128)(2,1)} %param.29) | copy-start | bytes 786436
  6.6 30.3 %copy-start.7 = (f32[2048]{0:T(1024)S(1)}, f32[2048]{0:T(1024)}, u32[]{:S(2)}) copy-start(f32[2048]{0:T(1024)} %param.30) | copy-start | bytes 24580
  7.5 14.9 %all-to-all-start = ((bf16[16,2,1536]{2,1,0:T(2,128)(2,1)}), bf16[16,2,1536]{2,1,0:T(2,128)(2,1)S(1)}, u32[]{:S(2)}, u32[]{:S(2)}) async-start(bf16[16,2,1536]{2,1,0:T(2,128)(2,1)} %reshape.417), calls=%async_computation | async-start | bytes 196608 | tf_op jit(solution)/shard_map/all_to_all | solution.py:21
  23.7 12.9 %all-to-all-start.1 = ((f32[16,48,128]{2,1,0:T(8,128)}), f32[16,48,128]{2,1,0:T(8,128)S(1)}, u32[]{:S(2)}, u32[]{:S(2)}) async-start(f32[16,48,128]{2,1,0:T(8,128)} %broadcast_in_dim.9), calls=%async_computation.1 | async-start | bytes 786432 | tf_op jit(solution)/shard_map/all_to_all | solution.py:21
  75.9 4.7 %copy-start.11 = (bf16[64,16]{0,1:T(8,128)(2,1)S(1)}, bf16[64,16]{0,1:T(8,128)(2,1)}, u32[]{:S(2)}) copy-start(bf16[64,16]{0,1:T(8,128)(2,1)} %param.40) | copy-start | bytes 6148
  75.9 4.7 %copy-start.12 = (bf16[64,16]{0,1:T(8,128)(2,1)S(1)}, bf16[64,16]{0,1:T(8,128)(2,1)}, u32[]{:S(2)}) copy-start(bf16[64,16]{0,1:T(8,128)(2,1)} %param.39) | copy-start | bytes 6148
  75.9 42.4 %all-to-all-start.3 = ((bf16[16,128,5,128]{3,1,2,0:T(8,128)(2,1)}), bf16[16,128,5,128]{3,1,2,0:T(8,128)(2,1)S(1)}, u32[]{:S(2)}, u32[]{:S(2)}) async-start(bf16[16,128,5,128]{3,1,2,0:T(8,128)(2,1)} %broadcast_in_dim.10), calls=%async_computation.3 | async-start | bytes 5242880 | tf_op jit(solution)/shard_map/all_to_all | solution.py:21
  125.0 2.7 %copy-start.14 = (bf16[4,2048,32]{1,2,0:T(8,128)(2,1)S(1)}, bf16[4,2048,32]{1,2,0:T(8,128)(2,1)}, u32[]{:S(2)}) copy-start(bf16[4,2048,32]{1,2,0:T(8,128)(2,1)} %param.34) | copy-start | bytes 1572868
  129.9 8.2 %copy-start.9 = (s32[48,4]{0,1:T(4,128)S(1)}, s32[48,4]{0,1:T(4,128)}, u32[]{:S(2)}) copy-start(s32[48,4]{0,1:T(4,128)} %param.31) | copy-start | bytes 2308
  129.9 8.1 %copy-start.10 = (s32[48,4]{0,1:T(4,128)S(1)}, s32[48,4]{0,1:T(4,128)}, u32[]{:S(2)}) copy-start(s32[48,4]{0,1:T(4,128)} %copy.65) | copy-start | bytes 2308
  133.0 18.5 %all-to-all-start.4 = ((bf16[16,2,10240]{2,1,0:T(2,128)(2,1)}), bf16[16,2,10240]{2,1,0:T(2,128)(2,1)}, u32[]{:S(2)}, u32[]{:S(2)}) async-start(bf16[16,2,10240]{2,1,0:T(2,128)(2,1)} %reshape.419), calls=%async_computation.4 | async-start | bytes 1310720 | tf_op jit(solution)/shard_map/all_to_all | solution.py:21
  160.6 32.7 %copy-start.15 = (f32[48,4]{0,1:T(4,128)S(1)}, f32[48,4]{0,1:T(4,128)}, u32[]{:S(2)}) copy-start(f32[48,4]{0,1:T(4,128)} %param.32) | copy-start | bytes 2308
  162.0 31.6 %copy-start.5 = (bf16[512,128]{1,0:T(8,128)(2,1)S(1)}, bf16[512,128]{1,0:T(8,128)(2,1)}, u32[]{:S(2)}) copy-start(bf16[512,128]{1,0:T(8,128)(2,1)} %param.38) | copy-start | bytes 393220
  162.0 31.8 %copy-start.6 = (bf16[256,128]{1,0:T(8,128)(2,1)S(1)}, bf16[256,128]{1,0:T(8,128)(2,1)}, u32[]{:S(2)}) copy-start(bf16[256,128]{1,0:T(8,128)(2,1)} %param.41) | copy-start | bytes 196612
  162.0 50.7 %copy-start.13 = (f32[128]{0:T(128)S(1)}, f32[128]{0:T(128)}, u32[]{:S(2)}) copy-start(f32[128]{0:T(128)} %param.43) | copy-start | bytes 1540
  162.9 30.3 %all-to-all-start.5 = ((bf16[128,5,128]{2,1,0:T(8,128)(2,1)}), bf16[128,5,128]{2,1,0:T(8,128)(2,1)S(1)}, u32[]{:S(2)}, u32[]{:S(2)}) async-start(bf16[128,5,128]{2,1,0:T(8,128)(2,1)} %copy.72), calls=%async_computation.5 | async-start | bytes 524288 | tf_op jit(solution)/shard_map/all_to_all | solution.py:225
where the time goes:
time: 214 us; the launch traced here: 213 us
  blocking collectives  106 us (50%)
  waiting for transfers between devices  29.9 us (14%)
  local copies, waits for them, and re-layouts  29.6 us (14%)
  starting transfers between devices  26.3 us (12%)
  matrix products  14.2 us (7%)
  other arithmetic  6.02 us (3%)
    all_to_all x1, blocking collectives, on_device(): lax.all_to_all(outgoing.reshape(expert_count, capacity, col_count), 'ep',...  36.1 us
    all_to_all x4, waiting for transfers between devices, from_everyone(): lax.all_to_all(jnp.broadcast_to(shard[None], (length, *shard.shape)), axi...  29.9 us
    all_gather x1, blocking collectives, in_one_piece(): lax.all_gather(both, axis, axis=dim, tiled=True)  29.6 us
    all_gather x1, blocking collectives, one_gather(): lines, at, finished = (lax.all_gather(line, axis), 0, [])  21.7 us
    all_to_all x4, starting transfers between devices, from_everyone(): lax.all_to_all(jnp.broadcast_to(shard[None], (length, *shard.shape)), axi...  19.4 us
    psum x2, blocking collectives, by_axis(): return functools.reduce(lax.psum, axes, shard)  18.7 us
    unnamed x43, local copies, waits for them, and re-layouts  10.4 us
    all_to_all x1, starting transfers between devices, on_device(): lax.all_to_all(result.reshape(ep_count * local_experts, slot_count, col_c...  6.89 us
  transfers between devices with their start and end apart: 5, of which 4 were waited for; matrix products, arithmetic and copies ran while one was open for 5% of the time, Pallas kernels for 0%

commit v1 on v0

v1 whole, which is shorter than its diff:
```python
import jax
import jax.numpy as jnp
from jax import lax
from jax.sharding import Mesh
from jax.sharding import PartitionSpec as P

HEADS = 16
TP = ("tp_0", "tp_1")


RESIDUAL_SCALE = 2.0**0.25
NORM_EPS = 1e-05
GROUP_EPS = 1e-06
ROPE_BASE = 10000.0


def in_order(parts, dim):
    parts = jnp.moveaxis(parts, 0, dim)
    dims = parts.shape
    return parts.reshape(*dims[:dim], dims[dim] * dims[dim + 1], *dims[dim + 2 :])


def rotate(vector, positions):
    half_width = vector.shape[-1] // 2
    frequency = ROPE_BASE ** (-jnp.arange(half_width, dtype=jnp.float32) / half_width)
    angles = positions.astype(jnp.float32)[:, None, None] * frequency[None, None, :]
    cosine = jnp.cos(angles)
    sine_part = jnp.sin(angles)
    first_half = vector[..., :half_width]
    second_half = vector[..., half_width:]
    return jnp.concatenate(
        [
            first_half * cosine - second_half * sine_part,
            second_half * cosine + first_half * sine_part,
        ],
        -1,
    )


def retain(
    tokens,
    retention_state,
    lengths,
    query_weight,
    key_weight,
    value_weight,
    gate_weight,
    first_head,
):
    row_count = tokens.shape[0]
    head_count = retention_state.shape[1]
    head_width = retention_state.shape[2]

    def project(weight):
        rounded = jnp.dot(tokens, weight, preferred_element_type=jnp.float32).astype(jnp.bfloat16)
        return lax.optimization_barrier(rounded).astype(jnp.float32)

    queries = rotate(project(query_weight).reshape(row_count, head_count, head_width), lengths)
    key_rows = rotate(
        project(key_weight).reshape(row_count, head_count, head_width), lengths
    ) * head_width ** (-0.5)
    values = project(value_weight).reshape(row_count, head_count, head_width)
    gate_act = project(gate_weight)
    head_index = (first_head + jnp.arange(head_count)).astype(jnp.float32)
    decays = 1.0 - 2.0 ** (-5.0 - 7.0 * head_index / (HEADS - 1))
    own_term = jnp.sum(queries * key_rows, -1, keepdims=True) * values
    carried = decays[None, :, None] * jnp.einsum("bhd,bhde->bhe", queries, retention_state)
    result = own_term + carried
    new_state = (
        decays[None, :, None, None] * retention_state
        + key_rows[:, :, :, None] * values[:, :, None, :]
    )
    normed = result * lax.rsqrt(jnp.mean(result * result, -1, keepdims=True) + GROUP_EPS)
    mixed_heads = (
        normed.reshape(row_count, head_count * head_width) * jax.nn.silu(gate_act)
    ).astype(jnp.bfloat16)
    return (mixed_heads, new_state)


EP = ("z", "core")
PITCH = 24
RIDER = 8


def swap(parts, axis):
    return lax.all_to_all(parts, axis, 0, 0, tiled=True)


def to_all(shard, axis):
    length = lax.axis_size(axis)
    return swap(jnp.broadcast_to(shard[None], (length, *shard.shape)), axis)


def after(value, other):
    return lax.optimization_barrier((value, other))[0]


def normalize(rows, gain, axes):
    count = 1
    for a in axes:
        count *= rows.shape[a]
    mean = jnp.sum(rows, axes, keepdims=True) / count
    square = jnp.sum(rows * rows, axes, keepdims=True) / count
    return (rows - mean) * lax.rsqrt(square - mean * mean + NORM_EPS) * gain, mean, square


def f32_dot(a, b, dims):
    return lax.dot_general(a, b, (dims, ((), ())), preferred_element_type=jnp.float32)


def on_device(
    tokens,
    retention_state,
    lengths,
    query_weight,
    key_weight,
    value_weight,
    gate_weight,
    out_weight,
    first_gain,
    routing,
    route_weight,
    expert_gate,
    expert_up,
    expert_down,
    shared_gate,
    shared_up,
    shared_down,
    side_gate,
    side_up,
    side_down,
    side_switch,
    second_gain,
):
    bf16 = jnp.bfloat16
    seq_rows, model_width = tokens.shape
    head_count = retention_state.shape[1]
    col_count = out_weight.shape[1]
    ep_count = lax.axis_size(EP)
    tp_count = lax.axis_size(TP)
    class_count = lax.axis_size("tp_1")
    part_count = lax.axis_size("tp_0")
    local_experts = expert_gate.shape[0]
    hidden_cols = expert_gate.shape[2]
    top_count = routing.shape[1]
    capacity = (3 * seq_rows * top_count + local_experts * ep_count - 1) // (local_experts * ep_count)
    slots = ep_count * capacity
    tp_rank = lax.axis_index(TP)
    col_start = tp_rank * col_count

    mixed_heads, new_state = retain(
        tokens,
        retention_state,
        lengths,
        query_weight,
        key_weight,
        value_weight,
        gate_weight,
        tp_rank * head_count,
    )
    mixed_all = in_order(to_all(mixed_heads, TP), 1)

    same = routing.reshape(-1)[:, None] == routing.reshape(-1)[None, :]
    row_of = jnp.arange(seq_rows * top_count, dtype=jnp.int32) // top_count
    earlier = row_of[None, :] < row_of[:, None]
    position = jnp.sum((same & earlier).astype(jnp.int32), 1).reshape(seq_rows, top_count)
    slot_ids = (
        (routing // local_experts) * PITCH + (routing % local_experts) * capacity + position
    )
    wire_ids = jnp.arange(ep_count * PITCH, dtype=jnp.int32)
    table = jnp.zeros((ep_count * PITCH, seq_rows), jnp.bool_)
    for k in range(top_count):
        table = table | (wire_ids[:, None] == slot_ids[None, :, k])
    table = table.astype(bf16)
    slot_hot = (slot_ids.T.reshape(-1)[:, None] == wire_ids[None, :]).astype(bf16)

    lane = lax.axis_index("tp_1")
    gate_up = (jnp.swapaxes(expert_gate, 1, 2), jnp.swapaxes(expert_up, 1, 2))

    def piece_for(expert):
        return jnp.stack([lax.dynamic_index_in_dim(w, expert, 0, False) for w in gate_up])

    pieces = [piece_for(lane)]
    for d in range(1, class_count):
        steps = [(i, (i + d) % class_count) for i in range(class_count)]
        pieces.append(lax.ppermute(piece_for((lane + d) % class_count), "tp_1", steps))
    gate_t, up_t = (jnp.concatenate([p[i] for p in pieces], 0) for i in range(2))
    down = expert_down.reshape(local_experts, part_count, class_count, hidden_cols, col_count)
    down = jnp.stack(
        [
            jnp.concatenate([down[j, :, (j - d) % class_count] for d in range(class_count)], 1)
            for j in range(local_experts)
        ]
    )

    mixing = jnp.dot(mixed_all, out_weight, preferred_element_type=jnp.float32)
    own_cols = lax.dynamic_slice_in_dim(tokens, col_start, col_count, 1).astype(jnp.float32)
    pre_first = RESIDUAL_SCALE * own_cols + mixing
    pre_short = pre_first.astype(bf16)

    side_cols = side_gate.shape[1]
    side_rows = side_gate.shape[0]
    core_count = lax.axis_size("core")
    side_piece = jnp.concatenate([side_gate.T, side_up.T], 1)
    rider = jnp.broadcast_to(
        side_piece.reshape(1, core_count, RIDER, 2 * side_rows),
        (ep_count // core_count, core_count, RIDER, 2 * side_rows),
    ).reshape(ep_count, RIDER, 2 * side_rows)
    outgoing = jnp.dot(table, pre_short, preferred_element_type=jnp.float32).astype(bf16)
    arrived = swap(
        jnp.concatenate([outgoing.reshape(ep_count, PITCH, col_count), rider], 1), EP
    )
    side_own = arrived[:, PITCH:]
    side_other = lax.ppermute(side_own, "core", [(0, 1), (1, 0)])
    first_core = lax.axis_index("core") == 0
    side_all = jnp.concatenate(
        [
            jnp.where(first_core, side_own, side_other),
            jnp.where(first_core, side_other, side_own),
        ],
        1,
    ).reshape(ep_count, side_cols, 2, side_rows)
    side_all = jnp.transpose(side_all, (2, 1, 0, 3)).reshape(2, side_cols, model_width)

    order = jnp.arange(local_experts * slots, dtype=jnp.int32)
    source, expert, place = (order % slots) // capacity, order // slots, order % capacity
    spot = expert * capacity + place
    came_at = source * (PITCH + RIDER) + spot
    regroup = (
        came_at[:, None] == jnp.arange(ep_count * (PITCH + RIDER), dtype=jnp.int32)[None, :]
    ).astype(bf16)
    by_expert = jnp.dot(
        regroup, arrived.reshape(-1, col_count), preferred_element_type=jnp.float32
    ).astype(bf16)
    own_too = jnp.concatenate(
        [
            by_expert.reshape(local_experts, slots, col_count),
            jnp.broadcast_to(pre_short[None], (local_experts, seq_rows, col_count)),
        ],
        1,
    )
    to_send = jnp.broadcast_to(own_too[None], (part_count, *own_too.shape))
    rows_pre = swap(to_send.reshape(tp_count, slots + seq_rows, col_count), TP)
    gains = first_gain.reshape(tp_count, 1, col_count)
    parts, mean, square = normalize(rows_pre.astype(jnp.float32), gains, (0, 2))
    normed_rows = in_order(parts.astype(bf16), 1)
    slot_rows, normed_full = normed_rows[:slots], normed_rows[slots:]
    mean, square = mean[0, slots:], square[0, slots:]
    own_gain = lax.dynamic_slice_in_dim(first_gain, col_start, col_count, 0)
    normed_cols = (
        (pre_first - mean) * lax.rsqrt(square - mean * mean + NORM_EPS) * own_gain
    ).astype(bf16)

    across = ((1,), (1,))
    hidden = (
        jax.nn.silu(f32_dot(slot_rows, gate_t, across)) * f32_dot(slot_rows, up_t, across)
    ).astype(bf16)
    side_hidden = (
        jax.nn.silu(f32_dot(normed_full, side_all[0], across))
        * f32_dot(normed_full, side_all[1], across)
    ).astype(bf16)
    shared_hidden = (
        jax.nn.silu(jnp.dot(normed_full, shared_gate, preferred_element_type=jnp.float32))
        * jnp.dot(normed_full, shared_up, preferred_element_type=jnp.float32)
    ).astype(bf16)
    switch = jax.nn.sigmoid(jnp.dot(normed_full, side_switch, preferred_element_type=jnp.float32))

    shared_cols = shared_hidden.shape[1]
    units = hidden.shape[1]
    spare = units - shared_cols - side_cols
    local_hidden = jnp.concatenate(
        [shared_hidden, side_hidden, jnp.zeros((seq_rows, spare), bf16)], 1
    )
    hidden_all = to_all(jnp.concatenate([hidden, local_hidden], 0), TP)
    expert_hidden = hidden_all[:, :slots].reshape(part_count, class_count, slots, units)
    local_all = in_order(hidden_all[:, slots:], 1)
    result = jnp.einsum("qjrf,jqfd->jrd", expert_hidden, down, preferred_element_type=jnp.float32)
    goes_at = source * PITCH + spot
    sent_back = jnp.dot(
        (wire_ids[:, None] == goes_at[None, :]).astype(bf16),
        result.astype(bf16).reshape(local_experts * slots, col_count),
        preferred_element_type=jnp.float32,
    ).astype(bf16)
    returned = swap(sent_back.reshape(ep_count, PITCH, col_count), EP)

    shared_part = jnp.pad(
        shared_down.reshape(tp_count, shared_cols, col_count),
        ((0, 0), (0, units - shared_cols), (0, 0)),
    ).reshape(tp_count * units, col_count)
    side_part = jnp.pad(
        side_down.reshape(tp_count, side_cols, col_count),
        ((0, 0), (shared_cols, spare), (0, 0)),
    ).reshape(tp_count * units, col_count)
    shared_out = jnp.dot(local_all, shared_part, preferred_element_type=jnp.float32)
    side_out = jnp.dot(local_all, side_part, preferred_element_type=jnp.float32)
    local_sum = (
        RESIDUAL_SCALE * normed_cols.astype(jnp.float32) + shared_out + switch[:, None] * side_out
    )

    picked = jnp.dot(
        slot_hot, returned.reshape(-1, col_count), preferred_element_type=jnp.float32
    ).reshape(top_count, seq_rows, col_count)
    routed = jnp.sum(picked * route_weight.T[:, :, None], 0)
    pre_second = local_sum + routed
    sums = jnp.stack([jnp.sum(pre_second, -1), jnp.sum(pre_second * pre_second, -1)])
    totals = jnp.sum(to_all(sums, TP), 0)
    mean_second = totals[0][:, None] / model_width
    square_second = totals[1][:, None] / model_width
    output = (
        (pre_second - mean_second)
        * lax.rsqrt(square_second - mean_second * mean_second + NORM_EPS)
        * second_gain
    ).astype(bf16)
    return (output, new_state)


def solution(mesh):
    chips = mesh.devices.reshape(mesh.shape["ep"] // 2, 2, 4, 4)
    finer = Mesh(chips, (*EP, *TP))
    return jax.shard_map(
        on_device,
        mesh=finer,
        in_specs=(
            P(EP, None),
            P(EP, TP, None, None),
            P(EP),
            P(None, TP),
            P(None, TP),
            P(None, TP),
            P(None, TP),
            P(None, TP),
            P(),
            P(EP, None),
            P(EP, None),
            P(EP, None, TP),
            P(EP, None, TP),
            P(EP, None, TP),
            P(None, TP),
            P(None, TP),
            P(None, TP),
            P(EP, TP),
            P(EP, TP),
            P(None, TP),
            P(),
            P(TP),
        ),
        out_specs=(P(EP, TP), P(EP, TP, None, None)),
        check_vma=False,
    )
```

time: 214 us -> 160 us (0.75)
  the two profiles are of different devices: /device:TPU:32 before, /device:TPU:2 now
where the time goes in v1:
time: 160 us; the launch traced here: 159 us
  waiting for transfers between devices  68.7 us (43%)
  starting transfers between devices  55.2 us (34%)
  matrix products  15 us (9%)
  local copies, waits for them, and re-layouts  10.8 us (7%)
  other arithmetic  8.14 us (5%)
    all_to_all x6, waiting for transfers between devices, swap(): return lax.all_to_all(parts, axis, 0, 0, tiled=True)  68.7 us
    all_to_all x6, starting transfers between devices, swap(): return lax.all_to_all(parts, axis, 0, 0, tiled=True)  42.3 us
    ppermute x3, starting transfers between devices, on_device(): lax.ppermute(piece_for((lane + d) % class_count), 'tp_1', steps)  11 us
    dot_general x4, matrix products, project(): jnp.dot(tokens, weight, preferred_element_type=jnp.float32)  5.05 us
  transfers between devices with their start and end apart: 10, of which 5 were waited for; matrix products, arithmetic and copies ran while one was open for 10% of the time, Pallas kernels for 0%

profile of v1, /device:TPU:2, one launch (start us, length us, event | category | flops | bytes accessed | tf_op | source)
XLA Modules:
  0.0 159.4 jit_solution(6792488627475037966)
XLA Ops:
  0.7 0.8 convert_element_type.86
  1.5 1.3 convolution_convert_fusion.4
  2.7 1.3 convolution_convert_fusion.3
  4.0 1.3 convolution_convert_fusion.2
  5.3 1.3 convolution_convert_fusion.1
  7.6 0.8 reshape.561
  8.5 9.2 %all-to-all-start = ((bf16[16,2,1536]{2,1,0:T(2,128)(2,1)}), bf16[16,2,1536]{2,1,0:T(2,128)(2,1)S(1)}, u32[]{:S(2)}, u32[]{:S(2)}) async-start(bf16[16,2,1536]{2,1,0:T(2,128)(2,1)} %reshape.561), calls=%async_computation | async-start | bytes 196608 | tf_op jit(solution)/shard_map/all_to_all | solution.py:86
  17.7 0.8 dynamic-slice_bitcast_fusion
  18.5 0.7 pad_maximum_fusion.3
  19.3 2.2 %collective-permute-start.2 = (bf16[2,32,2048]{2,1,0:T(8,128)(2,1)}, bf16[2,32,2048]{2,1,0:T(8,128)(2,1)}, u32[]{:S(2)}, u32[]{:S(2)}) collective-permute-start(bf16[2,32,2048]{2,1,0:T(8,128)(2,1)} %pad_maximum_fusion.3), channel_id=1, source_target_pairs={{0,3},{1,0},{2,1},{3,2},{4,7},{5,4},{6,5},{7,6},{8,11},{9,8},{10,9... | collective-permute-start | bytes 786440 | tf_op jit(solution)/shard_map/ppermute | solution.py:186
  21.4 0.7 pad_maximum_fusion.1
  22.2 3.7 %collective-permute-start = (bf16[2,32,2048]{2,1,0:T(8,128)(2,1)}, bf16[2,32,2048]{2,1,0:T(8,128)(2,1)S(1)}, u32[]{:S(2)}, u32[]{:S(2)}) collective-permute-start(bf16[2,32,2048]{2,1,0:T(8,128)(2,1)} %pad_maximum_fusion.1), channel_id=1, source_target_pairs={{0,1},{1,2},{2,3},{3,0},{4,5},{5,6},{6,7},{7,4},{8,9},{9,10},{10,1... | collective-permute-start | bytes 786440 | tf_op jit(solution)/shard_map/ppermute | solution.py:186
  25.8 0.7 pad_maximum_fusion.2
  26.5 5.2 %collective-permute-start.1 = (bf16[2,32,2048]{2,1,0:T(8,128)(2,1)}, bf16[2,32,2048]{2,1,0:T(8,128)(2,1)S(1)}, u32[]{:S(2)}, u32[]{:S(2)}) collective-permute-start(bf16[2,32,2048]{2,1,0:T(8,128)(2,1)} %pad_maximum_fusion.2), channel_id=1, source_target_pairs={{0,2},{1,3},{2,0},{3,1},{4,6},{5,7},{6,4},{7,5},{8,10},{9,11},{10,... | collective-permute-start | bytes 786440 | tf_op jit(solution)/shard_map/ppermute | solution.py:186
  33.1 0.9 fusion.137
  34.3 0.7 pad_maximum_fusion
  35.0 13.8 %all-to-all-start.1 = ((bf16[32,32,128]{2,1,0:T(8,128)(2,1)}), bf16[32,32,128]{2,1,0:T(8,128)(2,1)S(1)}, u32[]{:S(2)}, u32[]{:S(2)}) async-start(bf16[32,32,128]{2,1,0:T(8,128)(2,1)} %pad_maximum_fusion), calls=%async_computation.1 | async-start | bytes 524288 | tf_op jit(solution)/shard_map/all_to_all | solution.py:86
  48.8 1.7 %slice_bitcast_fusion.8 = (bf16[32,2048]{1,0:T(8,128)(2,1)}, bf16[32,2048]{1,0:T(8,128)(2,1)}) fusion(bf16[2,32,2048]{2,1,0:T(8,128)(2,1)} %collective-permute-done.2), kind=kLoop, calls=%fused_computation.107 | loop fusion | bytes 524288 | tf_op jit(solution)/shard_map/squeeze | solution.py:187
  50.5 0.7 slice_bitcast_fusion.10
  51.2 20.2 %all-to-all-done.1 = bf16[32,32,128]{2,1,0:T(8,128)(2,1)S(1)} async-done(((bf16[32,32,128]{2,1,0:T(8,128)(2,1)}), bf16[32,32,128]{2,1,0:T(8,128)(2,1)S(1)}, u32[]{:S(2)}, u32[]{:S(2)}) %all-to-all-start.1) | async-done | bytes 262176 | tf_op jit(solution)/shard_map/all_to_all | solution.py:86
  71.5 1.9 %collective-permute-start.3 = (bf16[32,8,128]{2,1,0:T(8,128)(2,1)S(1)}, bf16[32,8,128]{2,1,0:T(8,128)(2,1)S(1)}, u32[]{:S(2)}, u32[]{:S(2)}) collective-permute-start(bf16[32,8,128]{2,1,0:T(8,128)(2,1)S(1)} %slice.192), channel_id=1, source_target_pairs={{0,16},{16,0},{1,17},{17,1},{2,18},{18,2},{3,19},{19,3},{4,20},{20... | collective-permute-start | bytes 196616 | tf_op jit(solution)/shard_map/ppermute | solution.py:214
  73.4 0.6 fusion.11
  74.0 1.0 broadcast_in_dim.20
  75.0 5.7 %all-to-all-start.2 = ((bf16[16,208,128]{2,1,0:T(8,128)(2,1)}), bf16[16,208,128]{2,1,0:T(8,128)(2,1)S(1)}, u32[]{:S(2)}, u32[]{:S(2)}) async-start(bf16[16,208,128]{2,1,0:T(8,128)(2,1)} %bitcast.18), calls=%async_computation.2 | async-start | bytes 1703936 | tf_op jit(solution)/shard_map/all_to_all | solution.py:86
  80.8 0.7 slice_bitcast_fusion.9
  81.7 0.4 fusion.136
  82.7 12.5 %all-to-all-done.2 = bf16[16,208,128]{2,1,0:T(8,128)(2,1)S(1)} async-done(((bf16[16,208,128]{2,1,0:T(8,128)(2,1)}), bf16[16,208,128]{2,1,0:T(8,128)(2,1)S(1)}, u32[]{:S(2)}, u32[]{:S(2)}) %all-to-all-start.2) | async-done | bytes 852000 | tf_op jit(solution)/shard_map/all_to_all | solution.py:86
  95.2 0.3 fusion.2
  95.5 0.4 fusion.25
  96.1 0.7 copy-done.2
  97.1 1.1 fusion.66
  98.2 1.1 fusion.18
  99.5 1.6 fusion.27
  101.1 0.3 fusion.12
  101.6 1.0 broadcast_in_dim.22
  102.6 4.9 %all-to-all-start.3 = ((bf16[16,208,128]{2,1,0:T(8,128)(2,1)}), bf16[16,208,128]{2,1,0:T(8,128)(2,1)S(1)}, u32[]{:S(2)}, u32[]{:S(2)}) async-start(bf16[16,208,128]{2,1,0:T(8,128)(2,1)} %broadcast_in_dim.22), calls=%async_computation.3 | async-start | bytes 1703936 | tf_op jit(solution)/shard_map/all_to_all | solution.py:86
  108.0 12.9 %all-to-all-done.3 = bf16[16,208,128]{2,1,0:T(8,128)(2,1)S(1)} async-done(((bf16[16,208,128]{2,1,0:T(8,128)(2,1)}), bf16[16,208,128]{2,1,0:T(8,128)(2,1)S(1)}, u32[]{:S(2)}, u32[]{:S(2)}) %all-to-all-start.3) | async-done | bytes 852000 | tf_op jit(solution)/shard_map/all_to_all | solution.py:86
  120.9 0.3 fusion.10
  121.3 1.2 fusion.9
  122.4 3.9 %all-to-all-start.4 = ((bf16[32,24,128]{2,1,0:T(8,128)(2,1)}), bf16[32,24,128]{2,1,0:T(8,128)(2,1)S(1)}, u32[]{:S(2)}, u32[]{:S(2)}) async-start(bf16[32,24,128]{2,1,0:T(8,128)(2,1)} %bitcast.74), calls=%async_computation.4 | async-start | bytes 393216 | tf_op jit(solution)/shard_map/all_to_all | solution.py:86
  126.5 1.1 fusion.23
  127.8 18.5 %all-to-all-done.4 = bf16[32,24,128]{2,1,0:T(8,128)(2,1)S(1)} async-done(((bf16[32,24,128]{2,1,0:T(8,128)(2,1)}), bf16[32,24,128]{2,1,0:T(8,128)(2,1)S(1)}, u32[]{:S(2)}, u32[]{:S(2)}) %all-to-all-start.4) | async-done | bytes 196640 | tf_op jit(solution)/shard_map/all_to_all | solution.py:86
  146.6 0.3 fusion.134
  146.9 0.6 broadcast_in_dim.23
  147.6 4.8 %all-to-all-start.5 = ((f32[16,2,48]{2,1,0:T(2,128)}), f32[16,2,48]{2,1,0:T(2,128)S(1)}, u32[]{:S(2)}, u32[]{:S(2)}) async-start(f32[16,2,48]{2,1,0:T(2,128)} %broadcast_in_dim.23), calls=%async_computation.5 | async-start | bytes 32768 | tf_op jit(solution)/shard_map/all_to_all | solution.py:86
  152.4 1.6 %multiply_add_fusion = f32[48,1,64,64]{3,2,1,0:T(8,128)} fusion(f32[48,1,64,64]{3,2,1,0:T(8,128)S(1)} %copy-done.1, f32[48,64]{1,0:T(8,128)S(1)} %convert_element_type.89, f32[48,64]{1,0:T(8,128)S(1)} %maximum_multiply_fusion.1, f32[]{:T(128)S(6)} %sub.107), kind=kLoop, calls=%fused_computation.13 | loop fusion | flops 589824 | bytes 1597444 | tf_op jit(solution)/shard_map/add | solution.py:70
  154.0 4.6 %all-to-all-done.5 = f32[16,2,48]{2,1,0:T(2,128)S(1)} async-done(((f32[16,2,48]{2,1,0:T(2,128)}), f32[16,2,48]{2,1,0:T(2,128)S(1)}, u32[]{:S(2)}, u32[]{:S(2)}) %all-to-all-start.5) | async-done | bytes 6176 | tf_op jit(solution)/shard_map/all_to_all | solution.py:86
  158.7 0.7 multiply_convert_fusion
  (110 shorter events, 5.2 us)
Async XLA Ops:
  0.6 32.4 %copy-start = (bf16[1024,128]{1,0:T(8,128)(2,1)S(1)}, bf16[1024,128]{1,0:T(8,128)(2,1)}, u32[]{:S(2)}) copy-start(bf16[1024,128]{1,0:T(8,128)(2,1)} %param.29) | copy-start | bytes 786436
  0.6 6.4 %copy-start.1 = (f32[48,1,64,64]{3,2,1,0:T(8,128)S(1)}, f32[48,1,64,64]{3,2,1,0:T(8,128)}, u32[]{:S(2)}) copy-start(f32[48,1,64,64]{3,2,1,0:T(8,128)} %param.23) | copy-start | bytes 2359300
  6.5 11.1 %copy-start.4 = (bf16[4,2048,32]{1,2,0:T(8,128)(2,1)S(1)}, bf16[4,2048,32]{1,2,0:T(8,128)(2,1)}, u32[]{:S(2)}) copy-start(bf16[4,2048,32]{1,2,0:T(8,128)(2,1)} %param.34) | copy-start | bytes 1572868
  6.6 11.1 %copy-start.5 = (bf16[4,2048,32]{1,2,0:T(8,128)(2,1)S(1)}, bf16[4,2048,32]{1,2,0:T(8,128)(2,1)}, u32[]{:S(2)}) copy-start(bf16[4,2048,32]{1,2,0:T(8,128)(2,1)} %param.33) | copy-start | bytes 1572868
  8.5 24.2 %all-to-all-start = ((bf16[16,2,1536]{2,1,0:T(2,128)(2,1)}), bf16[16,2,1536]{2,1,0:T(2,128)(2,1)S(1)}, u32[]{:S(2)}, u32[]{:S(2)}) async-start(bf16[16,2,1536]{2,1,0:T(2,128)(2,1)} %reshape.561), calls=%async_computation | async-start | bytes 196608 | tf_op jit(solution)/shard_map/all_to_all | solution.py:86
  17.7 14.1 %copy-start.17 = (s32[48,4]{0,1:T(4,128)S(1)}, s32[48,4]{0,1:T(4,128)}, u32[]{:S(2)}) copy-start(s32[48,4]{0,1:T(4,128)} %param.31) | copy-start | bytes 2308
  17.7 14.9 %copy-start.14 = (bf16[64,16]{0,1:T(8,128)(2,1)S(1)}, bf16[64,16]{0,1:T(8,128)(2,1)}, u32[]{:S(2)}) copy-start(bf16[64,16]{0,1:T(8,128)(2,1)} %param.40) | copy-start | bytes 6148
  17.7 14.9 %copy-start.15 = (bf16[64,16]{0,1:T(8,128)(2,1)S(1)}, bf16[64,16]{0,1:T(8,128)(2,1)}, u32[]{:S(2)}) copy-start(bf16[64,16]{0,1:T(8,128)(2,1)} %param.39) | copy-start | bytes 6148
  19.3 29.5 %collective-permute-start.2 = (bf16[2,32,2048]{2,1,0:T(8,128)(2,1)}, bf16[2,32,2048]{2,1,0:T(8,128)(2,1)}, u32[]{:S(2)}, u32[]{:S(2)}) collective-permute-start(bf16[2,32,2048]{2,1,0:T(8,128)(2,1)} %pad_maximum_fusion.3), channel_id=1, source_target_pairs={{0,3},{1,0},{2,1},{3,2},{4,7},{5,4},{6,5},{7,6},{8,11},{9,8},{10,9... | collective-permute-start | bytes 786440 | tf_op jit(solution)/shard_map/ppermute | solution.py:186
  22.2 28.4 %collective-permute-start = (bf16[2,32,2048]{2,1,0:T(8,128)(2,1)}, bf16[2,32,2048]{2,1,0:T(8,128)(2,1)S(1)}, u32[]{:S(2)}, u32[]{:S(2)}) collective-permute-start(bf16[2,32,2048]{2,1,0:T(8,128)(2,1)} %pad_maximum_fusion.1), channel_id=1, source_target_pairs={{0,1},{1,2},{2,3},{3,0},{4,5},{5,6},{6,7},{7,4},{8,9},{9,10},{10,1... | collective-permute-start | bytes 786440 | tf_op jit(solution)/shard_map/ppermute | solution.py:186
  26.5 54.2 %collective-permute-start.1 = (bf16[2,32,2048]{2,1,0:T(8,128)(2,1)}, bf16[2,32,2048]{2,1,0:T(8,128)(2,1)S(1)}, u32[]{:S(2)}, u32[]{:S(2)}) collective-permute-start(bf16[2,32,2048]{2,1,0:T(8,128)(2,1)} %pad_maximum_fusion.2), channel_id=1, source_target_pairs={{0,2},{1,3},{2,0},{3,1},{4,6},{5,7},{6,4},{7,5},{8,10},{9,11},{10,... | collective-permute-start | bytes 786440 | tf_op jit(solution)/shard_map/ppermute | solution.py:186
  35.0 36.5 %all-to-all-start.1 = ((bf16[32,32,128]{2,1,0:T(8,128)(2,1)}), bf16[32,32,128]{2,1,0:T(8,128)(2,1)S(1)}, u32[]{:S(2)}, u32[]{:S(2)}) async-start(bf16[32,32,128]{2,1,0:T(8,128)(2,1)} %pad_maximum_fusion), calls=%async_computation.1 | async-start | bytes 524288 | tf_op jit(solution)/shard_map/all_to_all | solution.py:86
  71.5 10.1 %collective-permute-start.3 = (bf16[32,8,128]{2,1,0:T(8,128)(2,1)S(1)}, bf16[32,8,128]{2,1,0:T(8,128)(2,1)S(1)}, u32[]{:S(2)}, u32[]{:S(2)}) collective-permute-start(bf16[32,8,128]{2,1,0:T(8,128)(2,1)S(1)} %slice.192), channel_id=1, source_target_pairs={{0,16},{16,0},{1,17},{17,1},{2,18},{18,2},{3,19},{19,3},{4,20},{20... | collective-permute-start | bytes 196616 | tf_op jit(solution)/shard_map/ppermute | solution.py:214
  75.0 20.1 %all-to-all-start.2 = ((bf16[16,208,128]{2,1,0:T(8,128)(2,1)}), bf16[16,208,128]{2,1,0:T(8,128)(2,1)S(1)}, u32[]{:S(2)}, u32[]{:S(2)}) async-start(bf16[16,208,128]{2,1,0:T(8,128)(2,1)} %bitcast.18), calls=%async_computation.2 | async-start | bytes 1703936 | tf_op jit(solution)/shard_map/all_to_all | solution.py:86
  81.7 13.8 %copy-start.13 = (f32[2048]{0:T(1024)S(1)}, f32[2048]{0:T(1024)}, u32[]{:S(2)}) copy-start(f32[2048]{0:T(1024)} %param.30) | copy-start | bytes 24580
  82.7 14.4 %copy-start.19 = (bf16[2048,32]{0,1:T(8,128)(2,1)S(1)}, bf16[2048,32]{0,1:T(8,128)(2,1)}, u32[]{:S(2)}) copy-start(bf16[2048,32]{0,1:T(8,128)(2,1)} %param.36) | copy-start | bytes 393220
  95.5 2.7 %copy-start.20 = (bf16[2048,32]{0,1:T(8,128)(2,1)S(1)}, bf16[2048,32]{0,1:T(8,128)(2,1)}, u32[]{:S(2)}) copy-start(bf16[2048,32]{0,1:T(8,128)(2,1)} %param.37) | copy-start | bytes 393220
  95.5 4.0 %copy-start.8 = (bf16[32,2048]{1,0:T(8,128)(2,1)S(1)}, bf16[32,2048]{1,0:T(8,128)(2,1)}, u32[]{:S(2)}) copy-start(bf16[32,2048]{1,0:T(8,128)(2,1)} %get-tuple-element.63) | copy-start | bytes 393220
  95.5 4.0 %copy-start.10 = (bf16[32,2048]{1,0:T(8,128)(2,1)S(1)}, bf16[32,2048]{1,0:T(8,128)(2,1)}, u32[]{:S(2)}) copy-start(bf16[32,2048]{1,0:T(8,128)(2,1)} %get-tuple-element.42) | copy-start | bytes 393220
  95.9 0.9 copy-start.2
  99.3 1.7 %copy-start.3 = (bf16[208,16,128]{2,0,1:T(8,128)(2,1)S(1)}, bf16[208,16,128]{2,0,1:T(8,128)(2,1)}, u32[]{:S(2)}) copy-start(bf16[208,16,128]{2,0,1:T(8,128)(2,1)} %copy-done.2) | copy-start | bytes 2555908
  99.4 1.7 %copy-start.7 = (bf16[32,2048]{1,0:T(8,128)(2,1)S(1)}, bf16[32,2048]{1,0:T(8,128)(2,1)}, u32[]{:S(2)}) copy-start(bf16[32,2048]{1,0:T(8,128)(2,1)} %get-tuple-element.32) | copy-start | bytes 393220
  99.4 1.7 %copy-start.9 = (bf16[32,2048]{1,0:T(8,128)(2,1)S(1)}, bf16[32,2048]{1,0:T(8,128)(2,1)}, u32[]{:S(2)}) copy-start(bf16[32,2048]{1,0:T(8,128)(2,1)} %get-tuple-element.43) | copy-start | bytes 393220
  99.4 1.7 %copy-start.11 = (bf16[32,2048]{1,0:T(8,128)(2,1)S(1)}, bf16[32,2048]{1,0:T(8,128)(2,1)}, u32[]{:S(2)}) copy-start(bf16[32,2048]{1,0:T(8,128)(2,1)} %get-tuple-element.39) | copy-start | bytes 393220
  99.5 1.6 %copy-start.12 = (bf16[32,2048]{1,0:T(8,128)(2,1)S(1)}, bf16[32,2048]{1,0:T(8,128)(2,1)}, u32[]{:S(2)}) copy-start(bf16[32,2048]{1,0:T(8,128)(2,1)} %get-tuple-element.41) | copy-start | bytes 393220
  101.5 6.2 %copy-start.16 = (bf16[2048]{0:T(1024)(128)(2,1)S(1)}, bf16[2048]{0:T(1024)(128)(2,1)}, u32[]{:S(2)}) copy-start(bf16[2048]{0:T(1024)(128)(2,1)} %param.42) | copy-start | bytes 12292
  101.5 6.3 %copy-start.6 = (bf16[4,512,128]{2,1,0:T(8,128)(2,1)S(1)}, bf16[4,512,128]{2,1,0:T(8,128)(2,1)}, u32[]{:S(2)}) copy-start(bf16[4,512,128]{2,1,0:T(8,128)(2,1)} %param.35) | copy-start | bytes 1572868
  102.6 18.2 %all-to-all-start.3 = ((bf16[16,208,128]{2,1,0:T(8,128)(2,1)}), bf16[16,208,128]{2,1,0:T(8,128)(2,1)S(1)}, u32[]{:S(2)}, u32[]{:S(2)}) async-start(bf16[16,208,128]{2,1,0:T(8,128)(2,1)} %broadcast_in_dim.22), calls=%async_computation.3 | async-start | bytes 1703936 | tf_op jit(solution)/shard_map/all_to_all | solution.py:86
  120.9 6.7 %copy-start.21 = (bf16[512,128]{1,0:T(8,128)(2,1)S(1)}, bf16[512,128]{1,0:T(8,128)(2,1)}, u32[]{:S(2)}) copy-start(bf16[512,128]{1,0:T(8,128)(2,1)} %param.38) | copy-start | bytes 393220
  121.3 25.0 %copy-start.23 = (f32[48,4]{0,1:T(4,128)S(1)}, f32[48,4]{0,1:T(4,128)}, u32[]{:S(2)}) copy-start(f32[48,4]{0,1:T(4,128)} %param.32) | copy-start | bytes 2308
  121.3 25.3 %copy-start.22 = (bf16[256,128]{1,0:T(8,128)(2,1)S(1)}, bf16[256,128]{1,0:T(8,128)(2,1)}, u32[]{:S(2)}) copy-start(bf16[256,128]{1,0:T(8,128)(2,1)} %param.41) | copy-start | bytes 196612
  122.4 23.8 %all-to-all-start.4 = ((bf16[32,24,128]{2,1,0:T(8,128)(2,1)}), bf16[32,24,128]{2,1,0:T(8,128)(2,1)S(1)}, u32[]{:S(2)}, u32[]{:S(2)}) async-start(bf16[32,24,128]{2,1,0:T(8,128)(2,1)} %bitcast.74), calls=%async_computation.4 | async-start | bytes 393216 | tf_op jit(solution)/shard_map/all_to_all | solution.py:86
  147.6 11.1 %all-to-all-start.5 = ((f32[16,2,48]{2,1,0:T(2,128)}), f32[16,2,48]{2,1,0:T(2,128)S(1)}, u32[]{:S(2)}, u32[]{:S(2)}) async-start(f32[16,2,48]{2,1,0:T(2,128)} %broadcast_in_dim.23), calls=%async_computation.5 | async-start | bytes 32768 | tf_op jit(solution)/shard_map/all_to_all | solution.py:86
  152.4 6.3 %copy-start.18 = (f32[128]{0:T(128)S(1)}, f32[128]{0:T(128)}, u32[]{:S(2)}) copy-start(f32[128]{0:T(128)} %param.43) | copy-start | bytes 1540

commit v2 on v1

--- a/solution.py
+++ b/solution.py
@@ -1,6 +1,8 @@
 import jax
 import jax.numpy as jnp
 from jax import lax
+from jax.experimental import pallas as pl
+from jax.experimental.pallas import tpu as pltpu
 from jax.sharding import Mesh
 from jax.sharding import PartitionSpec as P
 
@@ -12,6 +14,7 @@
 NORM_EPS = 1e-05
 GROUP_EPS = 1e-06
 ROPE_BASE = 10000.0
+ACROSS = ((1,), (1,))
 
 
 def in_order(parts, dim):
@@ -37,6 +40,39 @@
     )
 
 
+def project_kernel(tokens, *refs):
+    weights, out, total = refs[:-2], refs[-2], refs[-1]
+    step = pl.program_id(0)
+
+    @pl.when(step == 0)
+    def _():
+        total[...] = jnp.zeros_like(total)
+
+    stacked = jnp.concatenate([w[...] for w in weights], 0)
+    total[...] += f32_dot(tokens[...], stacked, ACROSS)
+
+    @pl.when(step == pl.num_programs(0) - 1)
+    def _():
+        out[...] = total[...].astype(out.dtype)
+
+
+def project_all(tokens, weights):
+    rows, width = tokens.shape
+    cols = weights[0].shape[1]
+    steps = 4
+    span = width // steps
+    return pl.pallas_call(
+        project_kernel,
+        grid=(steps,),
+        in_specs=[pl.BlockSpec((rows, span), lambda i: (0, i))]
+        + [pl.BlockSpec((cols, span), lambda i: (0, i)) for _ in weights],
+        out_specs=pl.BlockSpec((rows, cols * len(weights)), lambda i: (0, 0)),
+        out_shape=jax.ShapeDtypeStruct((rows, cols * len(weights)), jnp.bfloat16),
+        scratch_shapes=[pltpu.VMEM((rows, cols * len(weights)), jnp.float32)],
+        name="project",
+    )(tokens, *[w.T for w in weights])
+
+
 def retain(
     tokens,
     retention_state,
@@ -51,16 +87,12 @@
     head_count = retention_state.shape[1]
     head_width = retention_state.shape[2]
 
-    def project(weight):
-        rounded = jnp.dot(tokens, weight, preferred_element_type=jnp.float32).astype(jnp.bfloat16)
-        return lax.optimization_barrier(rounded).astype(jnp.float32)
-
-    queries = rotate(project(query_weight).reshape(row_count, head_count, head_width), lengths)
-    key_rows = rotate(
-        project(key_weight).reshape(row_count, head_count, head_width), lengths
-    ) * head_width ** (-0.5)
-    values = project(value_weight).reshape(row_count, head_count, head_width)
-    gate_act = project(gate_weight)
+    projected = project_all(tokens, (query_weight, key_weight, value_weight, gate_weight))
+    queries, keys, values, gate_act = jnp.split(projected.astype(jnp.float32), 4, 1)
+    by_head = (row_count, head_count, head_width)
+    queries = rotate(queries.reshape(by_head), lengths)
+    key_rows = rotate(keys.reshape(by_head), lengths) * head_width ** (-0.5)
+    values = values.reshape(by_head)
     head_index = (first_head + jnp.arange(head_count)).astype(jnp.float32)
     decays = 1.0 - 2.0 ** (-5.0 - 7.0 * head_index / (HEADS - 1))
     own_term = jnp.sum(queries * key_rows, -1, keepdims=True) * values
@@ -91,21 +123,60 @@
     return swap(jnp.broadcast_to(shard[None], (length, *shard.shape)), axis)
 
 
-def after(value, other):
-    return lax.optimization_barrier((value, other))[0]
-
-
-def normalize(rows, gain, axes):
-    count = 1
-    for a in axes:
-        count *= rows.shape[a]
-    mean = jnp.sum(rows, axes, keepdims=True) / count
-    square = jnp.sum(rows * rows, axes, keepdims=True) / count
-    return (rows - mean) * lax.rsqrt(square - mean * mean + NORM_EPS) * gain, mean, square
-
-
 def f32_dot(a, b, dims):
     return lax.dot_general(a, b, (dims, ((), ())), preferred_element_type=jnp.float32)
+
+
+def hidden_kernel(rows_pre, gains, pre_first, own_gain, local_weights, *refs):
+    pieces, (hidden, normed_cols, switch, normed) = refs[:-4], refs[-4:]
+    parts, row_count, cols = rows_pre.shape
+    own_rows = pre_first.shape[0]
+    slots = row_count - own_rows
+    width = parts * cols
+    total = jnp.zeros((row_count, cols), jnp.float32)
+    total_square = jnp.zeros((row_count, cols), jnp.float32)
+    for t in range(parts):
+        block = rows_pre[t].astype(jnp.float32)
+        total = total + block
+        total_square = total_square + block * block
+    mean = jnp.sum(total, -1, keepdims=True) / width
+    square = jnp.sum(total_square, -1, keepdims=True) / width
+    scale = lax.rsqrt(square - mean * mean + NORM_EPS)
+    for t in range(parts):
+        block = (rows_pre[t].astype(jnp.float32) - mean) * scale * gains[t : t + 1]
+        normed[:, t * cols : (t + 1) * cols] = block.astype(normed.dtype)
+    normed_cols[...] = ((pre_first[...] - mean[slots:]) * scale[slots:] * own_gain[...]).astype(
+        normed_cols.dtype
+    )
+    gate_up = jnp.concatenate([p[i] for i in range(2) for p in pieces], 0)
+    units = gate_up.shape[0] // 2
+    both = f32_dot(normed[:slots], gate_up, ACROSS)
+    hidden[:slots] = (jax.nn.silu(both[:, :units]) * both[:, units:]).astype(hidden.dtype)
+    local = f32_dot(normed[slots:], local_weights[...], ACROSS)
+    cut = (local.shape[1] - RIDER) // 2
+    mine = jax.nn.silu(local[:, :cut]) * local[:, cut : 2 * cut]
+    hidden[slots:] = jnp.zeros((own_rows, units), hidden.dtype)
+    hidden[slots:, :cut] = mine.astype(hidden.dtype)
+    switch[...] = jax.nn.sigmoid(local[:, 2 * cut : 2 * cut + 1])
+
+
+def hidden_units(rows_pre, gains, pre_first, own_gain, local_weights, pieces):
+    parts, row_count, cols = rows_pre.shape
+    units = sum(p.shape[1] for p in pieces)
+    own_rows = pre_first.shape[0]
+    whole = pl.BlockSpec(memory_space=pltpu.VMEM)
+    return pl.pallas_call(
+        hidden_kernel,
+        in_specs=[whole] * (5 + len(pieces)),
+        out_specs=[whole] * 3,
+        out_shape=[
+            jax.ShapeDtypeStruct((row_count, units), jnp.bfloat16),
+            jax.ShapeDtypeStruct((own_rows, cols), jnp.bfloat16),
+            jax.ShapeDtypeStruct((own_rows, 1), jnp.float32),
+        ],
+        scratch_shapes=[pltpu.VMEM((row_count, parts * cols), jnp.bfloat16)],
+        name="hidden_units",
+    )(rows_pre, gains, pre_first, own_gain, local_weights, *pieces)
 
 
 def on_device(
@@ -158,7 +229,21 @@
         gate_weight,
         tp_rank * head_count,
     )
-    mixed_all = in_order(to_all(mixed_heads, TP), 1)
+    head_width = mixed_heads.shape[1]
+    half = seq_rows // 2
+    folded = jnp.concatenate([mixed_heads[:half], mixed_heads[half:]], 1)
+    folded_all = to_all(folded, TP)
+    left = jnp.arange(2 * head_width, dtype=jnp.int32)[None, None, :] < head_width
+    none = jnp.zeros_like(folded_all)
+    mixed_all = in_order(
+        jnp.concatenate(
+            [jnp.where(left, folded_all, none), jnp.where(left, none, folded_all)], 1
+        ),
+        1,
+    )
+    head_weight = out_weight.reshape(tp_count, 1, head_width, col_count)
+    head_weight = jnp.broadcast_to(head_weight, (tp_count, 2, head_width, col_count))
+    head_weight = head_weight.reshape(tp_count * 2 * head_width, col_count)
 
     same = routing.reshape(-1)[:, None] == routing.reshape(-1)[None, :]
     row_of = jnp.arange(seq_rows * top_count, dtype=jnp.int32) // top_count
@@ -184,7 +269,6 @@
     for d in range(1, class_count):
         steps = [(i, (i + d) % class_count) for i in range(class_count)]
         pieces.append(lax.ppermute(piece_for((lane + d) % class_count), "tp_1", steps))
-    gate_t, up_t = (jnp.concatenate([p[i] for p in pieces], 0) for i in range(2))
     down = expert_down.reshape(local_experts, part_count, class_count, hidden_cols, col_count)
     down = jnp.stack(
         [
@@ -193,7 +277,7 @@
         ]
     )
 
-    mixing = jnp.dot(mixed_all, out_weight, preferred_element_type=jnp.float32)
+    mixing = jnp.dot(mixed_all, head_weight, preferred_element_type=jnp.float32)
     own_cols = lax.dynamic_slice_in_dim(tokens, col_start, col_count, 1).astype(jnp.float32)
     pre_first = RESIDUAL_SCALE * own_cols + mixing
     pre_short = pre_first.astype(bf16)
@@ -207,9 +291,7 @@
         (ep_count // core_count, core_count, RIDER, 2 * side_rows),
     ).reshape(ep_count, RIDER, 2 * side_rows)
     outgoing = jnp.dot(table, pre_short, preferred_element_type=jnp.float32).astype(bf16)
-    arrived = swap(
-        jnp.concatenate([outgoing.reshape(ep_count, PITCH, col_count), rider], 1), EP
-    )
+    arrived = swap(jnp.concatenate([outgoing.reshape(ep_count, PITCH, col_count), rider], 1), EP)
     side_own = arrived[:, PITCH:]
     side_other = lax.ppermute(side_own, "core", [(0, 1), (1, 0)])
     first_core = lax.axis_index("core") == 0
@@ -241,37 +323,25 @@
     )
     to_send = jnp.broadcast_to(own_too[None], (part_count, *own_too.shape))
     rows_pre = swap(to_send.reshape(tp_count, slots + seq_rows, col_count), TP)
-    gains = first_gain.reshape(tp_count, 1, col_count)
-    parts, mean, square = normalize(rows_pre.astype(jnp.float32), gains, (0, 2))
-    normed_rows = in_order(parts.astype(bf16), 1)
-    slot_rows, normed_full = normed_rows[:slots], normed_rows[slots:]
-    mean, square = mean[0, slots:], square[0, slots:]
     own_gain = lax.dynamic_slice_in_dim(first_gain, col_start, col_count, 0)
-    normed_cols = (
-        (pre_first - mean) * lax.rsqrt(square - mean * mean + NORM_EPS) * own_gain
-    ).astype(bf16)
-
-    across = ((1,), (1,))
-    hidden = (
-        jax.nn.silu(f32_dot(slot_rows, gate_t, across)) * f32_dot(slot_rows, up_t, across)
-    ).astype(bf16)
-    side_hidden = (
-        jax.nn.silu(f32_dot(normed_full, side_all[0], across))
-        * f32_dot(normed_full, side_all[1], across)
-    ).astype(bf16)
-    shared_hidden = (
-        jax.nn.silu(jnp.dot(normed_full, shared_gate, preferred_element_type=jnp.float32))
-        * jnp.dot(normed_full, shared_up, preferred_element_type=jnp.float32)
-    ).astype(bf16)
-    switch = jax.nn.sigmoid(jnp.dot(normed_full, side_switch, preferred_element_type=jnp.float32))
-
-    shared_cols = shared_hidden.shape[1]
-    units = hidden.shape[1]
+    units = class_count * hidden_cols
+    shared_cols = shared_gate.shape[1]
     spare = units - shared_cols - side_cols
-    local_hidden = jnp.concatenate(
-        [shared_hidden, side_hidden, jnp.zeros((seq_rows, spare), bf16)], 1
-    )
-    hidden_all = to_all(jnp.concatenate([hidden, local_hidden], 0), TP)
+    local_weights = jnp.concatenate(
+        [
+            shared_gate.T,
+            side_all[0],
+            shared_up.T,
+            side_all[1],
+            jnp.broadcast_to(side_switch[None], (RIDER, model_width)),
+        ],
+        0,
+    )
+    hidden, normed_cols, switch = hidden_units(
+        rows_pre, first_gain.reshape(tp_count, col_count), pre_first, own_gain[None], local_weights, pieces
+    )
+
+    hidden_all = to_all(hidden, TP)
     expert_hidden = hidden_all[:, :slots].reshape(part_count, class_count, slots, units)
     local_all = in_order(hidden_all[:, slots:], 1)
     result = jnp.einsum("qjrf,jqfd->jrd", expert_hidden, down, preferred_element_type=jnp.float32)
@@ -294,7 +364,7 @@
     shared_out = jnp.dot(local_all, shared_part, preferred_element_type=jnp.float32)
     side_out = jnp.dot(local_all, side_part, preferred_element_type=jnp.float32)
     local_sum = (
-        RESIDUAL_SCALE * normed_cols.astype(jnp.float32) + shared_out + switch[:, None] * side_out
+        RESIDUAL_SCALE * normed_cols.astype(jnp.float32) + shared_out + switch * side_out
     )
 
     picked = jnp.dot(
@@ -317,6 +387,7 @@
 def solution(mesh):
     chips = mesh.devices.reshape(mesh.shape["ep"] // 2, 2, 4, 4)
     finer = Mesh(chips, (*EP, *TP))
+
     return jax.shard_map(
         on_device,
         mesh=finer,

time: 160 us -> 154 us (0.963)
  matrix products: 15 us -> 5.05 us
  waiting for transfers between devices: 68.7 us -> 62 us
  Pallas kernels: 0 us -> 6.53 us
  local copies, waits for them, and re-layouts: 10.8 us -> 12.5 us
  other arithmetic: 8.14 us -> 9.81 us
    dot_general x12 -> x1, matrix products: 11.5 us -> 1.55 us  [on_device(): mixing = jnp.dot(mixed_all, head_weight, preferred_element_type=jnp.float32)]
    all_to_all x6, waiting for transfers between devices: 68.7 us -> 62 us  [swap(): return lax.all_to_all(parts, axis, 0, 0, tiled=True)]
    pallas_call x0 -> x2, Pallas kernels: none -> 6.53 us  [the longest x1 3.34 us: project_all(): pl.pallas_call(project_kernel, grid=(steps,), in_specs=[pl.BlockSpec((row...]
    squeeze x4 -> x0, local copies, waits for them, and re-layouts: 3.98 us -> none  [the longest x3 3.15 us: on_device(): p[i]]
    unnamed x52 -> x43, local copies, waits for them, and re-layouts: 1.97 us -> 4.57 us
    all_to_all x6, starting transfers between devices: 42.3 us -> 44 us  [swap(): return lax.all_to_all(parts, axis, 0, 0, tiled=True)]
  transfers between devices with their start and end apart: 10 -> 10, of which waited for: 5 -> 5; matrix products, arithmetic and copies ran while one was open for 10% -> 12% of each run, Pallas kernels for 0% -> 0%
where the time goes in v2:
time: 154 us
  waiting for transfers between devices  62 us (40%)
  starting transfers between devices  56.4 us (37%)
  local copies, waits for them, and re-layouts  12.5 us (8%)
  other arithmetic  9.81 us (6%)
  Pallas kernels  6.53 us (4%)
  matrix products  5.05 us (3%)
    all_to_all x6, waiting for transfers between devices, swap(): return lax.all_to_all(parts, axis, 0, 0, tiled=True)  62 us
    all_to_all x6, starting transfers between devices, swap(): return lax.all_to_all(parts, axis, 0, 0, tiled=True)  44 us
    ppermute x3, starting transfers between devices, on_device(): lax.ppermute(piece_for((lane + d) % class_count), 'tp_1', steps)  10.5 us
    unnamed x43, local copies, waits for them, and re-layouts  4.57 us
    pallas_call x1, Pallas kernels, project_all(): pl.pallas_call(project_kernel, grid=(steps,), in_specs=[pl.BlockSpec((row...  3.34 us
    pallas_call x1, Pallas kernels, hidden_units(): pl.pallas_call(hidden_kernel, in_specs=[whole] * (5 + len(pieces)), out_s...  3.19 us
    broadcast_in_dim x3, local copies, waits for them, and re-layouts, to_all(): return swap(jnp.broadcast_to(shard[None], (length, *shard.shape)), axis)  3.14 us
  transfers between devices with their start and end apart: 10, of which 5 were waited for; matrix products, arithmetic and copies ran while one was open for 12% of the time, Pallas kernels for 0%

profile of v2, /device:TPU:2, one launch (start us, length us, event | category | flops | bytes accessed | tf_op | source)
XLA Modules:
  0.0 153.5 jit_solution(8715534792078514274)
XLA Ops:
  0.7 3.3 %project.1 = bf16[48,256]{1,0:T(8,128)(2,1)} custom-call(bf16[48,2048]{1,0:T(8,128)(2,1)} %tokens.1, bf16[64,2048]{1,0:T(8,128)(2,1)} %bitcast.207, bf16[64,2048]{1,0:T(8,128)(2,1)} %bitcast.208, bf16[64,2048]{1,0:T(8,128)(2,1)} %bitcast.209, bf16[64,2048]{1,0:T(8,128)(2,1)} %bitcast.210), custom_call_target="tpu_custom_call" | custom-call | tf_op jit(solution)/shard_map/project/pallas_call | solution.py:64
  4.0 0.8 convert_element_type.51
  4.9 0.7 convert_element_type.52
  6.0 0.3 fusion.86
  6.7 0.7 broadcast_in_dim.38
  7.4 9.8 %all-to-all-start = ((bf16[16,24,128]{2,1,0:T(8,128)(2,1)}), bf16[16,24,128]{2,1,0:T(8,128)(2,1)}, u32[]{:S(2)}, u32[]{:S(2)}) async-start(bf16[16,24,128]{2,1,0:T(8,128)(2,1)} %broadcast_in_dim.38), calls=%async_computation | async-start | bytes 196608 | tf_op jit(solution)/shard_map/all_to_all | solution.py:118
  17.3 0.7 pad_maximum_fusion.2
  18.0 3.4 %collective-permute-start.1 = (bf16[2,32,2048]{2,1,0:T(8,128)(2,1)}, bf16[2,32,2048]{2,1,0:T(8,128)(2,1)}, u32[]{:S(2)}, u32[]{:S(2)}) collective-permute-start(bf16[2,32,2048]{2,1,0:T(8,128)(2,1)} %pad_maximum_fusion.2), channel_id=1, source_target_pairs={{0,1},{1,2},{2,3},{3,0},{4,5},{5,6},{6,7},{7,4},{8,9},{9,10},{10,1... | collective-permute-start | bytes 786440 | tf_op jit(solution)/shard_map/ppermute | solution.py:271
  21.4 0.7 pad_maximum_fusion.3
  22.1 2.8 %collective-permute-start.2 = (bf16[2,32,2048]{2,1,0:T(8,128)(2,1)}, bf16[2,32,2048]{2,1,0:T(8,128)(2,1)}, u32[]{:S(2)}, u32[]{:S(2)}) collective-permute-start(bf16[2,32,2048]{2,1,0:T(8,128)(2,1)} %pad_maximum_fusion.3), channel_id=1, source_target_pairs={{0,2},{1,3},{2,0},{3,1},{4,6},{5,7},{6,4},{7,5},{8,10},{9,11},{10,... | collective-permute-start | bytes 786440 | tf_op jit(solution)/shard_map/ppermute | solution.py:271
  25.9 0.9 broadcast_select_fusion.1
  26.9 1.5 %fusion.85 = (bf16[48,128]{1,0:T(8,128)(2,1)S(1)}, f32[48,128]{1,0:T(8,128)}) fusion(bf16[2048,128]{1,0:T(8,128)(2,1)S(1)} %bitcast.205, bf16[48,2048]{1,0:T(8,128)(2,1)} %tokens.1, s32[]{:T(128)S(6)} %select_n.144, bf16[16,24,128]{2,1,0:T(8,128)(2,1)S(1)} %get-tuple-element.45, bf16[16,24,128]{2,1,0:T(8,128)(2,1)S(1)} %get-tuple-element.44), kind=kOutput, calls=%fused_computation.185 | convolution fusion | flops 25583616 | bytes 770052 | tf_op jit(solution)/shard_map/dot_general | solution.py:280
  28.4 0.3 convolution_convert_fusion
  28.7 0.7 pad_maximum_fusion
  29.5 13.1 %all-to-all-start.1 = ((bf16[32,32,128]{2,1,0:T(8,128)(2,1)}), bf16[32,32,128]{2,1,0:T(8,128)(2,1)S(1)}, u32[]{:S(2)}, u32[]{:S(2)}) async-start(bf16[32,32,128]{2,1,0:T(8,128)(2,1)} %pad_maximum_fusion), calls=%async_computation.1 | async-start | bytes 524288 | tf_op jit(solution)/shard_map/all_to_all | solution.py:118
  42.5 0.7 pad_maximum_fusion.4
  43.3 4.3 %collective-permute-start.3 = (bf16[2,32,2048]{2,1,0:T(8,128)(2,1)}, bf16[2,32,2048]{2,1,0:T(8,128)(2,1)S(1)}, u32[]{:S(2)}, u32[]{:S(2)}) collective-permute-start(bf16[2,32,2048]{2,1,0:T(8,128)(2,1)} %pad_maximum_fusion.4), channel_id=1, source_target_pairs={{0,3},{1,0},{2,1},{3,2},{4,7},{5,4},{6,5},{7,6},{8,11},{9,8},{10,9... | collective-permute-start | bytes 786440 | tf_op jit(solution)/shard_map/ppermute | solution.py:271
  47.6 1.2 dynamic-slice_bitcast_fusion.8.own_gain
  48.9 0.7 pad_maximum_fusion.1.refs_0_
  49.6 0.7 bitcast_dynamic-update-slice_fusion.1
  50.3 14.9 %all-to-all-done.1 = bf16[32,32,128]{2,1,0:T(8,128)(2,1)S(1)} async-done(((bf16[32,32,128]{2,1,0:T(8,128)(2,1)}), bf16[32,32,128]{2,1,0:T(8,128)(2,1)S(1)}, u32[]{:S(2)}, u32[]{:S(2)}) %all-to-all-start.1) | async-done | bytes 262176 | tf_op jit(solution)/shard_map/all_to_all | solution.py:118
  65.2 1.9 %collective-permute-start = (bf16[32,8,128]{2,1,0:T(8,128)(2,1)S(1)}, bf16[32,8,128]{2,1,0:T(8,128)(2,1)S(1)}, u32[]{:S(2)}, u32[]{:S(2)}) collective-permute-start(bf16[32,8,128]{2,1,0:T(8,128)(2,1)S(1)} %slice.144), channel_id=1, source_target_pairs={{0,16},{16,0},{1,17},{17,1},{2,18},{18,2},{3,19},{19,3},{4,20},{20... | collective-permute-start | bytes 196616 | tf_op jit(solution)/shard_map/ppermute | solution.py:296
  67.2 0.6 fusion.7
  67.8 1.0 broadcast_in_dim.45
  68.8 7.6 %all-to-all-start.2 = ((bf16[16,208,128]{2,1,0:T(8,128)(2,1)}), bf16[16,208,128]{2,1,0:T(8,128)(2,1)S(1)}, u32[]{:S(2)}, u32[]{:S(2)}) async-start(bf16[16,208,128]{2,1,0:T(8,128)(2,1)} %bitcast.22), calls=%async_computation.2 | async-start | bytes 1703936 | tf_op jit(solution)/shard_map/all_to_all | solution.py:118
  76.6 0.4 fusion.83
  77.3 0.6 constant_dynamic-update-slice_fusion.1
  77.9 1.6 %bitcast_dynamic-update-slice_fusion = bf16[104,2048]{1,0:T(8,128)(2,1)} fusion(bf16[104,2048]{1,0:T(8,128)(2,1)} %constant_dynamic-update-slice_fusion.1, bf16[2048,32]{0,1:T(8,128)(2,1)} %param.37), kind=kLoop, calls=%fused_computation.58 | loop fusion | bytes 262144
  79.7 0.6 constant_dynamic-update-slice_fusion
  80.4 0.6 broadcast_dynamic-update-slice_fusion.local_weights
  81.0 9.8 %all-to-all-done.2.rows_pre = bf16[16,208,128]{2,1,0:T(8,128)(2,1)S(1)} async-done(((bf16[16,208,128]{2,1,0:T(8,128)(2,1)}), bf16[16,208,128]{2,1,0:T(8,128)(2,1)S(1)}, u32[]{:S(2)}, u32[]{:S(2)}) %all-to-all-start.2) | async-done | bytes 852000 | tf_op jit(solution)/shard_map/all_to_all | solution.py:118
  90.8 0.9 copy-done.2
  91.7 3.2 %hidden_units.1 = (bf16[208,128]{1,0:T(8,128)(2,1)}, bf16[48,128]{1,0:T(8,128)(2,1)}, f32[48,1]{1,0:T(8,128)}) custom-call(bf16[16,208,128]{2,1,0:T(8,128)(2,1)} %copy-done.2, f32[16,128]{1,0:T(8,128)} %bitcast.220, f32[48,128]{1,0:T(8,128)} %get-tuple-element.57.pre_first, f32[1,128]{1,0:T(1,128)} %dynamic-slice_bitcast_fusion.8.own_gain, ...), custom_call_target="tpu_custom_call" | custom-call | tf_op jit(solution)/shard_map/hidden_units/pallas_call | solution.py:168
  94.9 1.9 %broadcast_in_dim.48 = bf16[16,208,128]{2,1,0:T(8,128)(2,1)} broadcast(bf16[208,128]{1,0:T(8,128)(2,1)} %get-tuple-element.6), dimensions={1,2} | broadcast | bytes 905216 | tf_op jit(solution)/shard_map/broadcast_in_dim | solution.py:123
  96.8 4.9 %all-to-all-start.3 = ((bf16[16,208,128]{2,1,0:T(8,128)(2,1)}), bf16[16,208,128]{2,1,0:T(8,128)(2,1)S(1)}, u32[]{:S(2)}, u32[]{:S(2)}) async-start(bf16[16,208,128]{2,1,0:T(8,128)(2,1)} %broadcast_in_dim.48), calls=%async_computation.3 | async-start | bytes 1703936 | tf_op jit(solution)/shard_map/all_to_all | solution.py:118
  101.8 13.1 %all-to-all-done.3 = bf16[16,208,128]{2,1,0:T(8,128)(2,1)S(1)} async-done(((bf16[16,208,128]{2,1,0:T(8,128)(2,1)}), bf16[16,208,128]{2,1,0:T(8,128)(2,1)S(1)}, u32[]{:S(2)}, u32[]{:S(2)}) %all-to-all-start.3) | async-done | bytes 852000 | tf_op jit(solution)/shard_map/all_to_all | solution.py:118
  115.1 0.3 fusion.6
  115.4 1.1 fusion.5
  116.6 3.9 %all-to-all-start.4 = ((bf16[32,24,128]{2,1,0:T(8,128)(2,1)}), bf16[32,24,128]{2,1,0:T(8,128)(2,1)S(1)}, u32[]{:S(2)}, u32[]{:S(2)}) async-start(bf16[32,24,128]{2,1,0:T(8,128)(2,1)} %bitcast.67), calls=%async_computation.4 | async-start | bytes 393216 | tf_op jit(solution)/shard_map/all_to_all | solution.py:118
  120.8 0.2 convolution_bitcast_fusion.2
  121.0 19.4 %all-to-all-done.4 = bf16[32,24,128]{2,1,0:T(8,128)(2,1)S(1)} async-done(((bf16[32,24,128]{2,1,0:T(8,128)(2,1)}), bf16[32,24,128]{2,1,0:T(8,128)(2,1)S(1)}, u32[]{:S(2)}, u32[]{:S(2)}) %all-to-all-start.4) | async-done | bytes 196640 | tf_op jit(solution)/shard_map/all_to_all | solution.py:118
  140.4 0.3 fusion.8
  140.7 0.3 fusion.81
  141.1 0.6 broadcast_in_dim.49
  141.7 4.8 %all-to-all-start.5 = ((f32[16,2,48]{2,1,0:T(2,128)}), f32[16,2,48]{2,1,0:T(2,128)S(1)}, u32[]{:S(2)}, u32[]{:S(2)}) async-start(f32[16,2,48]{2,1,0:T(2,128)} %broadcast_in_dim.49), calls=%async_computation.5 | async-start | bytes 32768 | tf_op jit(solution)/shard_map/all_to_all | solution.py:118
  146.5 1.6 %multiply_add_fusion = f32[48,1,64,64]{3,2,1,0:T(8,128)} fusion(f32[48,1,64,64]{3,2,1,0:T(8,128)S(1)} %copy-done.1, f32[48,64]{1,0:T(8,128)S(1)} %split.18, f32[48,64]{1,0:T(8,128)S(1)} %maximum_multiply_fusion.1, f32[]{:T(128)S(6)} %sub.66), kind=kLoop, calls=%fused_computation.6 | loop fusion | flops 589824 | bytes 1597444 | tf_op jit(solution)/shard_map/add | solution.py:102
  148.1 4.7 %all-to-all-done.5 = f32[16,2,48]{2,1,0:T(2,128)S(1)} async-done(((f32[16,2,48]{2,1,0:T(2,128)}), f32[16,2,48]{2,1,0:T(2,128)S(1)}, u32[]{:S(2)}, u32[]{:S(2)}) %all-to-all-start.5) | async-done | bytes 6176 | tf_op jit(solution)/shard_map/all_to_all | solution.py:118
  152.9 0.7 multiply_convert_fusion
  (87 shorter events, 3.2 us)
Async XLA Ops:
  0.6 26.1 %copy-start = (bf16[1024,128]{1,0:T(8,128)(2,1)S(1)}, bf16[1024,128]{1,0:T(8,128)(2,1)}, u32[]{:S(2)}) copy-start(bf16[1024,128]{1,0:T(8,128)(2,1)} %param.29) | copy-start | bytes 786436
  0.6 5.3 %copy-start.1 = (f32[48,1,64,64]{3,2,1,0:T(8,128)S(1)}, f32[48,1,64,64]{3,2,1,0:T(8,128)}, u32[]{:S(2)}) copy-start(f32[48,1,64,64]{3,2,1,0:T(8,128)} %param.23) | copy-start | bytes 2359300
  4.0 13.1 %copy-start.3 = (bf16[4,2048,32]{1,2,0:T(8,128)(2,1)S(1)}, bf16[4,2048,32]{1,2,0:T(8,128)(2,1)}, u32[]{:S(2)}) copy-start(bf16[4,2048,32]{1,2,0:T(8,128)(2,1)} %param.34) | copy-start | bytes 1572868
  4.0 13.1 %copy-start.4 = (bf16[4,2048,32]{1,2,0:T(8,128)(2,1)S(1)}, bf16[4,2048,32]{1,2,0:T(8,128)(2,1)}, u32[]{:S(2)}) copy-start(bf16[4,2048,32]{1,2,0:T(8,128)(2,1)} %param.33) | copy-start | bytes 1572868
  7.4 18.5 %all-to-all-start = ((bf16[16,24,128]{2,1,0:T(8,128)(2,1)}), bf16[16,24,128]{2,1,0:T(8,128)(2,1)}, u32[]{:S(2)}, u32[]{:S(2)}) async-start(bf16[16,24,128]{2,1,0:T(8,128)(2,1)} %broadcast_in_dim.38), calls=%async_computation | async-start | bytes 196608 | tf_op jit(solution)/shard_map/all_to_all | solution.py:118
  17.2 7.8 %copy-start.13 = (s32[48,4]{0,1:T(4,128)S(1)}, s32[48,4]{0,1:T(4,128)}, u32[]{:S(2)}) copy-start(s32[48,4]{0,1:T(4,128)} %param.31) | copy-start | bytes 2308
  17.2 8.6 %copy-start.10 = (bf16[64,16]{0,1:T(8,128)(2,1)S(1)}, bf16[64,16]{0,1:T(8,128)(2,1)}, u32[]{:S(2)}) copy-start(bf16[64,16]{0,1:T(8,128)(2,1)} %param.40) | copy-start | bytes 6148
  17.2 8.6 %copy-start.11 = (bf16[64,16]{0,1:T(8,128)(2,1)S(1)}, bf16[64,16]{0,1:T(8,128)(2,1)}, u32[]{:S(2)}) copy-start(bf16[64,16]{0,1:T(8,128)(2,1)} %param.39) | copy-start | bytes 6148
  18.0 63.0 %collective-permute-start.1 = (bf16[2,32,2048]{2,1,0:T(8,128)(2,1)}, bf16[2,32,2048]{2,1,0:T(8,128)(2,1)}, u32[]{:S(2)}, u32[]{:S(2)}) collective-permute-start(bf16[2,32,2048]{2,1,0:T(8,128)(2,1)} %pad_maximum_fusion.2), channel_id=1, source_target_pairs={{0,1},{1,2},{2,3},{3,0},{4,5},{5,6},{6,7},{7,4},{8,9},{9,10},{10,1... | collective-permute-start | bytes 786440 | tf_op jit(solution)/shard_map/ppermute | solution.py:271
  22.1 58.9 %collective-permute-start.2 = (bf16[2,32,2048]{2,1,0:T(8,128)(2,1)}, bf16[2,32,2048]{2,1,0:T(8,128)(2,1)}, u32[]{:S(2)}, u32[]{:S(2)}) collective-permute-start(bf16[2,32,2048]{2,1,0:T(8,128)(2,1)} %pad_maximum_fusion.3), channel_id=1, source_target_pairs={{0,2},{1,3},{2,0},{3,1},{4,6},{5,7},{6,4},{7,5},{8,10},{9,11},{10,... | collective-permute-start | bytes 786440 | tf_op jit(solution)/shard_map/ppermute | solution.py:271
  28.4 21.2 %copy-start.8 = (bf16[2048,32]{0,1:T(8,128)(2,1)S(1)}, bf16[2048,32]{0,1:T(8,128)(2,1)}, u32[]{:S(2)}) copy-start(bf16[2048,32]{0,1:T(8,128)(2,1)} %param.36) | copy-start | bytes 393220
  29.5 35.8 %all-to-all-start.1 = ((bf16[32,32,128]{2,1,0:T(8,128)(2,1)}), bf16[32,32,128]{2,1,0:T(8,128)(2,1)S(1)}, u32[]{:S(2)}, u32[]{:S(2)}) async-start(bf16[32,32,128]{2,1,0:T(8,128)(2,1)} %pad_maximum_fusion), calls=%async_computation.1 | async-start | bytes 524288 | tf_op jit(solution)/shard_map/all_to_all | solution.py:118
  43.3 37.7 %collective-permute-start.3 = (bf16[2,32,2048]{2,1,0:T(8,128)(2,1)}, bf16[2,32,2048]{2,1,0:T(8,128)(2,1)S(1)}, u32[]{:S(2)}, u32[]{:S(2)}) collective-permute-start(bf16[2,32,2048]{2,1,0:T(8,128)(2,1)} %pad_maximum_fusion.4), channel_id=1, source_target_pairs={{0,3},{1,0},{2,1},{3,2},{4,7},{5,4},{6,5},{7,6},{8,11},{9,8},{10,9... | collective-permute-start | bytes 786440 | tf_op jit(solution)/shard_map/ppermute | solution.py:271
  65.2 11.2 %collective-permute-start = (bf16[32,8,128]{2,1,0:T(8,128)(2,1)S(1)}, bf16[32,8,128]{2,1,0:T(8,128)(2,1)S(1)}, u32[]{:S(2)}, u32[]{:S(2)}) collective-permute-start(bf16[32,8,128]{2,1,0:T(8,128)(2,1)S(1)} %slice.144), channel_id=1, source_target_pairs={{0,16},{16,0},{1,17},{17,1},{2,18},{18,2},{3,19},{19,3},{4,20},{20... | collective-permute-start | bytes 196616 | tf_op jit(solution)/shard_map/ppermute | solution.py:296
  68.8 22.0 %all-to-all-start.2 = ((bf16[16,208,128]{2,1,0:T(8,128)(2,1)}), bf16[16,208,128]{2,1,0:T(8,128)(2,1)S(1)}, u32[]{:S(2)}, u32[]{:S(2)}) async-start(bf16[16,208,128]{2,1,0:T(8,128)(2,1)} %bitcast.22), calls=%async_computation.2 | async-start | bytes 1703936 | tf_op jit(solution)/shard_map/all_to_all | solution.py:118
  76.5 3.9 %copy-start.12 = (bf16[2048]{0:T(1024)(128)(2,1)S(1)}, bf16[2048]{0:T(1024)(128)(2,1)}, u32[]{:S(2)}) copy-start(bf16[2048]{0:T(1024)(128)(2,1)} %param.42) | copy-start | bytes 12292
  81.0 9.8 %copy-start.6 = (bf16[2,32,2048]{2,1,0:T(8,128)(2,1)}, bf16[2,32,2048]{2,1,0:T(8,128)(2,1)S(1)}, u32[]{:S(2)}) copy-start(bf16[2,32,2048]{2,1,0:T(8,128)(2,1)S(1)} %collective-permute-done.3.refs_3_) | copy-start | bytes 786436
  90.8 0.9 copy-start.2
  94.9 6.8 %copy-start.5 = (bf16[4,512,128]{2,1,0:T(8,128)(2,1)S(1)}, bf16[4,512,128]{2,1,0:T(8,128)(2,1)}, u32[]{:S(2)}) copy-start(bf16[4,512,128]{2,1,0:T(8,128)(2,1)} %param.35) | copy-start | bytes 1572868
  96.8 18.2 %all-to-all-start.3 = ((bf16[16,208,128]{2,1,0:T(8,128)(2,1)}), bf16[16,208,128]{2,1,0:T(8,128)(2,1)S(1)}, u32[]{:S(2)}, u32[]{:S(2)}) async-start(bf16[16,208,128]{2,1,0:T(8,128)(2,1)} %broadcast_in_dim.48), calls=%async_computation.3 | async-start | bytes 1703936 | tf_op jit(solution)/shard_map/all_to_all | solution.py:118
  115.0 5.4 %copy-start.7 = (bf16[48,256]{1,0:T(8,128)(2,1)S(1)}, bf16[48,256]{1,0:T(8,128)(2,1)}, u32[]{:S(2)}) copy-start(bf16[48,256]{1,0:T(8,128)(2,1)} %project.1) | copy-start | bytes 73732
  115.0 5.6 %copy-start.9 = (f32[48,1]{1,0:T(8,128)S(1)}, f32[48,1]{1,0:T(8,128)}, u32[]{:S(2)}) copy-start(f32[48,1]{1,0:T(8,128)} %get-tuple-element.7) | copy-start | bytes 580
  115.1 5.7 %copy-start.15 = (bf16[512,128]{1,0:T(8,128)(2,1)S(1)}, bf16[512,128]{1,0:T(8,128)(2,1)}, u32[]{:S(2)}) copy-start(bf16[512,128]{1,0:T(8,128)(2,1)} %param.38) | copy-start | bytes 393220
  115.4 25.0 %copy-start.18 = (f32[48,4]{0,1:T(4,128)S(1)}, f32[48,4]{0,1:T(4,128)}, u32[]{:S(2)}) copy-start(f32[48,4]{0,1:T(4,128)} %param.32) | copy-start | bytes 2308
  115.4 25.3 %copy-start.16 = (bf16[256,128]{1,0:T(8,128)(2,1)S(1)}, bf16[256,128]{1,0:T(8,128)(2,1)}, u32[]{:S(2)}) copy-start(bf16[256,128]{1,0:T(8,128)(2,1)} %param.41) | copy-start | bytes 196612
  115.4 25.3 %copy-start.17 = (bf16[48,128]{1,0:T(8,128)(2,1)S(1)}, bf16[48,128]{1,0:T(8,128)(2,1)}, u32[]{:S(2)}) copy-start(bf16[48,128]{1,0:T(8,128)(2,1)} %get-tuple-element.5) | copy-start | bytes 36868
  116.6 23.8 %all-to-all-start.4 = ((bf16[32,24,128]{2,1,0:T(8,128)(2,1)}), bf16[32,24,128]{2,1,0:T(8,128)(2,1)S(1)}, u32[]{:S(2)}, u32[]{:S(2)}) async-start(bf16[32,24,128]{2,1,0:T(8,128)(2,1)} %bitcast.67), calls=%async_computation.4 | async-start | bytes 393216 | tf_op jit(solution)/shard_map/all_to_all | solution.py:118
  141.7 11.1 %all-to-all-start.5 = ((f32[16,2,48]{2,1,0:T(2,128)}), f32[16,2,48]{2,1,0:T(2,128)S(1)}, u32[]{:S(2)}, u32[]{:S(2)}) async-start(f32[16,2,48]{2,1,0:T(2,128)} %broadcast_in_dim.49), calls=%async_computation.5 | async-start | bytes 32768 | tf_op jit(solution)/shard_map/all_to_all | solution.py:118
  146.5 6.3 %copy-start.14 = (f32[128]{0:T(128)S(1)}, f32[128]{0:T(128)}, u32[]{:S(2)}) copy-start(f32[128]{0:T(128)} %param.43) | copy-start | bytes 1540

commit v3 on v2

--- a/solution.py
+++ b/solution.py
@@ -26,7 +26,7 @@
 def rotate(vector, positions):
     half_width = vector.shape[-1] // 2
     frequency = ROPE_BASE ** (-jnp.arange(half_width, dtype=jnp.float32) / half_width)
-    angles = positions.astype(jnp.float32)[:, None, None] * frequency[None, None, :]
+    angles = positions[:, None, None] * frequency[None, None, :]
     cosine = jnp.cos(angles)
     sine_part = jnp.sin(angles)
     first_half = vector[..., :half_width]
@@ -40,37 +40,122 @@
     )
 
 
-def project_kernel(tokens, *refs):
-    weights, out, total = refs[:-2], refs[-2], refs[-1]
-    step = pl.program_id(0)
-
-    @pl.when(step == 0)
-    def _():
-        total[...] = jnp.zeros_like(total)
-
-    stacked = jnp.concatenate([w[...] for w in weights], 0)
-    total[...] += f32_dot(tokens[...], stacked, ACROSS)
-
-    @pl.when(step == pl.num_programs(0) - 1)
-    def _():
-        out[...] = total[...].astype(out.dtype)
-
-
-def project_all(tokens, weights):
+def near(*arrays):
+    return [pltpu.with_memory_space_constraint(a, pltpu.VMEM) for a in arrays]
+
+
+def project_kernel(tokens, lengths, *refs):
+    count = (len(refs) - 4) // 2
+    weights, (out, positions) = refs[:count], refs[count : count + 2]
+    rows, held, arrived = refs[count + 2], refs[count + 3 : -1], refs[-1]
+    fetch = [
+        pltpu.make_async_copy(source, target, arrived.at[i])
+        for i, (source, target) in enumerate(zip((tokens, *weights), (rows, *held)))
+    ]
+    for f in fetch:
+        f.start()
+    positions[...] = lengths[...].astype(jnp.float32)
+    fetch[0].wait()
+    for i, w in enumerate(held):
+        fetch[i + 1].wait()
+        cols = w.shape[0]
+        part = f32_dot(rows[...], w[...], ACROSS).astype(jnp.bfloat16)
+        out[:, i * cols : (i + 1) * cols] = part.astype(jnp.float32)
+
+
+def project_all(tokens, lengths, weights):
     rows, width = tokens.shape
     cols = weights[0].shape[1]
-    steps = 4
-    span = width // steps
+    count = len(weights)
+    anywhere = pl.BlockSpec(memory_space=pl.ANY)
+    whole = pl.BlockSpec(memory_space=pltpu.VMEM)
     return pl.pallas_call(
         project_kernel,
-        grid=(steps,),
-        in_specs=[pl.BlockSpec((rows, span), lambda i: (0, i))]
-        + [pl.BlockSpec((cols, span), lambda i: (0, i)) for _ in weights],
-        out_specs=pl.BlockSpec((rows, cols * len(weights)), lambda i: (0, 0)),
-        out_shape=jax.ShapeDtypeStruct((rows, cols * len(weights)), jnp.bfloat16),
-        scratch_shapes=[pltpu.VMEM((rows, cols * len(weights)), jnp.float32)],
+        in_specs=[anywhere, whole] + [anywhere] * count,
+        out_specs=[whole, whole],
+        out_shape=[
+            pltpu.VMEM((rows, cols * count), jnp.float32),
+            pltpu.VMEM(lengths.shape, jnp.float32),
+        ],
+        scratch_shapes=[pltpu.VMEM((rows, width), tokens.dtype)]
+        + [pltpu.VMEM((cols, width), weights[0].dtype)] * count
+        + [pltpu.SemaphoreType.DMA((count + 1,))],
         name="project",
-    )(tokens, *[w.T for w in weights])
+    )(tokens, lengths, *[w.T for w in weights])
+
+
+def dispatch_kernel(folded_all, out_weight, own_cols, table, rider, outgoing, exact, short, lhs, rhs):
+    parts, half, lanes = folded_all.shape
+    width = lanes // 2
+    lane = lax.broadcasted_iota(jnp.int32, (half, lanes), 1)
+    for t in range(parts):
+        block = folded_all[t].astype(jnp.float32)
+        at = slice(t * lanes, (t + 1) * lanes)
+        lhs[0, :, at] = jnp.where(lane < width, block, 0.0).astype(lhs.dtype)
+        lhs[1, :, at] = jnp.where(lane < width, 0.0, block).astype(lhs.dtype)
+        for i in range(2):
+            rhs[t * lanes + i * width : t * lanes + (i + 1) * width] = out_weight[
+                t * width : (t + 1) * width
+            ]
+    flat = ((1,), (0,))
+    mixing = jnp.concatenate([f32_dot(lhs[i], rhs[...], flat) for i in range(2)], 0)
+    pre_first = RESIDUAL_SCALE * own_cols[...].astype(jnp.float32) + mixing
+    exact[...] = pre_first
+    pre_short = pre_first.astype(short.dtype)
+    short[...] = pre_short
+    peers, _, cols = outgoing.shape
+    rows = f32_dot(table[...], pre_short, flat).reshape(peers, PITCH, cols)
+    riders = rider[...].astype(jnp.float32)
+    riders = jnp.broadcast_to(riders[None], (peers // riders.shape[0], *riders.shape))
+    riders = riders.reshape(peers, RIDER, cols)
+    outgoing[...] = jnp.concatenate([rows, riders], 1).astype(outgoing.dtype)
+
+
+def dispatch_rows(folded_all, out_weight, own_cols, table, rider, peers):
+    parts, half, lanes = folded_all.shape
+    rows, cols = own_cols.shape
+    bf16 = jnp.bfloat16
+    whole = pl.BlockSpec(memory_space=pltpu.VMEM)
+    return pl.pallas_call(
+        dispatch_kernel,
+        in_specs=[whole] * 5,
+        out_specs=[whole] * 3,
+        out_shape=[
+            jax.ShapeDtypeStruct((peers, PITCH + RIDER, cols), bf16),
+            pltpu.VMEM((rows, cols), jnp.float32),
+            pltpu.VMEM((rows, cols), bf16),
+        ],
+        scratch_shapes=[
+            pltpu.VMEM((2, half, parts * lanes), bf16),
+            pltpu.VMEM((parts * lanes, cols), bf16),
+        ],
+        name="dispatch_rows",
+    )(*near(folded_all, out_weight, own_cols, table, rider))
+
+
+def return_kernel(hidden_all, down, goes, sent_back):
+    parts, experts = down.shape[1], down.shape[0]
+    slots = goes.shape[1] // experts
+    flat = ((1,), (0,))
+    results = []
+    for j in range(experts):
+        rows = jnp.concatenate([hidden_all[q * experts + j, :slots] for q in range(parts)], 1)
+        mats = jnp.concatenate([down[j, q] for q in range(parts)], 0)
+        results.append(f32_dot(rows, mats, flat).astype(sent_back.dtype))
+    back = f32_dot(goes[...], jnp.concatenate(results, 0), flat)
+    sent_back[...] = back.reshape(sent_back.shape).astype(sent_back.dtype)
+
+
+def return_rows(hidden_all, down, goes, peers):
+    cols = down.shape[-1]
+    whole = pl.BlockSpec(memory_space=pltpu.VMEM)
+    return pl.pallas_call(
+        return_kernel,
+        in_specs=[whole] * 3,
+        out_specs=whole,
+        out_shape=jax.ShapeDtypeStruct((peers, goes.shape[0] // peers, cols), jnp.bfloat16),
+        name="return_rows",
+    )(*near(hidden_all, down, goes))
 
 
 def retain(
@@ -87,11 +172,13 @@
     head_count = retention_state.shape[1]
     head_width = retention_state.shape[2]
 
-    projected = project_all(tokens, (query_weight, key_weight, value_weight, gate_weight))
-    queries, keys, values, gate_act = jnp.split(projected.astype(jnp.float32), 4, 1)
+    projected, positions = project_all(
+        tokens, lengths, (query_weight, key_weight, value_weight, gate_weight)
+    )
+    queries, keys, values, gate_act = jnp.split(projected, 4, 1)
     by_head = (row_count, head_count, head_width)
-    queries = rotate(queries.reshape(by_head), lengths)
-    key_rows = rotate(keys.reshape(by_head), lengths) * head_width ** (-0.5)
+    queries = rotate(queries.reshape(by_head), positions)
+    key_rows = rotate(keys.reshape(by_head), positions) * head_width ** (-0.5)
     values = values.reshape(by_head)
     head_index = (first_head + jnp.arange(head_count)).astype(jnp.float32)
     decays = 1.0 - 2.0 ** (-5.0 - 7.0 * head_index / (HEADS - 1))
@@ -128,7 +215,7 @@
 
 
 def hidden_kernel(rows_pre, gains, pre_first, own_gain, local_weights, *refs):
-    pieces, (hidden, normed_cols, switch, normed) = refs[:-4], refs[-4:]
+    pieces, (message, normed_cols, switch, normed, hidden, sent) = refs[:-6], refs[-6:]
     parts, row_count, cols = rows_pre.shape
     own_rows = pre_first.shape[0]
     slots = row_count - own_rows
@@ -155,9 +242,17 @@
     local = f32_dot(normed[slots:], local_weights[...], ACROSS)
     cut = (local.shape[1] - RIDER) // 2
     mine = jax.nn.silu(local[:, :cut]) * local[:, cut : 2 * cut]
-    hidden[slots:] = jnp.zeros((own_rows, units), hidden.dtype)
-    hidden[slots:, :cut] = mine.astype(hidden.dtype)
+    mine = jnp.concatenate([mine, jnp.zeros((own_rows, units // 2 - cut), jnp.float32)], 1)
+    half = own_rows // 2
+    hidden[slots:] = jnp.concatenate([mine[:half], mine[half:]], 1).astype(hidden.dtype)
+    copies = [
+        pltpu.make_async_copy(hidden, message.at[t], sent.at[t]) for t in range(message.shape[0])
+    ]
+    for c in copies:
+        c.start()
     switch[...] = jax.nn.sigmoid(local[:, 2 * cut : 2 * cut + 1])
+    for c in copies:
+        c.wait()
 
 
 def hidden_units(rows_pre, gains, pre_first, own_gain, local_weights, pieces):
@@ -168,15 +263,19 @@
     return pl.pallas_call(
         hidden_kernel,
         in_specs=[whole] * (5 + len(pieces)),
-        out_specs=[whole] * 3,
+        out_specs=[pl.BlockSpec(memory_space=pl.ANY), whole, whole],
         out_shape=[
-            jax.ShapeDtypeStruct((row_count, units), jnp.bfloat16),
-            jax.ShapeDtypeStruct((own_rows, cols), jnp.bfloat16),
-            jax.ShapeDtypeStruct((own_rows, 1), jnp.float32),
-        ],
-        scratch_shapes=[pltpu.VMEM((row_count, parts * cols), jnp.bfloat16)],
+            jax.ShapeDtypeStruct((parts, row_count - own_rows // 2, units), jnp.bfloat16),
+            pltpu.VMEM((own_rows, cols), jnp.bfloat16),
+            pltpu.VMEM((own_rows, 1), jnp.float32),
+        ],
+        scratch_shapes=[
+            pltpu.VMEM((row_count, parts * cols), jnp.bfloat16),
+            pltpu.VMEM((row_count - own_rows // 2, units), jnp.bfloat16),
+            pltpu.SemaphoreType.DMA((parts,)),
+        ],
         name="hidden_units",
-    )(rows_pre, gains, pre_first, own_gain, local_weights, *pieces)
+    )(*near(rows_pre, gains, pre_first, own_gain, local_weights, *pieces))
 
 
 def on_device(
@@ -229,21 +328,9 @@
         gate_weight,
         tp_rank * head_count,
     )
-    head_width = mixed_heads.shape[1]
     half = seq_rows // 2
     folded = jnp.concatenate([mixed_heads[:half], mixed_heads[half:]], 1)
     folded_all = to_all(folded, TP)
-    left = jnp.arange(2 * head_width, dtype=jnp.int32)[None, None, :] < head_width
-    none = jnp.zeros_like(folded_all)
-    mixed_all = in_order(
-        jnp.concatenate(
-            [jnp.where(left, folded_all, none), jnp.where(left, none, folded_all)], 1
-        ),
-        1,
-    )
-    head_weight = out_weight.reshape(tp_count, 1, head_width, col_count)
-    head_weight = jnp.broadcast_to(head_weight, (tp_count, 2, head_width, col_count))
-    head_weight = head_weight.reshape(tp_count * 2 * head_width, col_count)
 
     same = routing.reshape(-1)[:, None] == routing.reshape(-1)[None, :]
     row_of = jnp.arange(seq_rows * top_count, dtype=jnp.int32) // top_count
@@ -277,21 +364,21 @@
         ]
     )
 
-    mixing = jnp.dot(mixed_all, head_weight, preferred_element_type=jnp.float32)
-    own_cols = lax.dynamic_slice_in_dim(tokens, col_start, col_count, 1).astype(jnp.float32)
-    pre_first = RESIDUAL_SCALE * own_cols + mixing
-    pre_short = pre_first.astype(bf16)
+    own_cols = lax.dynamic_slice_in_dim(tokens, col_start, col_count, 1)
 
     side_cols = side_gate.shape[1]
     side_rows = side_gate.shape[0]
     core_count = lax.axis_size("core")
     side_piece = jnp.concatenate([side_gate.T, side_up.T], 1)
-    rider = jnp.broadcast_to(
-        side_piece.reshape(1, core_count, RIDER, 2 * side_rows),
-        (ep_count // core_count, core_count, RIDER, 2 * side_rows),
-    ).reshape(ep_count, RIDER, 2 * side_rows)
-    outgoing = jnp.dot(table, pre_short, preferred_element_type=jnp.float32).astype(bf16)
-    arrived = swap(jnp.concatenate([outgoing.reshape(ep_count, PITCH, col_count), rider], 1), EP)
+    outgoing, pre_first, pre_short = dispatch_rows(
+        folded_all,
+        out_weight,
+        own_cols,
+        table,
+        side_piece.reshape(core_count, RIDER, 2 * side_rows),
+        ep_count,
+    )
+    arrived = swap(outgoing, EP)
     side_own = arrived[:, PITCH:]
     side_other = lax.ppermute(side_own, "core", [(0, 1), (1, 0)])
     first_core = lax.axis_index("core") == 0
@@ -326,7 +413,6 @@
     own_gain = lax.dynamic_slice_in_dim(first_gain, col_start, col_count, 0)
     units = class_count * hidden_cols
     shared_cols = shared_gate.shape[1]
-    spare = units - shared_cols - side_cols
     local_weights = jnp.concatenate(
         [
             shared_gate.T,
@@ -341,28 +427,34 @@
         rows_pre, first_gain.reshape(tp_count, col_count), pre_first, own_gain[None], local_weights, pieces
     )
 
-    hidden_all = to_all(hidden, TP)
-    expert_hidden = hidden_all[:, :slots].reshape(part_count, class_count, slots, units)
-    local_all = in_order(hidden_all[:, slots:], 1)
-    result = jnp.einsum("qjrf,jqfd->jrd", expert_hidden, down, preferred_element_type=jnp.float32)
+    hidden_all = swap(hidden, TP)
     goes_at = source * PITCH + spot
-    sent_back = jnp.dot(
-        (wire_ids[:, None] == goes_at[None, :]).astype(bf16),
-        result.astype(bf16).reshape(local_experts * slots, col_count),
-        preferred_element_type=jnp.float32,
-    ).astype(bf16)
-    returned = swap(sent_back.reshape(ep_count, PITCH, col_count), EP)
-
-    shared_part = jnp.pad(
-        shared_down.reshape(tp_count, shared_cols, col_count),
-        ((0, 0), (0, units - shared_cols), (0, 0)),
-    ).reshape(tp_count * units, col_count)
-    side_part = jnp.pad(
-        side_down.reshape(tp_count, side_cols, col_count),
-        ((0, 0), (shared_cols, spare), (0, 0)),
-    ).reshape(tp_count * units, col_count)
-    shared_out = jnp.dot(local_all, shared_part, preferred_element_type=jnp.float32)
-    side_out = jnp.dot(local_all, side_part, preferred_element_type=jnp.float32)
+    goes = (wire_ids[:, None] == goes_at[None, :]).astype(bf16)
+    down = down.reshape(local_experts, part_count, units, col_count)
+    returned = swap(return_rows(hidden_all, down, goes, ep_count), EP)
+
+    local_all = hidden_all[:, slots:]
+    left = jnp.arange(units, dtype=jnp.int32)[None, None, :] < units // 2
+    none = jnp.zeros_like(local_all)
+    local_all = in_order(
+        jnp.concatenate([jnp.where(left, local_all, none), jnp.where(left, none, local_all)], 1), 1
+    )
+
+    def spread(weight, first):
+        count = weight.shape[0] // tp_count
+        weight = jnp.pad(
+            weight.reshape(tp_count, 1, count, col_count),
+            ((0, 0), (0, 0), (first, units // 2 - first - count), (0, 0)),
+        )
+        weight = jnp.broadcast_to(weight, (tp_count, 2, units // 2, col_count))
+        return weight.reshape(tp_count * units, col_count)
+
+    shared_out = jnp.dot(
+        local_all, spread(shared_down, 0), preferred_element_type=jnp.float32
+    )
+    side_out = jnp.dot(
+        local_all, spread(side_down, shared_cols), preferred_element_type=jnp.float32
+    )
     local_sum = (
         RESIDUAL_SCALE * normed_cols.astype(jnp.float32) + shared_out + switch * side_out
     )

time: 154 us -> 150 us (0.974)
  waiting for transfers between devices: 62 us -> 68.8 us
  local copies, waits for them, and re-layouts: 12.5 us -> 6.73 us
  matrix products: 5.05 us -> 1.61 us
  other arithmetic: 9.81 us -> 8.24 us
    all_to_all x6, waiting for transfers between devices: 62 us -> 68.8 us  [swap(): return lax.all_to_all(parts, axis, 0, 0, tiled=True)]
    dot_general x6 -> x2, matrix products: 3.86 us -> 0.42 us  [the longest x1 0.21 us: on_device(): jnp.dot(local_all, spread(shared_down, 0), preferred_element_type=jnp.flo...]
    unnamed x43 -> x71, local copies, waits for them, and re-layouts: 4.57 us -> 1.19 us
    pallas_call x1 -> x3, Pallas kernels: 3.34 us -> 5.6 us  [the longest x1 3.06 us: project_all(): pl.pallas_call(project_kernel, in_specs=[anywhere, whole] + [anywhere] *...]
    broadcast_in_dim x3 -> x2, local copies, waits for them, and re-layouts: 3.14 us -> 1.27 us  [to_all(): return swap(jnp.broadcast_to(shard[None], (length, *shard.shape)), axis)]
    all_to_all x6, starting transfers between devices: 44 us -> 42.3 us  [swap(): return lax.all_to_all(parts, axis, 0, 0, tiled=True)]
  transfers between devices with their start and end apart: 10 -> 10, of which waited for: 5 -> 5; matrix products, arithmetic and copies ran while one was open for 12% -> 9% of each run, Pallas kernels for 0% -> 1%
where the time goes in v3:
time: 150 us; the launch traced here: 149 us
  waiting for transfers between devices  68.8 us (46%)
  starting transfers between devices  54.9 us (37%)
  other arithmetic  8.24 us (5%)
  Pallas kernels  7.64 us (5%)
  local copies, waits for them, and re-layouts  6.73 us (4%)
  matrix products  1.61 us (1%)
  between operations  1.51 us (1%)
    all_to_all x6, waiting for transfers between devices, swap(): return lax.all_to_all(parts, axis, 0, 0, tiled=True)  68.8 us
    all_to_all x6, starting transfers between devices, swap(): return lax.all_to_all(parts, axis, 0, 0, tiled=True)  42.3 us
    ppermute x3, starting transfers between devices, on_device(): lax.ppermute(piece_for((lane + d) % class_count), 'tp_1', steps)  10.7 us
    pallas_call x1, Pallas kernels, project_all(): pl.pallas_call(project_kernel, in_specs=[anywhere, whole] + [anywhere] *...  3.06 us
  transfers between devices with their start and end apart: 10, of which 5 were waited for; matrix products, arithmetic and copies ran while one was open for 9% of the time, Pallas kernels for 1%

profile of v3, /device:TPU:2, one launch (start us, length us, event | category | flops | bytes accessed | tf_op | source)
XLA Modules:
  0.0 149.4 jit_solution(2144850357057055117)
XLA Ops:
  0.7 3.1 %project.1 = (f32[48,256]{1,0:T(8,128)S(1)}, f32[48]{0:T(128)S(1)}) custom-call(bf16[48,2048]{1,0:T(8,128)(2,1)} %tokens.1, s32[48]{0:T(128)} %lengths.1, bf16[64,2048]{1,0:T(8,128)(2,1)} %bitcast.190, bf16[64,2048]{1,0:T(8,128)(2,1)} %bitcast.191, bf16[64,2048]{1,0:T(8,128)(2,1)} %bitcast.192, bf16[64,2048]{1,0:T(8,128)(2,1)} %bitcast.193), custom_call_target="tpu_custom_call" | custom-call | tf_op jit(solution)/shard_map/project/pallas_call | solution.py:72
  3.8 0.2 fusion.28
  4.0 0.2 fusion.37
  4.2 0.3 fusion.69
  4.6 0.2 fusion.67
  5.0 0.7 broadcast_in_dim.32
  5.6 9.2 %all-to-all-start = ((bf16[16,24,128]{2,1,0:T(8,128)(2,1)}), bf16[16,24,128]{2,1,0:T(8,128)(2,1)S(1)}, u32[]{:S(2)}, u32[]{:S(2)}) async-start(bf16[16,24,128]{2,1,0:T(8,128)(2,1)} %broadcast_in_dim.32), calls=%async_computation | async-start | bytes 196608 | tf_op jit(solution)/shard_map/all_to_all | solution.py:205
  15.0 0.7 pad_maximum_fusion.2
  15.7 3.4 %collective-permute-start.1 = (bf16[2,32,2048]{2,1,0:T(8,128)(2,1)}, bf16[2,32,2048]{2,1,0:T(8,128)(2,1)S(1)}, u32[]{:S(2)}, u32[]{:S(2)}) collective-permute-start(bf16[2,32,2048]{2,1,0:T(8,128)(2,1)} %pad_maximum_fusion.2), channel_id=1, source_target_pairs={{0,1},{1,2},{2,3},{3,0},{4,5},{5,6},{6,7},{7,4},{8,9},{9,10},{10,1... | collective-permute-start | bytes 786440 | tf_op jit(solution)/shard_map/ppermute | solution.py:358
  19.1 0.7 pad_maximum_fusion.3
  19.8 2.9 %collective-permute-start.2 = (bf16[2,32,2048]{2,1,0:T(8,128)(2,1)}, bf16[2,32,2048]{2,1,0:T(8,128)(2,1)S(1)}, u32[]{:S(2)}, u32[]{:S(2)}) collective-permute-start(bf16[2,32,2048]{2,1,0:T(8,128)(2,1)} %pad_maximum_fusion.3), channel_id=1, source_target_pairs={{0,2},{1,3},{2,0},{3,1},{4,6},{5,7},{6,4},{7,5},{8,10},{9,11},{10,... | collective-permute-start | bytes 786440 | tf_op jit(solution)/shard_map/ppermute | solution.py:358
  22.7 0.7 pad_maximum_fusion.4
  23.5 4.4 %collective-permute-start.3 = (bf16[2,32,2048]{2,1,0:T(8,128)(2,1)}, bf16[2,32,2048]{2,1,0:T(8,128)(2,1)S(1)}, u32[]{:S(2)}, u32[]{:S(2)}) collective-permute-start(bf16[2,32,2048]{2,1,0:T(8,128)(2,1)} %pad_maximum_fusion.4), channel_id=1, source_target_pairs={{0,3},{1,0},{2,1},{3,2},{4,7},{5,4},{6,5},{7,6},{8,11},{9,8},{10,9... | collective-permute-start | bytes 786440 | tf_op jit(solution)/shard_map/ppermute | solution.py:358
  27.9 0.7 constant_dynamic-slice_fusion.own_cols
  28.8 0.2 convert_reduce_fusion
  29.2 0.2 slice_reduce_fusion.3
  29.5 0.7 maximum_multiply_fusion.1
  30.2 0.2 fusion.12.table
  30.5 1.2 dispatch_rows.1
  31.7 13.8 %all-to-all-start.1 = ((bf16[32,32,128]{2,1,0:T(8,128)(2,1)}), bf16[32,32,128]{2,1,0:T(8,128)(2,1)S(1)}, u32[]{:S(2)}, u32[]{:S(2)}) async-start(bf16[32,32,128]{2,1,0:T(8,128)(2,1)} %get-tuple-element.12), calls=%async_computation.1 | async-start | bytes 524288 | tf_op jit(solution)/shard_map/all_to_all | solution.py:205
  45.6 0.9 slice_bitcast_fusion.15
  46.5 21.7 %all-to-all-done.1 = bf16[32,32,128]{2,1,0:T(8,128)(2,1)S(1)} async-done(((bf16[32,32,128]{2,1,0:T(8,128)(2,1)}), bf16[32,32,128]{2,1,0:T(8,128)(2,1)S(1)}, u32[]{:S(2)}, u32[]{:S(2)}) %all-to-all-start.1) | async-done | bytes 262176 | tf_op jit(solution)/shard_map/all_to_all | solution.py:205
  68.2 1.9 %collective-permute-start = (bf16[32,8,128]{2,1,0:T(8,128)(2,1)S(1)}, bf16[32,8,128]{2,1,0:T(8,128)(2,1)}, u32[]{:S(2)}, u32[]{:S(2)}) collective-permute-start(bf16[32,8,128]{2,1,0:T(8,128)(2,1)S(1)} %slice.140), channel_id=1, source_target_pairs={{0,16},{16,0},{1,17},{17,1},{2,18},{18,2},{3,19},{19,3},{4,20},{20... | collective-permute-start | bytes 196616 | tf_op jit(solution)/shard_map/ppermute | solution.py:383
  70.1 0.6 fusion.5
  70.8 1.0 broadcast_in_dim.34
  71.8 5.7 %all-to-all-start.2 = ((bf16[16,208,128]{2,1,0:T(8,128)(2,1)}), bf16[16,208,128]{2,1,0:T(8,128)(2,1)S(1)}, u32[]{:S(2)}, u32[]{:S(2)}) async-start(bf16[16,208,128]{2,1,0:T(8,128)(2,1)} %bitcast.17), calls=%async_computation.2 | async-start | bytes 1703936 | tf_op jit(solution)/shard_map/all_to_all | solution.py:205
  77.5 0.9 broadcast_select_fusion.3
  78.4 0.1 reshape.464
  78.7 0.2 squeeze.63
  78.9 0.9 bitcast_dynamic-update-slice_fusion
  79.8 0.2 squeeze.64
  80.1 11.8 %all-to-all-done.2.rows_pre = bf16[16,208,128]{2,1,0:T(8,128)(2,1)S(1)} async-done(((bf16[16,208,128]{2,1,0:T(8,128)(2,1)}), bf16[16,208,128]{2,1,0:T(8,128)(2,1)S(1)}, u32[]{:S(2)}, u32[]{:S(2)}) %all-to-all-start.2) | async-done | bytes 852000 | tf_op jit(solution)/shard_map/all_to_all | solution.py:205
  92.0 2.0 %hidden_units.1 = (bf16[16,184,128]{2,1,0:T(8,128)(2,1)}, bf16[48,128]{1,0:T(8,128)(2,1)S(1)}, f32[48,1]{1,0:T(8,128)S(1)}) custom-call(bf16[16,208,128]{2,1,0:T(8,128)(2,1)S(1)} %all-to-all-done.2.rows_pre, f32[16,128]{1,0:T(8,128)S(1)} %bitcast.183, f32[48,128]{1,0:T(8,128)S(1)} %get-tuple-element.14.pre_first, ...), custom_call_target="tpu_custom_call" | custom-call | tf_op jit(solution)/shard_map/hidden_units/pallas_call | solution.py:263
  94.1 5.1 %all-to-all-start.3 = ((bf16[16,184,128]{2,1,0:T(8,128)(2,1)}), bf16[16,184,128]{2,1,0:T(8,128)(2,1)S(1)}, u32[]{:S(2)}, u32[]{:S(2)}) async-start(bf16[16,184,128]{2,1,0:T(8,128)(2,1)} %get-tuple-element.16), calls=%async_computation.3 | async-start | bytes 1507328 | tf_op jit(solution)/shard_map/all_to_all | solution.py:205
  99.5 0.3 fusion.1.goes
  99.8 11.6 %all-to-all-done.3.hidden_all = bf16[16,184,128]{2,1,0:T(8,128)(2,1)S(1)} async-done(((bf16[16,184,128]{2,1,0:T(8,128)(2,1)}), bf16[16,184,128]{2,1,0:T(8,128)(2,1)S(1)}, u32[]{:S(2)}, u32[]{:S(2)}) %all-to-all-start.3) | async-done | bytes 753696 | tf_op jit(solution)/shard_map/all_to_all | solution.py:205
  111.4 1.3 return_rows.1
  112.7 3.9 %all-to-all-start.4 = ((bf16[32,24,128]{2,1,0:T(8,128)(2,1)}), bf16[32,24,128]{2,1,0:T(8,128)(2,1)S(1)}, u32[]{:S(2)}, u32[]{:S(2)}) async-start(bf16[32,24,128]{2,1,0:T(8,128)(2,1)} %return_rows.1), calls=%async_computation.4 | async-start | bytes 393216 | tf_op jit(solution)/shard_map/all_to_all | solution.py:205
  117.0 0.2 fusion.14
  117.3 0.2 fusion.16
  117.5 19.0 %all-to-all-done.4 = bf16[32,24,128]{2,1,0:T(8,128)(2,1)S(1)} async-done(((bf16[32,24,128]{2,1,0:T(8,128)(2,1)}), bf16[32,24,128]{2,1,0:T(8,128)(2,1)S(1)}, u32[]{:S(2)}, u32[]{:S(2)}) %all-to-all-start.4) | async-done | bytes 196640 | tf_op jit(solution)/shard_map/all_to_all | solution.py:205
  136.6 0.3 fusion.6
  136.9 0.2 fusion.64
  137.1 0.6 broadcast_in_dim.46
  137.7 4.7 %all-to-all-start.5 = ((f32[16,2,48]{2,1,0:T(2,128)}), f32[16,2,48]{2,1,0:T(2,128)S(1)}, u32[]{:S(2)}, u32[]{:S(2)}) async-start(f32[16,2,48]{2,1,0:T(2,128)} %broadcast_in_dim.46), calls=%async_computation.5 | async-start | bytes 32768 | tf_op jit(solution)/shard_map/all_to_all | solution.py:205
  142.4 1.6 %multiply_add_fusion = f32[48,1,64,64]{3,2,1,0:T(8,128)} fusion(f32[48,1,64,64]{3,2,1,0:T(8,128)S(1)} %copy-done.3, f32[48,64]{1,0:T(8,128)S(1)} %get-tuple-element.57, f32[48,64]{1,0:T(8,128)S(1)} %copy-done.25, f32[]{:T(128)S(6)} %sub.66), kind=kLoop, calls=%fused_computation.6 | loop fusion | flops 589824 | bytes 1597444 | tf_op jit(solution)/shard_map/add | solution.py:189
  144.0 4.6 %all-to-all-done.5 = f32[16,2,48]{2,1,0:T(2,128)S(1)} async-done(((f32[16,2,48]{2,1,0:T(2,128)}), f32[16,2,48]{2,1,0:T(2,128)S(1)}, u32[]{:S(2)}, u32[]{:S(2)}) %all-to-all-start.5) | async-done | bytes 6176 | tf_op jit(solution)/shard_map/all_to_all | solution.py:205
  148.7 0.7 multiply_convert_fusion
  (113 shorter events, 2.0 us)
Async XLA Ops:
  0.6 3.6 %copy-start.2 = (f32[48,1,64,64]{3,2,1,0:T(8,128)S(1)}, f32[48,1,64,64]{3,2,1,0:T(8,128)}, u32[]{:S(2)}) copy-start(f32[48,1,64,64]{3,2,1,0:T(8,128)} %param.23) | copy-start | bytes 2359300
  3.7 11.1 %copy-start.4 = (bf16[4,2048,32]{1,2,0:T(8,128)(2,1)S(1)}, bf16[4,2048,32]{1,2,0:T(8,128)(2,1)}, u32[]{:S(2)}) copy-start(bf16[4,2048,32]{1,2,0:T(8,128)(2,1)} %param.34) | copy-start | bytes 1572868
  3.7 11.1 %copy-start.5 = (bf16[4,2048,32]{1,2,0:T(8,128)(2,1)S(1)}, bf16[4,2048,32]{1,2,0:T(8,128)(2,1)}, u32[]{:S(2)}) copy-start(bf16[4,2048,32]{1,2,0:T(8,128)(2,1)} %param.33) | copy-start | bytes 1572868
  5.6 24.9 %all-to-all-start = ((bf16[16,24,128]{2,1,0:T(8,128)(2,1)}), bf16[16,24,128]{2,1,0:T(8,128)(2,1)S(1)}, u32[]{:S(2)}, u32[]{:S(2)}) async-start(bf16[16,24,128]{2,1,0:T(8,128)(2,1)} %broadcast_in_dim.32), calls=%async_computation | async-start | bytes 196608 | tf_op jit(solution)/shard_map/all_to_all | solution.py:205
  14.8 13.8 %copy-start.30 = (s32[48,4]{0,1:T(4,128)S(1)}, s32[48,4]{0,1:T(4,128)}, u32[]{:S(2)}) copy-start(s32[48,4]{0,1:T(4,128)} %param.31) | copy-start | bytes 2308
  14.8 14.6 %copy-start.26 = (bf16[256,128]{1,0:T(8,128)(2,1)S(1)}, bf16[256,128]{1,0:T(8,128)(2,1)}, u32[]{:S(2)}) copy-start(bf16[256,128]{1,0:T(8,128)(2,1)} %param.41) | copy-start | bytes 196612
  14.9 14.6 %copy-start.7 = (bf16[512,128]{1,0:T(8,128)(2,1)S(1)}, bf16[512,128]{1,0:T(8,128)(2,1)}, u32[]{:S(2)}) copy-start(bf16[512,128]{1,0:T(8,128)(2,1)} %param.38) | copy-start | bytes 393220
  14.9 15.5 %copy-start.27 = (bf16[64,16]{0,1:T(8,128)(2,1)S(1)}, bf16[64,16]{0,1:T(8,128)(2,1)}, u32[]{:S(2)}) copy-start(bf16[64,16]{0,1:T(8,128)(2,1)} %param.40) | copy-start | bytes 6148
  14.9 15.5 %copy-start.28 = (bf16[64,16]{0,1:T(8,128)(2,1)S(1)}, bf16[64,16]{0,1:T(8,128)(2,1)}, u32[]{:S(2)}) copy-start(bf16[64,16]{0,1:T(8,128)(2,1)} %param.39) | copy-start | bytes 6148
  15.0 15.5 %copy-start = (bf16[1024,128]{1,0:T(8,128)(2,1)S(1)}, bf16[1024,128]{1,0:T(8,128)(2,1)}, u32[]{:S(2)}) copy-start(bf16[1024,128]{1,0:T(8,128)(2,1)} %out_weight.1) | copy-start | bytes 786436
  15.7 64.3 %collective-permute-start.1 = (bf16[2,32,2048]{2,1,0:T(8,128)(2,1)}, bf16[2,32,2048]{2,1,0:T(8,128)(2,1)S(1)}, u32[]{:S(2)}, u32[]{:S(2)}) collective-permute-start(bf16[2,32,2048]{2,1,0:T(8,128)(2,1)} %pad_maximum_fusion.2), channel_id=1, source_target_pairs={{0,1},{1,2},{2,3},{3,0},{4,5},{5,6},{6,7},{7,4},{8,9},{9,10},{10,1... | collective-permute-start | bytes 786440 | tf_op jit(solution)/shard_map/ppermute | solution.py:358
  19.8 25.7 %copy-start.1 = (f32[2048]{0:T(1024)S(1)}, f32[2048]{0:T(1024)}, u32[]{:S(2)}) copy-start(f32[2048]{0:T(1024)} %param.30) | copy-start | bytes 24580
  19.8 60.2 %collective-permute-start.2 = (bf16[2,32,2048]{2,1,0:T(8,128)(2,1)}, bf16[2,32,2048]{2,1,0:T(8,128)(2,1)S(1)}, u32[]{:S(2)}, u32[]{:S(2)}) collective-permute-start(bf16[2,32,2048]{2,1,0:T(8,128)(2,1)} %pad_maximum_fusion.3), channel_id=1, source_target_pairs={{0,2},{1,3},{2,0},{3,1},{4,6},{5,7},{6,4},{7,5},{8,10},{9,11},{10,... | collective-permute-start | bytes 786440 | tf_op jit(solution)/shard_map/ppermute | solution.py:358
  23.5 22.2 %copy-start.6 = (bf16[4,512,128]{2,1,0:T(8,128)(2,1)S(1)}, bf16[4,512,128]{2,1,0:T(8,128)(2,1)}, u32[]{:S(2)}) copy-start(bf16[4,512,128]{2,1,0:T(8,128)(2,1)} %param.35) | copy-start | bytes 1572868
  23.5 56.6 %collective-permute-start.3 = (bf16[2,32,2048]{2,1,0:T(8,128)(2,1)}, bf16[2,32,2048]{2,1,0:T(8,128)(2,1)S(1)}, u32[]{:S(2)}, u32[]{:S(2)}) collective-permute-start(bf16[2,32,2048]{2,1,0:T(8,128)(2,1)} %pad_maximum_fusion.4), channel_id=1, source_target_pairs={{0,3},{1,0},{2,1},{3,2},{4,7},{5,4},{6,5},{7,6},{8,11},{9,8},{10,9... | collective-permute-start | bytes 786440 | tf_op jit(solution)/shard_map/ppermute | solution.py:358
  29.5 17.0 %copy-start.24 = (bf16[2048,32]{0,1:T(8,128)(2,1)S(1)}, bf16[2048,32]{0,1:T(8,128)(2,1)}, u32[]{:S(2)}) copy-start(bf16[2048,32]{0,1:T(8,128)(2,1)} %param.36) | copy-start | bytes 393220
  31.7 36.4 %all-to-all-start.1 = ((bf16[32,32,128]{2,1,0:T(8,128)(2,1)}), bf16[32,32,128]{2,1,0:T(8,128)(2,1)S(1)}, u32[]{:S(2)}, u32[]{:S(2)}) async-start(bf16[32,32,128]{2,1,0:T(8,128)(2,1)} %get-tuple-element.12), calls=%async_computation.1 | async-start | bytes 524288 | tf_op jit(solution)/shard_map/all_to_all | solution.py:205
  68.2 9.3 %collective-permute-start = (bf16[32,8,128]{2,1,0:T(8,128)(2,1)S(1)}, bf16[32,8,128]{2,1,0:T(8,128)(2,1)}, u32[]{:S(2)}, u32[]{:S(2)}) collective-permute-start(bf16[32,8,128]{2,1,0:T(8,128)(2,1)S(1)} %slice.140), channel_id=1, source_target_pairs={{0,16},{16,0},{1,17},{17,1},{2,18},{18,2},{3,19},{19,3},{4,20},{20... | collective-permute-start | bytes 196616 | tf_op jit(solution)/shard_map/ppermute | solution.py:383
  71.8 20.1 %all-to-all-start.2 = ((bf16[16,208,128]{2,1,0:T(8,128)(2,1)}), bf16[16,208,128]{2,1,0:T(8,128)(2,1)S(1)}, u32[]{:S(2)}, u32[]{:S(2)}) async-start(bf16[16,208,128]{2,1,0:T(8,128)(2,1)} %bitcast.17), calls=%async_computation.2 | async-start | bytes 1703936 | tf_op jit(solution)/shard_map/all_to_all | solution.py:205
  77.5 2.5 %copy-start.29 = (bf16[2048]{0:T(1024)(128)(2,1)S(1)}, bf16[2048]{0:T(1024)(128)(2,1)}, u32[]{:S(2)}) copy-start(bf16[2048]{0:T(1024)(128)(2,1)} %param.42) | copy-start | bytes 12292
  91.9 7.3 %copy-start.16 = (bf16[4,32,128]{2,1,0:T(8,128)(2,1)S(1)}, bf16[4,32,128]{2,1,0:T(8,128)(2,1)}, u32[]{:S(2)}) copy-start(bf16[4,32,128]{2,1,0:T(8,128)(2,1)} %get-tuple-element.30) | copy-start | bytes 98308
  91.9 7.3 %copy-start.17 = (bf16[4,32,128]{2,1,0:T(8,128)(2,1)S(1)}, bf16[4,32,128]{2,1,0:T(8,128)(2,1)}, u32[]{:S(2)}) copy-start(bf16[4,32,128]{2,1,0:T(8,128)(2,1)} %get-tuple-element.31) | copy-start | bytes 98308
  91.9 7.3 %copy-start.18 = (bf16[4,32,128]{2,1,0:T(8,128)(2,1)S(1)}, bf16[4,32,128]{2,1,0:T(8,128)(2,1)}, u32[]{:S(2)}) copy-start(bf16[4,32,128]{2,1,0:T(8,128)(2,1)} %get-tuple-element.32) | copy-start | bytes 98308
  91.9 7.3 %copy-start.19 = (bf16[4,32,128]{2,1,0:T(8,128)(2,1)S(1)}, bf16[4,32,128]{2,1,0:T(8,128)(2,1)}, u32[]{:S(2)}) copy-start(bf16[4,32,128]{2,1,0:T(8,128)(2,1)} %get-tuple-element.33) | copy-start | bytes 98308
  91.9 7.3 %copy-start.20 = (bf16[4,32,128]{2,1,0:T(8,128)(2,1)S(1)}, bf16[4,32,128]{2,1,0:T(8,128)(2,1)}, u32[]{:S(2)}) copy-start(bf16[4,32,128]{2,1,0:T(8,128)(2,1)} %get-tuple-element.34) | copy-start | bytes 98308
  91.9 7.3 %copy-start.21 = (bf16[4,32,128]{2,1,0:T(8,128)(2,1)S(1)}, bf16[4,32,128]{2,1,0:T(8,128)(2,1)}, u32[]{:S(2)}) copy-start(bf16[4,32,128]{2,1,0:T(8,128)(2,1)} %get-tuple-element.35) | copy-start | bytes 98308
  91.9 7.3 %copy-start.22 = (bf16[4,32,128]{2,1,0:T(8,128)(2,1)S(1)}, bf16[4,32,128]{2,1,0:T(8,128)(2,1)}, u32[]{:S(2)}) copy-start(bf16[4,32,128]{2,1,0:T(8,128)(2,1)} %get-tuple-element.36) | copy-start | bytes 98308
  91.9 7.3 %copy-start.23 = (bf16[4,32,128]{2,1,0:T(8,128)(2,1)S(1)}, bf16[4,32,128]{2,1,0:T(8,128)(2,1)}, u32[]{:S(2)}) copy-start(bf16[4,32,128]{2,1,0:T(8,128)(2,1)} %get-tuple-element.44) | copy-start | bytes 98308
  94.0 5.3 %copy-start.8 = (bf16[4,32,128]{2,1,0:T(8,128)(2,1)S(1)}, bf16[4,32,128]{2,1,0:T(8,128)(2,1)}, u32[]{:S(2)}) copy-start(bf16[4,32,128]{2,1,0:T(8,128)(2,1)} %get-tuple-element.29) | copy-start | bytes 98308
  94.0 5.3 %copy-start.9 = (bf16[4,32,128]{2,1,0:T(8,128)(2,1)S(1)}, bf16[4,32,128]{2,1,0:T(8,128)(2,1)}, u32[]{:S(2)}) copy-start(bf16[4,32,128]{2,1,0:T(8,128)(2,1)} %get-tuple-element.37) | copy-start | bytes 98308
  94.0 5.3 %copy-start.10 = (bf16[4,32,128]{2,1,0:T(8,128)(2,1)S(1)}, bf16[4,32,128]{2,1,0:T(8,128)(2,1)}, u32[]{:S(2)}) copy-start(bf16[4,32,128]{2,1,0:T(8,128)(2,1)} %get-tuple-element.38) | copy-start | bytes 98308
  94.0 5.3 %copy-start.11 = (bf16[4,32,128]{2,1,0:T(8,128)(2,1)S(1)}, bf16[4,32,128]{2,1,0:T(8,128)(2,1)}, u32[]{:S(2)}) copy-start(bf16[4,32,128]{2,1,0:T(8,128)(2,1)} %get-tuple-element.39) | copy-start | bytes 98308
  94.0 5.3 %copy-start.12 = (bf16[4,32,128]{2,1,0:T(8,128)(2,1)S(1)}, bf16[4,32,128]{2,1,0:T(8,128)(2,1)}, u32[]{:S(2)}) copy-start(bf16[4,32,128]{2,1,0:T(8,128)(2,1)} %get-tuple-element.40) | copy-start | bytes 98308
  94.1 5.3 %copy-start.13 = (bf16[4,32,128]{2,1,0:T(8,128)(2,1)S(1)}, bf16[4,32,128]{2,1,0:T(8,128)(2,1)}, u32[]{:S(2)}) copy-start(bf16[4,32,128]{2,1,0:T(8,128)(2,1)} %get-tuple-element.41) | copy-start | bytes 98308
  94.1 5.3 %copy-start.14 = (bf16[4,32,128]{2,1,0:T(8,128)(2,1)S(1)}, bf16[4,32,128]{2,1,0:T(8,128)(2,1)}, u32[]{:S(2)}) copy-start(bf16[4,32,128]{2,1,0:T(8,128)(2,1)} %get-tuple-element.42) | copy-start | bytes 98308
  94.1 5.3 %copy-start.15 = (bf16[4,32,128]{2,1,0:T(8,128)(2,1)S(1)}, bf16[4,32,128]{2,1,0:T(8,128)(2,1)}, u32[]{:S(2)}) copy-start(bf16[4,32,128]{2,1,0:T(8,128)(2,1)} %get-tuple-element.43) | copy-start | bytes 98308
  94.1 17.3 %all-to-all-start.3 = ((bf16[16,184,128]{2,1,0:T(8,128)(2,1)}), bf16[16,184,128]{2,1,0:T(8,128)(2,1)S(1)}, u32[]{:S(2)}, u32[]{:S(2)}) async-start(bf16[16,184,128]{2,1,0:T(8,128)(2,1)} %get-tuple-element.16), calls=%async_computation.3 | async-start | bytes 1507328 | tf_op jit(solution)/shard_map/all_to_all | solution.py:205
  112.7 23.8 %all-to-all-start.4 = ((bf16[32,24,128]{2,1,0:T(8,128)(2,1)}), bf16[32,24,128]{2,1,0:T(8,128)(2,1)S(1)}, u32[]{:S(2)}, u32[]{:S(2)}) async-start(bf16[32,24,128]{2,1,0:T(8,128)(2,1)} %return_rows.1), calls=%async_computation.4 | async-start | bytes 393216 | tf_op jit(solution)/shard_map/all_to_all | solution.py:205
  116.8 19.7 %copy-start.32 = (f32[48,4]{0,1:T(4,128)S(1)}, f32[48,4]{0,1:T(4,128)}, u32[]{:S(2)}) copy-start(f32[48,4]{0,1:T(4,128)} %param.32) | copy-start | bytes 2308
  116.9 25.4 %copy-start.3 = (f32[48,1,64,64]{3,2,1,0:T(8,128)S(1)}, f32[48,1,64,64]{3,2,1,0:T(8,128)}, u32[]{:S(2)}) copy-start(f32[48,1,64,64]{3,2,1,0:T(8,128)} %param.23) | copy-start | bytes 2359300
  117.0 25.4 %copy-start.25 = (f32[48,64]{1,0:T(8,128)S(1)}, f32[48,64]{1,0:T(8,128)}, u32[]{:S(2)}) copy-start(f32[48,64]{1,0:T(8,128)} %maximum_multiply_fusion.1) | copy-start | bytes 36868
  137.7 11.0 %all-to-all-start.5 = ((f32[16,2,48]{2,1,0:T(2,128)}), f32[16,2,48]{2,1,0:T(2,128)S(1)}, u32[]{:S(2)}, u32[]{:S(2)}) async-start(f32[16,2,48]{2,1,0:T(2,128)} %broadcast_in_dim.46), calls=%async_computation.5 | async-start | bytes 32768 | tf_op jit(solution)/shard_map/all_to_all | solution.py:205
  142.4 6.3 %copy-start.31 = (f32[128]{0:T(128)S(1)}, f32[128]{0:T(128)}, u32[]{:S(2)}) copy-start(f32[128]{0:T(128)} %param.43) | copy-start | bytes 1540

commit v4 on v3

--- a/solution.py
+++ b/solution.py
@@ -15,6 +15,12 @@
 GROUP_EPS = 1e-06
 ROPE_BASE = 10000.0
 ACROSS = ((1,), (1,))
+EP = ("z", "core")
+PITCH = 24
+RIDER = 8
+FLAT = ((1,), (0,))
+GROUP = 8
+GRANT = 12 * 1024 * 1024
 
 
 def in_order(parts, dim):
@@ -44,26 +50,50 @@
     return [pltpu.with_memory_space_constraint(a, pltpu.VMEM) for a in arrays]
 
 
+def far(*arrays):
+    return [pltpu.with_memory_space_constraint(a, pltpu.HBM) for a in arrays]
+
+
 def project_kernel(tokens, lengths, *refs):
-    count = (len(refs) - 4) // 2
-    weights, (out, positions) = refs[:count], refs[count : count + 2]
-    rows, held, arrived = refs[count + 2], refs[count + 3 : -1], refs[-1]
-    fetch = [
-        pltpu.make_async_copy(source, target, arrived.at[i])
-        for i, (source, target) in enumerate(zip((tokens, *weights), (rows, *held)))
-    ]
-    for f in fetch:
-        f.start()
-    positions[...] = lengths[...].astype(jnp.float32)
-    fetch[0].wait()
-    for i, w in enumerate(held):
-        fetch[i + 1].wait()
-        cols = w.shape[0]
-        part = f32_dot(rows[...], w[...], ACROSS).astype(jnp.bfloat16)
-        out[:, i * cols : (i + 1) * cols] = part.astype(jnp.float32)
-
-
-def project_all(tokens, lengths, weights):
+    count = (len(refs) - 6) // 2
+    weights, outs = refs[:count], refs[count:-6]
+    positions, own_cols, rows, held, counts, arrived = refs[-6:]
+    cols, width = weights[0].shape
+    long = pltpu.make_async_copy(lengths, counts, arrived.at[2, 0])
+    span = width // 2
+    fetch = []
+    for h in range(2):
+        at = pl.ds(h * span, span)
+        fetch.append(
+            [pltpu.make_async_copy(tokens.at[:, at], rows.at[:, at], arrived.at[h, 0])]
+            + [
+                pltpu.make_async_copy(
+                    w.at[:, at], held.at[pl.ds(i * cols, cols), at], arrived.at[h, i + 1]
+                )
+                for i, w in enumerate(weights)
+            ]
+        )
+        for f in fetch[h]:
+            f.start()
+    long.start()
+    total = None
+    for h, group in enumerate(fetch):
+        for f in group:
+            f.wait()
+        at = slice(h * span, (h + 1) * span)
+        part = f32_dot(rows[:, at], held[:, at], ACROSS)
+        total = part if total is None else total + part
+    column = lax.axis_index("tp_0") * lax.axis_size("tp_1") + lax.axis_index("tp_1")
+    size = own_cols.shape[1]
+    own_cols[...] = rows[:, pl.ds(pl.multiple_of(column * size, size), size)]
+    long.wait()
+    positions[...] = counts[...].astype(jnp.float32)
+    rounded = total.astype(jnp.bfloat16).astype(jnp.float32)
+    for i, out in enumerate(outs):
+        out[...] = rounded[:, i * cols : (i + 1) * cols]
+
+
+def project_all(tokens, lengths, weights, parts):
     rows, width = tokens.shape
     cols = weights[0].shape[1]
     count = len(weights)
@@ -71,21 +101,29 @@
     whole = pl.BlockSpec(memory_space=pltpu.VMEM)
     return pl.pallas_call(
         project_kernel,
-        in_specs=[anywhere, whole] + [anywhere] * count,
-        out_specs=[whole, whole],
-        out_shape=[
-            pltpu.VMEM((rows, cols * count), jnp.float32),
+        in_specs=[anywhere] * (count + 2),
+        out_specs=[whole] * (count + 2),
+        out_shape=[pltpu.VMEM((rows, cols), jnp.float32)] * count
+        + [
             pltpu.VMEM(lengths.shape, jnp.float32),
-        ],
-        scratch_shapes=[pltpu.VMEM((rows, width), tokens.dtype)]
-        + [pltpu.VMEM((cols, width), weights[0].dtype)] * count
-        + [pltpu.SemaphoreType.DMA((count + 1,))],
+            pltpu.VMEM((rows, width // parts), tokens.dtype),
+        ],
+        scratch_shapes=[
+            pltpu.VMEM((rows, width), tokens.dtype),
+            pltpu.VMEM((cols * count, width), weights[0].dtype),
+            pltpu.VMEM(lengths.shape, lengths.dtype),
+            pltpu.SemaphoreType.DMA((3, count + 1)),
+        ],
         name="project",
-    )(tokens, lengths, *[w.T for w in weights])
-
-
-def dispatch_kernel(folded_all, out_weight, own_cols, table, rider, outgoing, exact, short, lhs, rhs):
+        compiler_params=pltpu.CompilerParams(vmem_limit_bytes=GRANT),
+    )(*far(tokens, lengths, *[w.T for w in weights]))
+
+
+def dispatch_kernel(
+    folded_all, out_weight, table, rider, own_cols, outgoing, exact, short, lhs, rhs
+):
     parts, half, lanes = folded_all.shape
+    cols = out_weight.shape[1]
     width = lanes // 2
     lane = lax.broadcasted_iota(jnp.int32, (half, lanes), 1)
     for t in range(parts):
@@ -97,21 +135,20 @@
             rhs[t * lanes + i * width : t * lanes + (i + 1) * width] = out_weight[
                 t * width : (t + 1) * width
             ]
-    flat = ((1,), (0,))
-    mixing = jnp.concatenate([f32_dot(lhs[i], rhs[...], flat) for i in range(2)], 0)
+    mixing = jnp.concatenate([f32_dot(lhs[i], rhs[...], FLAT) for i in range(2)], 0)
     pre_first = RESIDUAL_SCALE * own_cols[...].astype(jnp.float32) + mixing
     exact[...] = pre_first
     pre_short = pre_first.astype(short.dtype)
     short[...] = pre_short
-    peers, _, cols = outgoing.shape
-    rows = f32_dot(table[...], pre_short, flat).reshape(peers, PITCH, cols)
+    peers = outgoing.shape[0]
+    rows = f32_dot(table[...], pre_short, FLAT).reshape(peers, PITCH, cols)
     riders = rider[...].astype(jnp.float32)
     riders = jnp.broadcast_to(riders[None], (peers // riders.shape[0], *riders.shape))
     riders = riders.reshape(peers, RIDER, cols)
     outgoing[...] = jnp.concatenate([rows, riders], 1).astype(outgoing.dtype)
 
 
-def dispatch_rows(folded_all, out_weight, own_cols, table, rider, peers):
+def dispatch_rows(folded_all, out_weight, table, rider, own_cols, peers):
     parts, half, lanes = folded_all.shape
     rows, cols = own_cols.shape
     bf16 = jnp.bfloat16
@@ -130,20 +167,130 @@
             pltpu.VMEM((parts * lanes, cols), bf16),
         ],
         name="dispatch_rows",
-    )(*near(folded_all, out_weight, own_cols, table, rider))
+        compiler_params=pltpu.CompilerParams(vmem_limit_bytes=GRANT),
+    )(*near(folded_all, out_weight, table, rider, own_cols))
+
+
+def pieces_kernel(ready, gate_t, up_t, *refs):
+    del ready
+    pieces, moved = refs[:-1], refs[-1]
+    experts = gate_t.shape[0]
+    lane = lax.axis_index("tp_1")
+    moves = [
+        pltpu.make_async_copy(w.at[(lane + d) % experts], piece.at[i], moved.at[d, i])
+        for d, piece in enumerate(pieces)
+        for i, w in enumerate((gate_t, up_t))
+    ]
+    for m in moves:
+        m.start()
+    for m in moves:
+        m.wait()
+
+
+def expert_pieces(ready, gate_t, up_t):
+    experts, units, width = gate_t.shape
+    anywhere = pl.BlockSpec(memory_space=pl.ANY)
+    whole = pl.BlockSpec(memory_space=pltpu.VMEM)
+    return pl.pallas_call(
+        pieces_kernel,
+        in_specs=[whole] + [anywhere] * 2,
+        out_specs=[whole] * experts,
+        out_shape=[pltpu.VMEM((2, units, width), gate_t.dtype)] * experts,
+        scratch_shapes=[pltpu.SemaphoreType.DMA((experts, 2))],
+        name="expert_pieces",
+        compiler_params=pltpu.CompilerParams(vmem_limit_bytes=GRANT),
+    )(*near(ready), *far(gate_t, up_t))
+
+
+def mixed_kernel(result, gate_act, message, folded, sent):
+    value = result[...]
+    scale = lax.rsqrt(jnp.mean(value * value, -1, keepdims=True) + GROUP_EPS)
+    mixed = value * scale * jax.nn.silu(gate_act[...])
+    half = mixed.shape[0] // 2
+    folded[...] = jnp.concatenate([mixed[:half], mixed[half:]], 1).astype(folded.dtype)
+    copies = [
+        pltpu.make_async_copy(folded, message.at[t], sent.at[t]) for t in range(message.shape[0])
+    ]
+    for c in copies:
+        c.start()
+    for c in copies:
+        c.wait()
+
+
+def mixed_message(result, gate_act, peers):
+    rows, width = result.shape
+    whole = pl.BlockSpec(memory_space=pltpu.VMEM)
+    return pl.pallas_call(
+        mixed_kernel,
+        in_specs=[whole] * 2,
+        out_specs=pl.BlockSpec(memory_space=pl.ANY),
+        out_shape=jax.ShapeDtypeStruct((peers, rows // 2, 2 * width), jnp.bfloat16),
+        scratch_shapes=[
+            pltpu.VMEM((rows // 2, 2 * width), jnp.bfloat16),
+            pltpu.SemaphoreType.DMA((peers,)),
+        ],
+        name="mixed_message",
+        compiler_params=pltpu.CompilerParams(vmem_limit_bytes=GRANT),
+    )(*near(result, gate_act))
+
+
+def slot_kernel(arrived, own, regroup, message, rows, sent):
+    experts, row_count, cols = rows.shape
+    peers, pitch, _ = arrived.shape
+    slots = row_count - own.shape[0]
+    groups = peers // GROUP
+    count = slots // groups
+    for j in range(experts):
+        rows[j, slots:] = own[...]
+    for g in range(groups):
+        block = arrived[g * GROUP : (g + 1) * GROUP].reshape(GROUP * pitch, cols)
+        moved = f32_dot(regroup[...], block, FLAT).astype(rows.dtype)
+        for j in range(experts):
+            rows[j, g * count : (g + 1) * count] = moved[j * count : (j + 1) * count]
+    copies = [
+        pltpu.make_async_copy(rows, message.at[q], sent.at[q]) for q in range(message.shape[0])
+    ]
+    for c in copies:
+        c.start()
+    for c in copies:
+        c.wait()
+
+
+def slot_message(arrived, own, regroup, experts, slots, copies):
+    cols = own.shape[1]
+    whole = pl.BlockSpec(memory_space=pltpu.VMEM)
+    rows = slots + own.shape[0]
+    return pl.pallas_call(
+        slot_kernel,
+        in_specs=[whole] * 3,
+        out_specs=pl.BlockSpec(memory_space=pl.ANY),
+        out_shape=jax.ShapeDtypeStruct((copies, experts, rows, cols), jnp.bfloat16),
+        scratch_shapes=[
+            pltpu.VMEM((experts, rows, cols), jnp.bfloat16),
+            pltpu.SemaphoreType.DMA((copies,)),
+        ],
+        name="slot_message",
+        compiler_params=pltpu.CompilerParams(vmem_limit_bytes=GRANT),
+    )(*near(arrived, own, regroup))
 
 
 def return_kernel(hidden_all, down, goes, sent_back):
     parts, experts = down.shape[1], down.shape[0]
-    slots = goes.shape[1] // experts
-    flat = ((1,), (0,))
+    peers, pitch, cols = sent_back.shape
+    groups = peers // GROUP
+    count = goes.shape[1] // experts
+    slots = count * groups
     results = []
     for j in range(experts):
         rows = jnp.concatenate([hidden_all[q * experts + j, :slots] for q in range(parts)], 1)
         mats = jnp.concatenate([down[j, q] for q in range(parts)], 0)
-        results.append(f32_dot(rows, mats, flat).astype(sent_back.dtype))
-    back = f32_dot(goes[...], jnp.concatenate(results, 0), flat)
-    sent_back[...] = back.reshape(sent_back.shape).astype(sent_back.dtype)
+        results.append(f32_dot(rows, mats, FLAT))
+    for g in range(groups):
+        block = jnp.concatenate([r[g * count : (g + 1) * count] for r in results], 0)
+        back = f32_dot(goes[...], block.astype(sent_back.dtype), FLAT)
+        sent_back[g * GROUP : (g + 1) * GROUP] = back.reshape(GROUP, pitch, cols).astype(
+            sent_back.dtype
+        )
 
 
 def return_rows(hidden_all, down, goes, peers):
@@ -153,8 +300,9 @@
         return_kernel,
         in_specs=[whole] * 3,
         out_specs=whole,
-        out_shape=jax.ShapeDtypeStruct((peers, goes.shape[0] // peers, cols), jnp.bfloat16),
+        out_shape=jax.ShapeDtypeStruct((peers, PITCH, cols), jnp.bfloat16),
         name="return_rows",
+        compiler_params=pltpu.CompilerParams(vmem_limit_bytes=GRANT),
     )(*near(hidden_all, down, goes))
 
 
@@ -172,10 +320,9 @@
     head_count = retention_state.shape[1]
     head_width = retention_state.shape[2]
 
-    projected, positions = project_all(
-        tokens, lengths, (query_weight, key_weight, value_weight, gate_weight)
-    )
-    queries, keys, values, gate_act = jnp.split(projected, 4, 1)
+    queries, keys, values, gate_act, positions, own_cols = project_all(
+        tokens, lengths, (query_weight, key_weight, value_weight, gate_weight), lax.axis_size(TP)
+    )
     by_head = (row_count, head_count, head_width)
     queries = rotate(queries.reshape(by_head), positions)
     key_rows = rotate(keys.reshape(by_head), positions) * head_width ** (-0.5)
@@ -189,16 +336,8 @@
         decays[None, :, None, None] * retention_state
         + key_rows[:, :, :, None] * values[:, :, None, :]
     )
-    normed = result * lax.rsqrt(jnp.mean(result * result, -1, keepdims=True) + GROUP_EPS)
-    mixed_heads = (
-        normed.reshape(row_count, head_count * head_width) * jax.nn.silu(gate_act)
-    ).astype(jnp.bfloat16)
-    return (mixed_heads, new_state)
-
-
-EP = ("z", "core")
-PITCH = 24
-RIDER = 8
+    result = result.reshape(row_count, head_count * head_width)
+    return (mixed_message(result, gate_act, lax.axis_size(TP)), new_state, own_cols)
 
 
 def swap(parts, axis):
@@ -215,7 +354,7 @@
 
 
 def hidden_kernel(rows_pre, gains, pre_first, own_gain, local_weights, *refs):
-    pieces, (message, normed_cols, switch, normed, hidden, sent) = refs[:-6], refs[-6:]
+    pieces, (message, normed_cols, switch, normed, hidden, gate_up, sent) = refs[:-7], refs[-7:]
     parts, row_count, cols = rows_pre.shape
     own_rows = pre_first.shape[0]
     slots = row_count - own_rows
@@ -235,9 +374,14 @@
     normed_cols[...] = ((pre_first[...] - mean[slots:]) * scale[slots:] * own_gain[...]).astype(
         normed_cols.dtype
     )
-    gate_up = jnp.concatenate([p[i] for i in range(2) for p in pieces], 0)
     units = gate_up.shape[0] // 2
-    both = f32_dot(normed[:slots], gate_up, ACROSS)
+    lane = lax.axis_index("tp_1")
+    for d, piece in enumerate(pieces):
+        span = piece.shape[1]
+        start = (lane + len(pieces) - d) % len(pieces) * span
+        for i in range(2):
+            gate_up[pl.ds(pl.multiple_of(i * units + start, span), span)] = piece[i]
+    both = f32_dot(normed[:slots], gate_up[...], ACROSS)
     hidden[:slots] = (jax.nn.silu(both[:, :units]) * both[:, units:]).astype(hidden.dtype)
     local = f32_dot(normed[slots:], local_weights[...], ACROSS)
     cut = (local.shape[1] - RIDER) // 2
@@ -272,9 +416,11 @@
         scratch_shapes=[
             pltpu.VMEM((row_count, parts * cols), jnp.bfloat16),
             pltpu.VMEM((row_count - own_rows // 2, units), jnp.bfloat16),
+            pltpu.VMEM((2 * units, parts * cols), jnp.bfloat16),
             pltpu.SemaphoreType.DMA((parts,)),
         ],
         name="hidden_units",
+        compiler_params=pltpu.CompilerParams(vmem_limit_bytes=GRANT),
     )(*near(rows_pre, gains, pre_first, own_gain, local_weights, *pieces))
 
 
@@ -318,7 +464,7 @@
     tp_rank = lax.axis_index(TP)
     col_start = tp_rank * col_count
 
-    mixed_heads, new_state = retain(
+    folded, new_state, own_cols = retain(
         tokens,
         retention_state,
         lengths,
@@ -328,9 +474,7 @@
         gate_weight,
         tp_rank * head_count,
     )
-    half = seq_rows // 2
-    folded = jnp.concatenate([mixed_heads[:half], mixed_heads[half:]], 1)
-    folded_all = to_all(folded, TP)
+    folded_all = swap(folded, TP)
 
     same = routing.reshape(-1)[:, None] == routing.reshape(-1)[None, :]
     row_of = jnp.arange(seq_rows * top_count, dtype=jnp.int32) // top_count
@@ -345,26 +489,6 @@
         table = table | (wire_ids[:, None] == slot_ids[None, :, k])
     table = table.astype(bf16)
     slot_hot = (slot_ids.T.reshape(-1)[:, None] == wire_ids[None, :]).astype(bf16)
-
-    lane = lax.axis_index("tp_1")
-    gate_up = (jnp.swapaxes(expert_gate, 1, 2), jnp.swapaxes(expert_up, 1, 2))
-
-    def piece_for(expert):
-        return jnp.stack([lax.dynamic_index_in_dim(w, expert, 0, False) for w in gate_up])
-
-    pieces = [piece_for(lane)]
-    for d in range(1, class_count):
-        steps = [(i, (i + d) % class_count) for i in range(class_count)]
-        pieces.append(lax.ppermute(piece_for((lane + d) % class_count), "tp_1", steps))
-    down = expert_down.reshape(local_experts, part_count, class_count, hidden_cols, col_count)
-    down = jnp.stack(
-        [
-            jnp.concatenate([down[j, :, (j - d) % class_count] for d in range(class_count)], 1)
-            for j in range(local_experts)
-        ]
-    )
-
-    own_cols = lax.dynamic_slice_in_dim(tokens, col_start, col_count, 1)
 
     side_cols = side_gate.shape[1]
     side_rows = side_gate.shape[0]
@@ -373,11 +497,19 @@
     outgoing, pre_first, pre_short = dispatch_rows(
         folded_all,
         out_weight,
-        own_cols,
         table,
         side_piece.reshape(core_count, RIDER, 2 * side_rows),
+        own_cols,
         ep_count,
     )
+    pieces = list(
+        expert_pieces(
+            pre_short, jnp.swapaxes(expert_gate, 1, 2), jnp.swapaxes(expert_up, 1, 2)
+        )
+    )
+    for d in range(1, class_count):
+        steps = [(i, (i + d) % class_count) for i in range(class_count)]
+        pieces[d] = lax.ppermute(pieces[d], "tp_1", steps)
     arrived = swap(outgoing, EP)
     side_own = arrived[:, PITCH:]
     side_other = lax.ppermute(side_own, "core", [(0, 1), (1, 0)])
@@ -391,24 +523,14 @@
     ).reshape(ep_count, side_cols, 2, side_rows)
     side_all = jnp.transpose(side_all, (2, 1, 0, 3)).reshape(2, side_cols, model_width)
 
-    order = jnp.arange(local_experts * slots, dtype=jnp.int32)
-    source, expert, place = (order % slots) // capacity, order // slots, order % capacity
-    spot = expert * capacity + place
+    order = jnp.arange(local_experts * GROUP * capacity, dtype=jnp.int32)
+    expert, source = order // (GROUP * capacity), order // capacity % GROUP
+    spot = expert * capacity + order % capacity
     came_at = source * (PITCH + RIDER) + spot
     regroup = (
-        came_at[:, None] == jnp.arange(ep_count * (PITCH + RIDER), dtype=jnp.int32)[None, :]
+        came_at[:, None] == jnp.arange(GROUP * (PITCH + RIDER), dtype=jnp.int32)[None, :]
     ).astype(bf16)
-    by_expert = jnp.dot(
-        regroup, arrived.reshape(-1, col_count), preferred_element_type=jnp.float32
-    ).astype(bf16)
-    own_too = jnp.concatenate(
-        [
-            by_expert.reshape(local_experts, slots, col_count),
-            jnp.broadcast_to(pre_short[None], (local_experts, seq_rows, col_count)),
-        ],
-        1,
-    )
-    to_send = jnp.broadcast_to(own_too[None], (part_count, *own_too.shape))
+    to_send = slot_message(arrived, pre_short, regroup, local_experts, slots, part_count)
     rows_pre = swap(to_send.reshape(tp_count, slots + seq_rows, col_count), TP)
     own_gain = lax.dynamic_slice_in_dim(first_gain, col_start, col_count, 0)
     units = class_count * hidden_cols
@@ -429,8 +551,8 @@
 
     hidden_all = swap(hidden, TP)
     goes_at = source * PITCH + spot
-    goes = (wire_ids[:, None] == goes_at[None, :]).astype(bf16)
-    down = down.reshape(local_experts, part_count, units, col_count)
+    goes = (wire_ids[: GROUP * PITCH, None] == goes_at[None, :]).astype(bf16)
+    down = expert_down.reshape(local_experts, part_count, units, col_count)
     returned = swap(return_rows(hidden_all, down, goes, ep_count), EP)
 
     local_all = hidden_all[:, slots:]
@@ -465,6 +587,7 @@
     routed = jnp.sum(picked * route_weight.T[:, :, None], 0)
     pre_second = local_sum + routed
     sums = jnp.stack([jnp.sum(pre_second, -1), jnp.sum(pre_second * pre_second, -1)])
+    sums, new_state = lax.optimization_barrier((sums, new_state))
     totals = jnp.sum(to_all(sums, TP), 0)
     mean_second = totals[0][:, None] / model_width
     square_second = totals[1][:, None] / model_width

time: 150 us -> 150 us (level)
  blocking collectives: 0 us -> 10.4 us
  waiting for transfers between devices: 68.8 us -> 61.8 us
  starting transfers between devices: 54.9 us -> 49.9 us
  Pallas kernels: 7.64 us -> 10.1 us
  local copies, waits for them, and re-layouts: 6.73 us -> 8.95 us
  other arithmetic: 8.24 us -> 6.25 us
    all_to_all x0 -> x1, blocking collectives: none -> 10.4 us  [swap(): return lax.all_to_all(parts, axis, 0, 0, tiled=True)]
    all_to_all x6 -> x5, waiting for transfers between devices: 68.8 us -> 61.8 us  [swap(): return lax.all_to_all(parts, axis, 0, 0, tiled=True)]
    all_to_all x6 -> x5, starting transfers between devices: 42.3 us -> 38.3 us  [swap(): return lax.all_to_all(parts, axis, 0, 0, tiled=True)]
    pallas_call x1 -> x4, Pallas kernels: 3.06 us -> 5.58 us  [the longest x1 2.11 us: project_all(): pl.pallas_call(project_kernel, in_specs=[anywhere] * (count + 2), out_spe...]
    another operation x7 -> x0, other arithmetic: 2.36 us -> none  [the longest x4 2.24 us: piece_for(): jnp.stack([lax.dynamic_index_in_dim(w, expert, 0, False) for w in gate_up])]
    reshape x2, local copies, waits for them, and re-layouts: 0.24 us -> 1.89 us  [on_device(): side_all = jnp.concatenate([jnp.where(first_core, side_own, side_other),...]
    broadcast_in_dim x4, local copies, waits for them, and re-layouts: 0.29 us -> 1.84 us  [spread(): weight = jnp.broadcast_to(weight, (tp_count, 2, units // 2, col_count))]
  transfers between devices with their start and end apart: 10 -> 9, of which waited for: 5 -> 5; matrix products, arithmetic and copies ran while one was open for 9% -> 9% of each run, Pallas kernels for 1% -> 2%
where the time goes in v4:
time: 150 us
  waiting for transfers between devices  61.8 us (41%)
  starting transfers between devices  49.9 us (33%)
  blocking collectives  10.4 us (7%)
  Pallas kernels  10.1 us (7%)
  local copies, waits for them, and re-layouts  8.95 us (6%)
  other arithmetic  6.25 us (4%)
    all_to_all x5, waiting for transfers between devices, swap(): return lax.all_to_all(parts, axis, 0, 0, tiled=True)  61.8 us
    all_to_all x5, starting transfers between devices, swap(): return lax.all_to_all(parts, axis, 0, 0, tiled=True)  38.3 us
    all_to_all x1, blocking collectives, swap(): return lax.all_to_all(parts, axis, 0, 0, tiled=True)  10.4 us
    ppermute x3, starting transfers between devices, on_device(): pieces[d] = lax.ppermute(pieces[d], 'tp_1', steps)  9.72 us
    add x1, other arithmetic, retain(): decays[None, :, None, None] * retention_state  3.09 us
  transfers between devices with their start and end apart: 9, of which 5 were waited for; matrix products, arithmetic and copies ran while one was open for 9% of the time, Pallas kernels for 2%

profile of v4, /device:TPU:2, one launch (start us, length us, event | category | flops | bytes accessed | tf_op | source)
XLA Modules:
  0.0 149.6 jit_solution(6890543625791446462)
XLA Ops:
  0.7 2.1 %project.1 = (f32[48,64]{1,0:T(8,128)S(1)}, f32[48,64]{1,0:T(8,128)S(1)}, f32[48,64]{1,0:T(8,128)S(1)}, f32[48,64]{1,0:T(8,128)S(1)}, f32[48]{0:T(128)S(1)}, /*index=5*/bf16[48,128]{1,0:T(8,128)(2,1)S(1)}) custom-call(bf16[48,2048]{1,0:T(8,128)(2,1)} %tokens.1, s32[48]{0:T(128)} %lengths.1, bf16[64,2048]{1,0:T(8,128)(2,1)} %bitcast.102, ...), custom_call_target="tpu_custom_call" | custom-call | tf_op jit(solution)/shard_map/project/pallas_call | solution.py:102
  2.8 0.2 fusion.25
  3.0 0.2 fusion.34
  3.2 0.3 fusion.50
  3.7 1.0 mixed_message.1
  4.6 9.2 %all-to-all-start = ((bf16[16,24,128]{2,1,0:T(8,128)(2,1)}), bf16[16,24,128]{2,1,0:T(8,128)(2,1)S(1)}, u32[]{:S(2)}, u32[]{:S(2)}) async-start(bf16[16,24,128]{2,1,0:T(8,128)(2,1)} %mixed_message.1), calls=%async_computation | async-start | bytes 196608 | tf_op jit(solution)/shard_map/all_to_all | solution.py:344
  14.0 0.2 convert_reduce_fusion
  14.2 0.1 reshape.443
  14.4 0.2 slice_reduce_fusion.3
  14.6 0.2 fusion.8.table
  14.9 5.4 %all-to-all-done.folded_all = bf16[16,24,128]{2,1,0:T(8,128)(2,1)S(1)} async-done(((bf16[16,24,128]{2,1,0:T(8,128)(2,1)}), bf16[16,24,128]{2,1,0:T(8,128)(2,1)S(1)}, u32[]{:S(2)}, u32[]{:S(2)}) %all-to-all-start) | async-done | bytes 98336 | tf_op jit(solution)/shard_map/all_to_all | solution.py:344
  20.4 1.2 dispatch_rows.1
  21.6 13.7 %all-to-all-start.1 = ((bf16[32,32,128]{2,1,0:T(8,128)(2,1)}), bf16[32,32,128]{2,1,0:T(8,128)(2,1)S(1)}, u32[]{:S(2)}, u32[]{:S(2)}) async-start(bf16[32,32,128]{2,1,0:T(8,128)(2,1)} %get-tuple-element.26), calls=%async_computation.1 | async-start | bytes 524288 | tf_op jit(solution)/shard_map/all_to_all | solution.py:344
  35.4 0.7 pad_bitcast_fusion.1
  36.3 21.7 %all-to-all-done.1.arrived = bf16[32,32,128]{2,1,0:T(8,128)(2,1)S(1)} async-done(((bf16[32,32,128]{2,1,0:T(8,128)(2,1)}), bf16[32,32,128]{2,1,0:T(8,128)(2,1)S(1)}, u32[]{:S(2)}, u32[]{:S(2)}) %all-to-all-start.1) | async-done | bytes 262176 | tf_op jit(solution)/shard_map/all_to_all | solution.py:344
  58.0 0.6 slice.70
  58.6 1.9 %collective-permute-start = (bf16[32,8,128]{2,1,0:T(8,128)(2,1)}, bf16[32,8,128]{2,1,0:T(8,128)(2,1)}, u32[]{:S(2)}, u32[]{:S(2)}) collective-permute-start(bf16[32,8,128]{2,1,0:T(8,128)(2,1)} %slice.70), channel_id=1, source_target_pairs={{0,16},{16,0},{1,17},{17,1},{2,18},{18,2},{3,19},{19,3},{4,20},{20... | collective-permute-start | bytes 196616 | tf_op jit(solution)/shard_map/ppermute | solution.py:515
  60.6 1.3 expert_pieces.1
  62.0 2.6 %collective-permute-start.1 = (bf16[2,32,2048]{2,1,0:T(8,128)(2,1)S(1)}, bf16[2,32,2048]{2,1,0:T(8,128)(2,1)S(1)}, u32[]{:S(2)}, u32[]{:S(2)}) collective-permute-start(bf16[2,32,2048]{2,1,0:T(8,128)(2,1)S(1)} %get-tuple-element.30), channel_id=1, source_target_pairs={{0,1},{1,2},{2,3},{3,0},{4,5},{5,6},{6,7},{7,4},{8,9},{9,10},{10,1... | collective-permute-start | bytes 786440 | tf_op jit(solution)/shard_map/ppermute | solution.py:512
  64.6 4.8 %collective-permute-start.2 = (bf16[2,32,2048]{2,1,0:T(8,128)(2,1)S(1)}, bf16[2,32,2048]{2,1,0:T(8,128)(2,1)S(1)}, u32[]{:S(2)}, u32[]{:S(2)}) collective-permute-start(bf16[2,32,2048]{2,1,0:T(8,128)(2,1)S(1)} %get-tuple-element.31), channel_id=1, source_target_pairs={{0,2},{1,3},{2,0},{3,1},{4,6},{5,7},{6,4},{7,5},{8,10},{9,11},{10,... | collective-permute-start | bytes 786440 | tf_op jit(solution)/shard_map/ppermute | solution.py:512
  69.4 2.4 %collective-permute-start.3 = (bf16[2,32,2048]{2,1,0:T(8,128)(2,1)S(1)}, bf16[2,32,2048]{2,1,0:T(8,128)(2,1)S(1)}, u32[]{:S(2)}, u32[]{:S(2)}) collective-permute-start(bf16[2,32,2048]{2,1,0:T(8,128)(2,1)S(1)} %get-tuple-element.32), channel_id=1, source_target_pairs={{0,3},{1,0},{2,1},{3,2},{4,7},{5,4},{6,5},{7,6},{8,11},{9,8},{10,9... | collective-permute-start | bytes 786440 | tf_op jit(solution)/shard_map/ppermute | solution.py:512
  71.7 1.2 slot_message.1
  72.9 5.4 %all-to-all-start.2 = ((bf16[16,208,128]{2,1,0:T(8,128)(2,1)}), bf16[16,208,128]{2,1,0:T(8,128)(2,1)S(1)}, u32[]{:S(2)}, u32[]{:S(2)}) async-start(bf16[16,208,128]{2,1,0:T(8,128)(2,1)} %bitcast.15), calls=%async_computation.2 | async-start | bytes 1703936 | tf_op jit(solution)/shard_map/all_to_all | solution.py:344
  78.4 0.9 broadcast_select_fusion.3
  79.3 0.8 reshape.447
  80.1 1.1 copy.73
  81.1 0.7 fusion.49
  81.9 1.1 squeeze.6
  83.0 0.9 bitcast_dynamic-update-slice_fusion
  83.9 1.1 squeeze.7
  85.0 6.9 %all-to-all-done.2.rows_pre = bf16[16,208,128]{2,1,0:T(8,128)(2,1)S(1)} async-done(((bf16[16,208,128]{2,1,0:T(8,128)(2,1)}), bf16[16,208,128]{2,1,0:T(8,128)(2,1)S(1)}, u32[]{:S(2)}, u32[]{:S(2)}) %all-to-all-start.2) | async-done | bytes 852000 | tf_op jit(solution)/shard_map/all_to_all | solution.py:344
  91.9 2.1 %hidden_units.1 = (bf16[16,184,128]{2,1,0:T(8,128)(2,1)}, bf16[48,128]{1,0:T(8,128)(2,1)S(1)}, f32[48,1]{1,0:T(8,128)S(1)}) custom-call(bf16[16,208,128]{2,1,0:T(8,128)(2,1)S(1)} %all-to-all-done.2.rows_pre, f32[16,128]{1,0:T(8,128)S(1)} %bitcast.95, f32[48,128]{1,0:T(8,128)S(1)} %get-tuple-element.28.pre_first, ...), custom_call_target="tpu_custom_call" | custom-call | tf_op jit(solution)/shard_map/hidden_units/pallas_call | solution.py:407
  94.0 6.1 %all-to-all-start.3 = ((bf16[16,184,128]{2,1,0:T(8,128)(2,1)}), bf16[16,184,128]{2,1,0:T(8,128)(2,1)S(1)}, u32[]{:S(2)}, u32[]{:S(2)}) async-start(bf16[16,184,128]{2,1,0:T(8,128)(2,1)} %get-tuple-element.34), calls=%async_computation.3 | async-start | bytes 1507328 | tf_op jit(solution)/shard_map/all_to_all | solution.py:344
  100.1 0.9 pad_bitcast_fusion
  101.1 3.1 %multiply_add_fusion = f32[48,1,64,64]{3,2,1,0:T(8,128)} fusion(f32[48,1,64,64]{3,2,1,0:T(8,128)} %param.23, f32[48,64]{1,0:T(8,128)S(1)} %get-tuple-element.23, f32[48,64]{1,0:T(8,128)S(1)} %maximum_multiply_fusion.1, f32[]{:T(128)S(6)} %sub.66), kind=kLoop, calls=%fused_computation.2 | loop fusion | flops 589824 | bytes 1597444 | tf_op jit(solution)/shard_map/add | solution.py:336
  104.2 8.7 %all-to-all-done.3.hidden_all = bf16[16,184,128]{2,1,0:T(8,128)(2,1)S(1)} async-done(((bf16[16,184,128]{2,1,0:T(8,128)(2,1)}), bf16[16,184,128]{2,1,0:T(8,128)(2,1)S(1)}, u32[]{:S(2)}, u32[]{:S(2)}) %all-to-all-start.3) | async-done | bytes 753696 | tf_op jit(solution)/shard_map/all_to_all | solution.py:344
  112.9 1.2 return_rows.1
  114.1 3.9 %all-to-all-start.4 = ((bf16[32,24,128]{2,1,0:T(8,128)(2,1)}), bf16[32,24,128]{2,1,0:T(8,128)(2,1)S(1)}, u32[]{:S(2)}, u32[]{:S(2)}) async-start(bf16[32,24,128]{2,1,0:T(8,128)(2,1)} %return_rows.1), calls=%async_computation.4 | async-start | bytes 393216 | tf_op jit(solution)/shard_map/all_to_all | solution.py:344
  118.1 0.1 reduce.5
  118.2 0.1 broadcast_in_dim.34
  118.4 0.2 fusion.12
  118.6 0.1 broadcast_in_dim.36
  118.7 0.2 fusion.10
  118.9 19.0 %all-to-all-done.4 = bf16[32,24,128]{2,1,0:T(8,128)(2,1)S(1)} async-done(((bf16[32,24,128]{2,1,0:T(8,128)(2,1)}), bf16[32,24,128]{2,1,0:T(8,128)(2,1)S(1)}, u32[]{:S(2)}, u32[]{:S(2)}) %all-to-all-start.4) | async-done | bytes 196640 | tf_op jit(solution)/shard_map/all_to_all | solution.py:344
  138.0 0.3 fusion.2
  138.3 0.2 fusion.47
  138.5 10.4 %all_to_all.30 = f32[16,2,48]{2,1,0:T(2,128)S(1)} all-to-all(f32[16,2,48]{2,1,0:T(2,128)S(1)} %broadcast_in_dim.37), channel_id=1, replica_groups=mesh['z'=16,'core'=2,'tp_0'=4,'tp_1'=4] {'tp_0','tp_1'}, dimensions={0} | all-to-all | bytes 12288 | tf_op jit(solution)/shard_map/all_to_all | solution.py:344
  148.9 0.7 multiply_convert_fusion
  (61 shorter events, 1.1 us)
Async XLA Ops:
  0.6 2.6 %copy-start.3 = (f32[48,1,64,64]{3,2,1,0:T(8,128)S(1)}, f32[48,1,64,64]{3,2,1,0:T(8,128)}, u32[]{:S(2)}) copy-start(f32[48,1,64,64]{3,2,1,0:T(8,128)} %param.23) | copy-start | bytes 2359300
  0.7 13.2 %copy-start.11 = (s32[48,4]{0,1:T(4,128)S(1)}, s32[48,4]{0,1:T(4,128)}, u32[]{:S(2)}) copy-start(s32[48,4]{0,1:T(4,128)} %param.31) | copy-start | bytes 2308
  2.8 12.0 %copy-start.8 = (bf16[64,16]{0,1:T(8,128)(2,1)S(1)}, bf16[64,16]{0,1:T(8,128)(2,1)}, u32[]{:S(2)}) copy-start(bf16[64,16]{0,1:T(8,128)(2,1)} %param.40) | copy-start | bytes 6148
  2.8 12.0 %copy-start.9 = (bf16[64,16]{0,1:T(8,128)(2,1)S(1)}, bf16[64,16]{0,1:T(8,128)(2,1)}, u32[]{:S(2)}) copy-start(bf16[64,16]{0,1:T(8,128)(2,1)} %param.39) | copy-start | bytes 6148
  2.8 17.5 %copy-start.1 = (bf16[1024,128]{1,0:T(8,128)(2,1)S(1)}, bf16[1024,128]{1,0:T(8,128)(2,1)}, u32[]{:S(2)}) copy-start(bf16[1024,128]{1,0:T(8,128)(2,1)} %out_weight.1) | copy-start | bytes 786436
  3.2 32.2 %copy-start.5 = (bf16[512,128]{1,0:T(8,128)(2,1)S(1)}, bf16[512,128]{1,0:T(8,128)(2,1)}, u32[]{:S(2)}) copy-start(bf16[512,128]{1,0:T(8,128)(2,1)} %param.38) | copy-start | bytes 393220
  3.5 32.7 %copy-start.6 = (bf16[2048,32]{0,1:T(8,128)(2,1)S(1)}, bf16[2048,32]{0,1:T(8,128)(2,1)}, u32[]{:S(2)}) copy-start(bf16[2048,32]{0,1:T(8,128)(2,1)} %param.36) | copy-start | bytes 393220
  3.5 57.0 %copy-start.2 = (f32[2048]{0:T(1024)S(1)}, f32[2048]{0:T(1024)}, u32[]{:S(2)}) copy-start(f32[2048]{0:T(1024)} %param.30) | copy-start | bytes 24580
  4.6 15.7 %all-to-all-start = ((bf16[16,24,128]{2,1,0:T(8,128)(2,1)}), bf16[16,24,128]{2,1,0:T(8,128)(2,1)S(1)}, u32[]{:S(2)}, u32[]{:S(2)}) async-start(bf16[16,24,128]{2,1,0:T(8,128)(2,1)} %mixed_message.1), calls=%async_computation | async-start | bytes 196608 | tf_op jit(solution)/shard_map/all_to_all | solution.py:344
  14.6 47.4 %copy-start.7 = (s32[768]{0:T(1024)}, s32[768]{0:T(1024)S(1)}, u32[]{:S(2)}) copy-start(s32[768]{0:T(1024)S(1)} %iota.49) | copy-start | bytes 9220
  21.6 36.4 %all-to-all-start.1 = ((bf16[32,32,128]{2,1,0:T(8,128)(2,1)}), bf16[32,32,128]{2,1,0:T(8,128)(2,1)S(1)}, u32[]{:S(2)}, u32[]{:S(2)}) async-start(bf16[32,32,128]{2,1,0:T(8,128)(2,1)} %get-tuple-element.26), calls=%async_computation.1 | async-start | bytes 524288 | tf_op jit(solution)/shard_map/all_to_all | solution.py:344
  58.6 19.7 %collective-permute-start = (bf16[32,8,128]{2,1,0:T(8,128)(2,1)}, bf16[32,8,128]{2,1,0:T(8,128)(2,1)}, u32[]{:S(2)}, u32[]{:S(2)}) collective-permute-start(bf16[32,8,128]{2,1,0:T(8,128)(2,1)} %slice.70), channel_id=1, source_target_pairs={{0,16},{16,0},{1,17},{17,1},{2,18},{18,2},{3,19},{19,3},{4,20},{20... | collective-permute-start | bytes 196616 | tf_op jit(solution)/shard_map/ppermute | solution.py:515
  62.0 23.0 %collective-permute-start.1 = (bf16[2,32,2048]{2,1,0:T(8,128)(2,1)S(1)}, bf16[2,32,2048]{2,1,0:T(8,128)(2,1)S(1)}, u32[]{:S(2)}, u32[]{:S(2)}) collective-permute-start(bf16[2,32,2048]{2,1,0:T(8,128)(2,1)S(1)} %get-tuple-element.30), channel_id=1, source_target_pairs={{0,1},{1,2},{2,3},{3,0},{4,5},{5,6},{6,7},{7,4},{8,9},{9,10},{10,1... | collective-permute-start | bytes 786440 | tf_op jit(solution)/shard_map/ppermute | solution.py:512
  64.6 20.4 %collective-permute-start.2 = (bf16[2,32,2048]{2,1,0:T(8,128)(2,1)S(1)}, bf16[2,32,2048]{2,1,0:T(8,128)(2,1)S(1)}, u32[]{:S(2)}, u32[]{:S(2)}) collective-permute-start(bf16[2,32,2048]{2,1,0:T(8,128)(2,1)S(1)} %get-tuple-element.31), channel_id=1, source_target_pairs={{0,2},{1,3},{2,0},{3,1},{4,6},{5,7},{6,4},{7,5},{8,10},{9,11},{10,... | collective-permute-start | bytes 786440 | tf_op jit(solution)/shard_map/ppermute | solution.py:512
  69.4 15.6 %collective-permute-start.3 = (bf16[2,32,2048]{2,1,0:T(8,128)(2,1)S(1)}, bf16[2,32,2048]{2,1,0:T(8,128)(2,1)S(1)}, u32[]{:S(2)}, u32[]{:S(2)}) collective-permute-start(bf16[2,32,2048]{2,1,0:T(8,128)(2,1)S(1)} %get-tuple-element.32), channel_id=1, source_target_pairs={{0,3},{1,0},{2,1},{3,2},{4,7},{5,4},{6,5},{7,6},{8,11},{9,8},{10,9... | collective-permute-start | bytes 786440 | tf_op jit(solution)/shard_map/ppermute | solution.py:512
  72.9 19.0 %all-to-all-start.2 = ((bf16[16,208,128]{2,1,0:T(8,128)(2,1)}), bf16[16,208,128]{2,1,0:T(8,128)(2,1)S(1)}, u32[]{:S(2)}, u32[]{:S(2)}) async-start(bf16[16,208,128]{2,1,0:T(8,128)(2,1)} %bitcast.15), calls=%async_computation.2 | async-start | bytes 1703936 | tf_op jit(solution)/shard_map/all_to_all | solution.py:344
  78.3 6.6 %copy-start.10 = (bf16[2048]{0:T(1024)(128)(2,1)S(1)}, bf16[2048]{0:T(1024)(128)(2,1)}, u32[]{:S(2)}) copy-start(bf16[2048]{0:T(1024)(128)(2,1)} %param.42) | copy-start | bytes 12292
  91.9 9.1 %slice-start = ((s32[768]{0:T(1024)}), s32[192]{0:T(256)S(1)}, s32[]{:S(2)}) async-start(s32[768]{0:T(1024)} %copy-done.7), calls=%async_computation.6 | async-start | bytes 2048 | tf_op jit(solution)/shard_map/slice | solution.py:554
  94.0 18.9 %all-to-all-start.3 = ((bf16[16,184,128]{2,1,0:T(8,128)(2,1)}), bf16[16,184,128]{2,1,0:T(8,128)(2,1)S(1)}, u32[]{:S(2)}, u32[]{:S(2)}) async-start(bf16[16,184,128]{2,1,0:T(8,128)(2,1)} %get-tuple-element.34), calls=%async_computation.3 | async-start | bytes 1507328 | tf_op jit(solution)/shard_map/all_to_all | solution.py:344
  101.1 11.8 %copy-start = (bf16[4,512,128]{2,1,0:T(8,128)(2,1)S(1)}, bf16[4,512,128]{2,1,0:T(8,128)(2,1)}, u32[]{:S(2)}) copy-start(bf16[4,512,128]{2,1,0:T(8,128)(2,1)} %param.35) | copy-start | bytes 1572868
  104.2 14.0 %copy-start.4 = (bf16[16,64,128]{2,1,0:T(8,128)(2,1)S(1)}, bf16[16,64,128]{2,1,0:T(8,128)(2,1)}, u32[]{:S(2)}) copy-start(bf16[16,64,128]{2,1,0:T(8,128)(2,1)} %pad_bitcast_fusion.1) | copy-start | bytes 786436
  114.1 23.8 %all-to-all-start.4 = ((bf16[32,24,128]{2,1,0:T(8,128)(2,1)}), bf16[32,24,128]{2,1,0:T(8,128)(2,1)S(1)}, u32[]{:S(2)}, u32[]{:S(2)}) async-start(bf16[32,24,128]{2,1,0:T(8,128)(2,1)} %return_rows.1), calls=%async_computation.4 | async-start | bytes 393216 | tf_op jit(solution)/shard_map/all_to_all | solution.py:344
  118.2 19.7 %copy-start.13 = (f32[48,4]{0,1:T(4,128)S(1)}, f32[48,4]{0,1:T(4,128)}, u32[]{:S(2)}) copy-start(f32[48,4]{0,1:T(4,128)} %param.32) | copy-start | bytes 2308
  118.4 30.5 %copy-start.12 = (f32[128]{0:T(128)S(1)}, f32[128]{0:T(128)}, u32[]{:S(2)}) copy-start(f32[128]{0:T(128)} %param.43) | copy-start | bytes 1540

commit v5 on v4

--- a/solution.py
+++ b/solution.py
@@ -16,8 +16,8 @@
 ROPE_BASE = 10000.0
 ACROSS = ((1,), (1,))
 EP = ("z", "core")
-PITCH = 24
 RIDER = 8
+TILE = 4
 FLAT = ((1,), (0,))
 GROUP = 8
 GRANT = 12 * 1024 * 1024
@@ -120,10 +120,9 @@
 
 
 def dispatch_kernel(
-    folded_all, out_weight, table, rider, own_cols, outgoing, exact, short, lhs, rhs
+    folded_all, out_weight, table, side_piece, own_cols, outgoing, exact, short, lhs, rhs
 ):
     parts, half, lanes = folded_all.shape
-    cols = out_weight.shape[1]
     width = lanes // 2
     lane = lax.broadcasted_iota(jnp.int32, (half, lanes), 1)
     for t in range(parts):
@@ -140,15 +139,11 @@
     exact[...] = pre_first
     pre_short = pre_first.astype(short.dtype)
     short[...] = pre_short
-    peers = outgoing.shape[0]
-    rows = f32_dot(table[...], pre_short, FLAT).reshape(peers, PITCH, cols)
-    riders = rider[...].astype(jnp.float32)
-    riders = jnp.broadcast_to(riders[None], (peers // riders.shape[0], *riders.shape))
-    riders = riders.reshape(peers, RIDER, cols)
-    outgoing[...] = jnp.concatenate([rows, riders], 1).astype(outgoing.dtype)
-
-
-def dispatch_rows(folded_all, out_weight, table, rider, own_cols, peers):
+    chosen = jnp.concatenate([pre_first, side_piece[...].astype(jnp.float32)], 0)
+    outgoing[...] = f32_dot(table[...], chosen.astype(short.dtype), FLAT).astype(outgoing.dtype)
+
+
+def dispatch_rows(folded_all, out_weight, table, side_piece, own_cols):
     parts, half, lanes = folded_all.shape
     rows, cols = own_cols.shape
     bf16 = jnp.bfloat16
@@ -158,7 +153,7 @@
         in_specs=[whole] * 5,
         out_specs=[whole] * 3,
         out_shape=[
-            jax.ShapeDtypeStruct((peers, PITCH + RIDER, cols), bf16),
+            jax.ShapeDtypeStruct((table.shape[0], cols), bf16),
             pltpu.VMEM((rows, cols), jnp.float32),
             pltpu.VMEM((rows, cols), bf16),
         ],
@@ -168,7 +163,7 @@
         ],
         name="dispatch_rows",
         compiler_params=pltpu.CompilerParams(vmem_limit_bytes=GRANT),
-    )(*near(folded_all, out_weight, table, rider, own_cols))
+    )(*near(folded_all, out_weight, table, side_piece, own_cols))
 
 
 def pieces_kernel(ready, gate_t, up_t, *refs):
@@ -202,19 +197,13 @@
     )(*near(ready), *far(gate_t, up_t))
 
 
-def mixed_kernel(result, gate_act, message, folded, sent):
+def mixed_kernel(result, gate_act, message):
     value = result[...]
     scale = lax.rsqrt(jnp.mean(value * value, -1, keepdims=True) + GROUP_EPS)
     mixed = value * scale * jax.nn.silu(gate_act[...])
     half = mixed.shape[0] // 2
-    folded[...] = jnp.concatenate([mixed[:half], mixed[half:]], 1).astype(folded.dtype)
-    copies = [
-        pltpu.make_async_copy(folded, message.at[t], sent.at[t]) for t in range(message.shape[0])
-    ]
-    for c in copies:
-        c.start()
-    for c in copies:
-        c.wait()
+    folded = jnp.concatenate([mixed[:half], mixed[half:]], 1)
+    message[...] = jnp.broadcast_to(folded[None], message.shape).astype(message.dtype)
 
 
 def mixed_message(result, gate_act, peers):
@@ -223,30 +212,27 @@
     return pl.pallas_call(
         mixed_kernel,
         in_specs=[whole] * 2,
-        out_specs=pl.BlockSpec(memory_space=pl.ANY),
+        out_specs=whole,
         out_shape=jax.ShapeDtypeStruct((peers, rows // 2, 2 * width), jnp.bfloat16),
-        scratch_shapes=[
-            pltpu.VMEM((rows // 2, 2 * width), jnp.bfloat16),
-            pltpu.SemaphoreType.DMA((peers,)),
-        ],
         name="mixed_message",
         compiler_params=pltpu.CompilerParams(vmem_limit_bytes=GRANT),
     )(*near(result, gate_act))
 
 
-def slot_kernel(arrived, own, regroup, message, rows, sent):
-    experts, row_count, cols = rows.shape
-    peers, pitch, _ = arrived.shape
+def slot_kernel(arrived, own, regroup, message, side, rows, sent):
+    experts, row_count, _ = rows.shape
     slots = row_count - own.shape[0]
-    groups = peers // GROUP
+    span = regroup.shape[1]
+    groups = arrived.shape[0] // span
     count = slots // groups
+    side_count = side.shape[0] // groups
     for j in range(experts):
         rows[j, slots:] = own[...]
     for g in range(groups):
-        block = arrived[g * GROUP : (g + 1) * GROUP].reshape(GROUP * pitch, cols)
-        moved = f32_dot(regroup[...], block, FLAT).astype(rows.dtype)
+        moved = f32_dot(regroup[...], arrived[g * span : (g + 1) * span], FLAT).astype(rows.dtype)
         for j in range(experts):
             rows[j, g * count : (g + 1) * count] = moved[j * count : (j + 1) * count]
+        side[g * side_count : (g + 1) * side_count] = moved[experts * count :]
     copies = [
         pltpu.make_async_copy(rows, message.at[q], sent.at[q]) for q in range(message.shape[0])
     ]
@@ -260,11 +246,16 @@
     cols = own.shape[1]
     whole = pl.BlockSpec(memory_space=pltpu.VMEM)
     rows = slots + own.shape[0]
+    groups = arrived.shape[0] // regroup.shape[1]
+    side_rows = regroup.shape[0] * groups - experts * slots
     return pl.pallas_call(
         slot_kernel,
         in_specs=[whole] * 3,
-        out_specs=pl.BlockSpec(memory_space=pl.ANY),
-        out_shape=jax.ShapeDtypeStruct((copies, experts, rows, cols), jnp.bfloat16),
+        out_specs=[pl.BlockSpec(memory_space=pl.ANY), whole],
+        out_shape=[
+            jax.ShapeDtypeStruct((copies, experts, rows, cols), jnp.bfloat16),
+            pltpu.VMEM((side_rows, cols), jnp.bfloat16),
+        ],
         scratch_shapes=[
             pltpu.VMEM((experts, rows, cols), jnp.bfloat16),
             pltpu.SemaphoreType.DMA((copies,)),
@@ -276,8 +267,8 @@
 
 def return_kernel(hidden_all, down, goes, sent_back):
     parts, experts = down.shape[1], down.shape[0]
-    peers, pitch, cols = sent_back.shape
-    groups = peers // GROUP
+    span = goes.shape[0]
+    groups = sent_back.shape[0] // span
     count = goes.shape[1] // experts
     slots = count * groups
     results = []
@@ -288,19 +279,17 @@
     for g in range(groups):
         block = jnp.concatenate([r[g * count : (g + 1) * count] for r in results], 0)
         back = f32_dot(goes[...], block.astype(sent_back.dtype), FLAT)
-        sent_back[g * GROUP : (g + 1) * GROUP] = back.reshape(GROUP, pitch, cols).astype(
-            sent_back.dtype
-        )
-
-
-def return_rows(hidden_all, down, goes, peers):
+        sent_back[g * span : (g + 1) * span] = back.astype(sent_back.dtype)
+
+
+def return_rows(hidden_all, down, goes, groups):
     cols = down.shape[-1]
     whole = pl.BlockSpec(memory_space=pltpu.VMEM)
     return pl.pallas_call(
         return_kernel,
         in_specs=[whole] * 3,
         out_specs=whole,
-        out_shape=jax.ShapeDtypeStruct((peers, PITCH, cols), jnp.bfloat16),
+        out_shape=jax.ShapeDtypeStruct((goes.shape[0] * groups, cols), jnp.bfloat16),
         name="return_rows",
         compiler_params=pltpu.CompilerParams(vmem_limit_bytes=GRANT),
     )(*near(hidden_all, down, goes))
@@ -480,27 +469,34 @@
     row_of = jnp.arange(seq_rows * top_count, dtype=jnp.int32) // top_count
     earlier = row_of[None, :] < row_of[:, None]
     position = jnp.sum((same & earlier).astype(jnp.int32), 1).reshape(seq_rows, top_count)
-    slot_ids = (
-        (routing // local_experts) * PITCH + (routing % local_experts) * capacity + position
-    )
-    wire_ids = jnp.arange(ep_count * PITCH, dtype=jnp.int32)
-    table = jnp.zeros((ep_count * PITCH, seq_rows), jnp.bool_)
-    for k in range(top_count):
-        table = table | (wire_ids[:, None] == slot_ids[None, :, k])
-    table = table.astype(bf16)
-    slot_hot = (slot_ids.T.reshape(-1)[:, None] == wire_ids[None, :]).astype(bf16)
-
+    back_pitch = local_experts * capacity
+    out_pitch = back_pitch + RIDER
+    place = (routing % local_experts) * capacity + position
+    out_ids = (routing // local_experts) * out_pitch + place
+    back_ids = (routing // local_experts) * back_pitch + place
     side_cols = side_gate.shape[1]
     side_rows = side_gate.shape[0]
     core_count = lax.axis_size("core")
+    wire = jnp.arange(ep_count * out_pitch, dtype=jnp.int32)[:, None]
+    chosen = jnp.arange(seq_rows + side_cols, dtype=jnp.int32)[None, :]
+    rider_row = (wire // out_pitch) % core_count * RIDER + wire % out_pitch - back_pitch
+    table = (wire % out_pitch >= back_pitch) & (chosen == seq_rows + rider_row)
+    padded = jnp.pad(out_ids, ((0, side_cols), (0, 0)), constant_values=-1)
+    for k in range(top_count):
+        table = table | (wire == padded[None, :, k])
+    table = table.astype(bf16)
+    slot_hot = (
+        back_ids.T.reshape(-1)[:, None]
+        == jnp.arange(ep_count * back_pitch, dtype=jnp.int32)[None, :]
+    ).astype(bf16)
+
     side_piece = jnp.concatenate([side_gate.T, side_up.T], 1)
     outgoing, pre_first, pre_short = dispatch_rows(
         folded_all,
         out_weight,
         table,
-        side_piece.reshape(core_count, RIDER, 2 * side_rows),
+        side_piece,
         own_cols,
-        ep_count,
     )
     pieces = list(
         expert_pieces(
@@ -510,8 +506,23 @@
     for d in range(1, class_count):
         steps = [(i, (i + d) % class_count) for i in range(class_count)]
         pieces[d] = lax.ppermute(pieces[d], "tp_1", steps)
-    arrived = swap(outgoing, EP)
-    side_own = arrived[:, PITCH:]
+    arrived = swap(outgoing.reshape(-1, TILE, col_count), EP).reshape(-1, col_count)
+
+    group_slots = local_experts * GROUP * capacity
+    order = jnp.arange(group_slots, dtype=jnp.int32)
+    expert, source = order // (GROUP * capacity), order // capacity % GROUP
+    spot = expert * capacity + order % capacity
+    rider = jnp.arange(GROUP * RIDER, dtype=jnp.int32)
+    came_at = jnp.concatenate(
+        [source * out_pitch + spot, rider // RIDER * out_pitch + back_pitch + rider % RIDER]
+    )
+    regroup = (
+        came_at[:, None] == jnp.arange(GROUP * out_pitch, dtype=jnp.int32)[None, :]
+    ).astype(bf16)
+    to_send, side_own = slot_message(
+        arrived, pre_short, regroup, local_experts, slots, part_count
+    )
+    side_own = side_own.reshape(ep_count, RIDER, col_count)
     side_other = lax.ppermute(side_own, "core", [(0, 1), (1, 0)])
     first_core = lax.axis_index("core") == 0
     side_all = jnp.concatenate(
@@ -522,15 +533,6 @@
         1,
     ).reshape(ep_count, side_cols, 2, side_rows)
     side_all = jnp.transpose(side_all, (2, 1, 0, 3)).reshape(2, side_cols, model_width)
-
-    order = jnp.arange(local_experts * GROUP * capacity, dtype=jnp.int32)
-    expert, source = order // (GROUP * capacity), order // capacity % GROUP
-    spot = expert * capacity + order % capacity
-    came_at = source * (PITCH + RIDER) + spot
-    regroup = (
-        came_at[:, None] == jnp.arange(GROUP * (PITCH + RIDER), dtype=jnp.int32)[None, :]
-    ).astype(bf16)
-    to_send = slot_message(arrived, pre_short, regroup, local_experts, slots, part_count)
     rows_pre = swap(to_send.reshape(tp_count, slots + seq_rows, col_count), TP)
     own_gain = lax.dynamic_slice_in_dim(first_gain, col_start, col_count, 0)
     units = class_count * hidden_cols
@@ -550,10 +552,11 @@
     )
 
     hidden_all = swap(hidden, TP)
-    goes_at = source * PITCH + spot
-    goes = (wire_ids[: GROUP * PITCH, None] == goes_at[None, :]).astype(bf16)
+    goes_at = source * back_pitch + spot
+    goes = (order[:, None] == goes_at[None, :]).astype(bf16)
     down = expert_down.reshape(local_experts, part_count, units, col_count)
-    returned = swap(return_rows(hidden_all, down, goes, ep_count), EP)
+    sent_back = return_rows(hidden_all, down, goes, ep_count // GROUP)
+    returned = swap(sent_back.reshape(-1, TILE, col_count), EP)
 
     local_all = hidden_all[:, slots:]
     left = jnp.arange(units, dtype=jnp.int32)[None, None, :] < units // 2

time: 150 us -> 148 us (0.987)
  local copies, waits for them, and re-layouts: 8.95 us -> 7.05 us
  transfers between devices with their start and end apart: 9 -> 9, of which waited for: 5 -> 6; matrix products, arithmetic and copies ran while one was open for 9% -> 7% of each run, Pallas kernels for 2% -> 1%
where the time goes in v5:
time: 148 us; the launch traced here: 147 us
  waiting for transfers between devices  63 us (43%)
  starting transfers between devices  50 us (34%)
  blocking collectives  10.4 us (7%)
  Pallas kernels  9.94 us (7%)
  local copies, waits for them, and re-layouts  7.05 us (5%)
  other arithmetic  4.83 us (3%)
    all_to_all x5, waiting for transfers between devices, swap(): return lax.all_to_all(parts, axis, 0, 0, tiled=True)  62.6 us
    all_to_all x5, starting transfers between devices, swap(): return lax.all_to_all(parts, axis, 0, 0, tiled=True)  38.4 us
    all_to_all x1, blocking collectives, swap(): return lax.all_to_all(parts, axis, 0, 0, tiled=True)  10.4 us
    ppermute x3, starting transfers between devices, on_device(): pieces[d] = lax.ppermute(pieces[d], 'tp_1', steps)  9.71 us
  transfers between devices with their start and end apart: 9, of which 6 were waited for; matrix products, arithmetic and copies ran while one was open for 7% of the time, Pallas kernels for 1%

profile of v5, /device:TPU:2, one launch (start us, length us, event | category | flops | bytes accessed | tf_op | source)
XLA Modules:
  0.0 147.4 jit_solution(280394671484676607)
XLA Ops:
  0.7 2.1 %project.1 = (f32[48,64]{1,0:T(8,128)S(1)}, f32[48,64]{1,0:T(8,128)S(1)}, f32[48,64]{1,0:T(8,128)S(1)}, f32[48,64]{1,0:T(8,128)S(1)}, f32[48]{0:T(128)S(1)}, /*index=5*/bf16[48,128]{1,0:T(8,128)(2,1)S(1)}) custom-call(bf16[48,2048]{1,0:T(8,128)(2,1)} %tokens.1, s32[48]{0:T(128)} %lengths.1, bf16[64,2048]{1,0:T(8,128)(2,1)} %bitcast.106, ...), custom_call_target="tpu_custom_call" | custom-call | tf_op jit(solution)/shard_map/project/pallas_call | solution.py:102
  2.8 0.2 fusion.32
  3.0 0.2 fusion.39
  3.2 0.3 fusion.66
  3.7 0.8 mixed_message.1
  4.5 9.2 %all-to-all-start = ((bf16[16,24,128]{2,1,0:T(8,128)(2,1)}), bf16[16,24,128]{2,1,0:T(8,128)(2,1)S(1)}, u32[]{:S(2)}, u32[]{:S(2)}) async-start(bf16[16,24,128]{2,1,0:T(8,128)(2,1)} %mixed_message.1), calls=%async_computation | async-start | bytes 196608 | tf_op jit(solution)/shard_map/all_to_all | solution.py:333
  13.9 0.2 convert_reduce_fusion
  14.2 0.1 reshape.473
  14.3 0.2 fusion.28
  14.8 0.3 fusion.10.table
  15.1 5.1 %all-to-all-done.folded_all = bf16[16,24,128]{2,1,0:T(8,128)(2,1)S(1)} async-done(((bf16[16,24,128]{2,1,0:T(8,128)(2,1)}), bf16[16,24,128]{2,1,0:T(8,128)(2,1)S(1)}, u32[]{:S(2)}, u32[]{:S(2)}) %all-to-all-start) | async-done | bytes 98336 | tf_op jit(solution)/shard_map/all_to_all | solution.py:333
  20.2 1.2 dispatch_rows.1
  21.4 13.7 %all-to-all-start.1 = ((bf16[224,4,128]{2,1,0:T(4,128)(2,1)}), bf16[224,4,128]{2,1,0:T(4,128)(2,1)S(1)}, u32[]{:S(2)}, u32[]{:S(2)}) async-start(bf16[224,4,128]{2,1,0:T(4,128)(2,1)} %bitcast.14), calls=%async_computation.1 | async-start | bytes 458752 | tf_op jit(solution)/shard_map/all_to_all | solution.py:333
  35.2 0.7 pad_bitcast_fusion.1
  36.1 20.4 %all-to-all-done.1 = bf16[224,4,128]{2,1,0:T(4,128)(2,1)S(1)} async-done(((bf16[224,4,128]{2,1,0:T(4,128)(2,1)}), bf16[224,4,128]{2,1,0:T(4,128)(2,1)S(1)}, u32[]{:S(2)}, u32[]{:S(2)}) %all-to-all-start.1) | async-done | bytes 229408 | tf_op jit(solution)/shard_map/all_to_all | solution.py:333
  56.5 1.2 slot_message.1
  57.7 1.9 %collective-permute-start = (bf16[32,8,128]{2,1,0:T(8,128)(2,1)S(1)}, bf16[32,8,128]{2,1,0:T(8,128)(2,1)S(1)}, u32[]{:S(2)}, u32[]{:S(2)}) collective-permute-start(bf16[32,8,128]{2,1,0:T(8,128)(2,1)S(1)} %bitcast.99), channel_id=1, source_target_pairs={{0,16},{16,0},{1,17},{17,1},{2,18},{18,2},{3,19},{19,3},{4,20},{20... | collective-permute-start | bytes 196616 | tf_op jit(solution)/shard_map/ppermute | solution.py:526
  59.8 1.3 expert_pieces.1
  61.1 2.6 %collective-permute-start.1 = (bf16[2,32,2048]{2,1,0:T(8,128)(2,1)S(1)}, bf16[2,32,2048]{2,1,0:T(8,128)(2,1)S(1)}, u32[]{:S(2)}, u32[]{:S(2)}) collective-permute-start(bf16[2,32,2048]{2,1,0:T(8,128)(2,1)S(1)} %get-tuple-element.34), channel_id=1, source_target_pairs={{0,1},{1,2},{2,3},{3,0},{4,5},{5,6},{6,7},{7,4},{8,9},{9,10},{10,1... | collective-permute-start | bytes 786440 | tf_op jit(solution)/shard_map/ppermute | solution.py:508
  63.7 4.8 %collective-permute-start.2 = (bf16[2,32,2048]{2,1,0:T(8,128)(2,1)S(1)}, bf16[2,32,2048]{2,1,0:T(8,128)(2,1)S(1)}, u32[]{:S(2)}, u32[]{:S(2)}) collective-permute-start(bf16[2,32,2048]{2,1,0:T(8,128)(2,1)S(1)} %get-tuple-element.35), channel_id=1, source_target_pairs={{0,2},{1,3},{2,0},{3,1},{4,6},{5,7},{6,4},{7,5},{8,10},{9,11},{10,... | collective-permute-start | bytes 786440 | tf_op jit(solution)/shard_map/ppermute | solution.py:508
  68.5 2.4 %collective-permute-start.3 = (bf16[2,32,2048]{2,1,0:T(8,128)(2,1)S(1)}, bf16[2,32,2048]{2,1,0:T(8,128)(2,1)S(1)}, u32[]{:S(2)}, u32[]{:S(2)}) collective-permute-start(bf16[2,32,2048]{2,1,0:T(8,128)(2,1)S(1)} %get-tuple-element.36), channel_id=1, source_target_pairs={{0,3},{1,0},{2,1},{3,2},{4,7},{5,4},{6,5},{7,6},{8,11},{9,8},{10,9... | collective-permute-start | bytes 786440 | tf_op jit(solution)/shard_map/ppermute | solution.py:508
  70.8 5.4 %all-to-all-start.2 = ((bf16[16,208,128]{2,1,0:T(8,128)(2,1)}), bf16[16,208,128]{2,1,0:T(8,128)(2,1)S(1)}, u32[]{:S(2)}, u32[]{:S(2)}) async-start(bf16[16,208,128]{2,1,0:T(8,128)(2,1)} %bitcast.16), calls=%async_computation.2 | async-start | bytes 1703936 | tf_op jit(solution)/shard_map/all_to_all | solution.py:333
  76.3 0.7 pad_maximum_fusion
  77.0 1.0 reshape.479
  78.0 1.1 fusion.65
  79.2 0.2 squeeze.6
  79.4 0.9 bitcast_dynamic-update-slice_fusion
  80.3 1.0 copy.57
  81.4 0.2 squeeze.7
  81.6 0.4 collective-permute-done.3.refs_3_
  82.0 9.0 %all-to-all-done.2.rows_pre = bf16[16,208,128]{2,1,0:T(8,128)(2,1)S(1)} async-done(((bf16[16,208,128]{2,1,0:T(8,128)(2,1)}), bf16[16,208,128]{2,1,0:T(8,128)(2,1)S(1)}, u32[]{:S(2)}, u32[]{:S(2)}) %all-to-all-start.2) | async-done | bytes 852000 | tf_op jit(solution)/shard_map/all_to_all | solution.py:333
  91.0 2.1 %hidden_units.1 = (bf16[16,184,128]{2,1,0:T(8,128)(2,1)}, bf16[48,128]{1,0:T(8,128)(2,1)S(1)}, f32[48,1]{1,0:T(8,128)S(1)}) custom-call(bf16[16,208,128]{2,1,0:T(8,128)(2,1)S(1)} %all-to-all-done.2.rows_pre, f32[16,128]{1,0:T(8,128)S(1)} %bitcast.100, f32[48,128]{1,0:T(8,128)S(1)} %get-tuple-element.31.pre_first, ...), custom_call_target="tpu_custom_call" | custom-call | tf_op jit(solution)/shard_map/hidden_units/pallas_call | solution.py:396
  93.1 6.2 %all-to-all-start.3 = ((bf16[16,184,128]{2,1,0:T(8,128)(2,1)}), bf16[16,184,128]{2,1,0:T(8,128)(2,1)S(1)}, u32[]{:S(2)}, u32[]{:S(2)}) async-start(bf16[16,184,128]{2,1,0:T(8,128)(2,1)} %get-tuple-element.38), calls=%async_computation.3 | async-start | bytes 1507328 | tf_op jit(solution)/shard_map/all_to_all | solution.py:333
  99.4 0.8 pad_bitcast_fusion
  100.2 1.6 %multiply_add_fusion = f32[48,1,64,64]{3,2,1,0:T(8,128)} fusion(f32[48,1,64,64]{3,2,1,0:T(8,128)S(1)} %copy-done.4, f32[48,64]{1,0:T(8,128)S(1)} %get-tuple-element.25, f32[48,64]{1,0:T(8,128)S(1)} %maximum_multiply_fusion.1, f32[]{:T(128)S(6)} %sub.83), kind=kLoop, calls=%fused_computation.2 | loop fusion | flops 589824 | bytes 1597444 | tf_op jit(solution)/shard_map/add | solution.py:325
  101.8 0.1 reduce.5
  101.9 10.2 %all-to-all-done.3.hidden_all = bf16[16,184,128]{2,1,0:T(8,128)(2,1)S(1)} async-done(((bf16[16,184,128]{2,1,0:T(8,128)(2,1)}), bf16[16,184,128]{2,1,0:T(8,128)(2,1)S(1)}, u32[]{:S(2)}, u32[]{:S(2)}) %all-to-all-start.3) | async-done | bytes 753696 | tf_op jit(solution)/shard_map/all_to_all | solution.py:333
  112.2 1.2 return_rows.1
  113.3 3.9 %all-to-all-start.4 = ((bf16[160,4,128]{2,1,0:T(4,128)(2,1)}), bf16[160,4,128]{2,1,0:T(4,128)(2,1)S(1)}, u32[]{:S(2)}, u32[]{:S(2)}) async-start(bf16[160,4,128]{2,1,0:T(4,128)(2,1)} %bitcast.35), calls=%async_computation.4 | async-start | bytes 327680 | tf_op jit(solution)/shard_map/all_to_all | solution.py:333
  117.3 0.1 broadcast_in_dim.34
  117.4 0.2 fusion.15
  117.6 0.1 broadcast_in_dim.36
  117.7 0.2 fusion.13
  118.0 17.8 %all-to-all-done.4 = bf16[160,4,128]{2,1,0:T(4,128)(2,1)S(1)} async-done(((bf16[160,4,128]{2,1,0:T(4,128)(2,1)}), bf16[160,4,128]{2,1,0:T(4,128)(2,1)S(1)}, u32[]{:S(2)}, u32[]{:S(2)}) %all-to-all-start.4) | async-done | bytes 163872 | tf_op jit(solution)/shard_map/all_to_all | solution.py:333
  135.8 0.3 fusion.2
  136.0 0.2 fusion.63
  136.3 10.4 %all_to_all.30 = f32[16,2,48]{2,1,0:T(2,128)S(1)} all-to-all(f32[16,2,48]{2,1,0:T(2,128)S(1)} %broadcast_in_dim.37), channel_id=1, replica_groups=mesh['z'=16,'core'=2,'tp_0'=4,'tp_1'=4] {'tp_0','tp_1'}, dimensions={0} | all-to-all | bytes 12288 | tf_op jit(solution)/shard_map/all_to_all | solution.py:333
  146.7 0.7 multiply_convert_fusion
  (66 shorter events, 1.2 us)
Async XLA Ops:
  0.6 2.6 %copy-start.3 = (f32[48,1,64,64]{3,2,1,0:T(8,128)S(1)}, f32[48,1,64,64]{3,2,1,0:T(8,128)}, u32[]{:S(2)}) copy-start(f32[48,1,64,64]{3,2,1,0:T(8,128)} %param.23) | copy-start | bytes 2359300
  0.7 13.1 %copy-start.13 = (s32[48,4]{0,1:T(4,128)S(1)}, s32[48,4]{0,1:T(4,128)}, u32[]{:S(2)}) copy-start(s32[48,4]{0,1:T(4,128)} %param.31) | copy-start | bytes 2308
  2.8 11.8 %copy-start.10 = (bf16[64,16]{0,1:T(8,128)(2,1)S(1)}, bf16[64,16]{0,1:T(8,128)(2,1)}, u32[]{:S(2)}) copy-start(bf16[64,16]{0,1:T(8,128)(2,1)} %param.40) | copy-start | bytes 6148
  2.8 11.8 %copy-start.11 = (bf16[64,16]{0,1:T(8,128)(2,1)S(1)}, bf16[64,16]{0,1:T(8,128)(2,1)}, u32[]{:S(2)}) copy-start(bf16[64,16]{0,1:T(8,128)(2,1)} %param.39) | copy-start | bytes 6148
  2.8 17.4 %copy-start.1 = (bf16[1024,128]{1,0:T(8,128)(2,1)S(1)}, bf16[1024,128]{1,0:T(8,128)(2,1)}, u32[]{:S(2)}) copy-start(bf16[1024,128]{1,0:T(8,128)(2,1)} %out_weight.1) | copy-start | bytes 786436
  3.2 32.0 %copy-start.7 = (bf16[512,128]{1,0:T(8,128)(2,1)S(1)}, bf16[512,128]{1,0:T(8,128)(2,1)}, u32[]{:S(2)}) copy-start(bf16[512,128]{1,0:T(8,128)(2,1)} %param.38) | copy-start | bytes 393220
  3.5 32.5 %copy-start.8 = (bf16[2048,32]{0,1:T(8,128)(2,1)S(1)}, bf16[2048,32]{0,1:T(8,128)(2,1)}, u32[]{:S(2)}) copy-start(bf16[2048,32]{0,1:T(8,128)(2,1)} %param.36) | copy-start | bytes 393220
  3.7 56.0 %copy-start.2 = (f32[2048]{0:T(1024)S(1)}, f32[2048]{0:T(1024)}, u32[]{:S(2)}) copy-start(f32[2048]{0:T(1024)} %param.30) | copy-start | bytes 24580
  4.5 15.7 %all-to-all-start = ((bf16[16,24,128]{2,1,0:T(8,128)(2,1)}), bf16[16,24,128]{2,1,0:T(8,128)(2,1)S(1)}, u32[]{:S(2)}, u32[]{:S(2)}) async-start(bf16[16,24,128]{2,1,0:T(8,128)(2,1)} %mixed_message.1), calls=%async_computation | async-start | bytes 196608 | tf_op jit(solution)/shard_map/all_to_all | solution.py:333
  21.4 35.1 %all-to-all-start.1 = ((bf16[224,4,128]{2,1,0:T(4,128)(2,1)}), bf16[224,4,128]{2,1,0:T(4,128)(2,1)S(1)}, u32[]{:S(2)}, u32[]{:S(2)}) async-start(bf16[224,4,128]{2,1,0:T(4,128)(2,1)} %bitcast.14), calls=%async_computation.1 | async-start | bytes 458752 | tf_op jit(solution)/shard_map/all_to_all | solution.py:333
  57.7 18.6 %collective-permute-start = (bf16[32,8,128]{2,1,0:T(8,128)(2,1)S(1)}, bf16[32,8,128]{2,1,0:T(8,128)(2,1)S(1)}, u32[]{:S(2)}, u32[]{:S(2)}) collective-permute-start(bf16[32,8,128]{2,1,0:T(8,128)(2,1)S(1)} %bitcast.99), channel_id=1, source_target_pairs={{0,16},{16,0},{1,17},{17,1},{2,18},{18,2},{3,19},{19,3},{4,20},{20... | collective-permute-start | bytes 196616 | tf_op jit(solution)/shard_map/ppermute | solution.py:526
  61.1 20.5 %collective-permute-start.1 = (bf16[2,32,2048]{2,1,0:T(8,128)(2,1)S(1)}, bf16[2,32,2048]{2,1,0:T(8,128)(2,1)S(1)}, u32[]{:S(2)}, u32[]{:S(2)}) collective-permute-start(bf16[2,32,2048]{2,1,0:T(8,128)(2,1)S(1)} %get-tuple-element.34), channel_id=1, source_target_pairs={{0,1},{1,2},{2,3},{3,0},{4,5},{5,6},{6,7},{7,4},{8,9},{9,10},{10,1... | collective-permute-start | bytes 786440 | tf_op jit(solution)/shard_map/ppermute | solution.py:508
  63.7 17.9 %collective-permute-start.2 = (bf16[2,32,2048]{2,1,0:T(8,128)(2,1)S(1)}, bf16[2,32,2048]{2,1,0:T(8,128)(2,1)S(1)}, u32[]{:S(2)}, u32[]{:S(2)}) collective-permute-start(bf16[2,32,2048]{2,1,0:T(8,128)(2,1)S(1)} %get-tuple-element.35), channel_id=1, source_target_pairs={{0,2},{1,3},{2,0},{3,1},{4,6},{5,7},{6,4},{7,5},{8,10},{9,11},{10,... | collective-permute-start | bytes 786440 | tf_op jit(solution)/shard_map/ppermute | solution.py:508
  68.5 13.5 %collective-permute-start.3 = (bf16[2,32,2048]{2,1,0:T(8,128)(2,1)S(1)}, bf16[2,32,2048]{2,1,0:T(8,128)(2,1)S(1)}, u32[]{:S(2)}, u32[]{:S(2)}) collective-permute-start(bf16[2,32,2048]{2,1,0:T(8,128)(2,1)S(1)} %get-tuple-element.36), channel_id=1, source_target_pairs={{0,3},{1,0},{2,1},{3,2},{4,7},{5,4},{6,5},{7,6},{8,11},{9,8},{10,9... | collective-permute-start | bytes 786440 | tf_op jit(solution)/shard_map/ppermute | solution.py:508
  70.8 20.2 %all-to-all-start.2 = ((bf16[16,208,128]{2,1,0:T(8,128)(2,1)}), bf16[16,208,128]{2,1,0:T(8,128)(2,1)S(1)}, u32[]{:S(2)}, u32[]{:S(2)}) async-start(bf16[16,208,128]{2,1,0:T(8,128)(2,1)} %bitcast.16), calls=%async_computation.2 | async-start | bytes 1703936 | tf_op jit(solution)/shard_map/all_to_all | solution.py:333
  77.0 4.6 %copy-start.12 = (bf16[2048]{0:T(1024)(128)(2,1)S(1)}, bf16[2048]{0:T(1024)(128)(2,1)}, u32[]{:S(2)}) copy-start(bf16[2048]{0:T(1024)(128)(2,1)} %param.42) | copy-start | bytes 12292
  91.0 8.3 %copy-start.9 = (bf16[256,128]{1,0:T(8,128)(2,1)S(1)}, bf16[256,128]{1,0:T(8,128)(2,1)}, u32[]{:S(2)}) copy-start(bf16[256,128]{1,0:T(8,128)(2,1)} %param.41) | copy-start | bytes 196612
  93.1 7.0 %copy-start.4 = (f32[48,1,64,64]{3,2,1,0:T(8,128)S(1)}, f32[48,1,64,64]{3,2,1,0:T(8,128)}, u32[]{:S(2)}) copy-start(f32[48,1,64,64]{3,2,1,0:T(8,128)} %param.23) | copy-start | bytes 2359300
  93.1 19.0 %all-to-all-start.3 = ((bf16[16,184,128]{2,1,0:T(8,128)(2,1)}), bf16[16,184,128]{2,1,0:T(8,128)(2,1)S(1)}, u32[]{:S(2)}, u32[]{:S(2)}) async-start(bf16[16,184,128]{2,1,0:T(8,128)(2,1)} %get-tuple-element.38), calls=%async_computation.3 | async-start | bytes 1507328 | tf_op jit(solution)/shard_map/all_to_all | solution.py:333
  100.2 12.0 %copy-start = (bf16[4,512,128]{2,1,0:T(8,128)(2,1)S(1)}, bf16[4,512,128]{2,1,0:T(8,128)(2,1)}, u32[]{:S(2)}) copy-start(bf16[4,512,128]{2,1,0:T(8,128)(2,1)} %param.35) | copy-start | bytes 1572868
  101.8 15.4 %copy-start.6 = (bf16[16,64,128]{2,1,0:T(8,128)(2,1)S(1)}, bf16[16,64,128]{2,1,0:T(8,128)(2,1)}, u32[]{:S(2)}) copy-start(bf16[16,64,128]{2,1,0:T(8,128)(2,1)} %pad_bitcast_fusion.1) | copy-start | bytes 786436
  112.2 5.4 %copy-start.5 = (bf16[16,64,128]{2,1,0:T(8,128)(2,1)S(1)}, bf16[16,64,128]{2,1,0:T(8,128)(2,1)}, u32[]{:S(2)}) copy-start(bf16[16,64,128]{2,1,0:T(8,128)(2,1)} %pad_bitcast_fusion) | copy-start | bytes 786436
  113.3 22.4 %all-to-all-start.4 = ((bf16[160,4,128]{2,1,0:T(4,128)(2,1)}), bf16[160,4,128]{2,1,0:T(4,128)(2,1)S(1)}, u32[]{:S(2)}, u32[]{:S(2)}) async-start(bf16[160,4,128]{2,1,0:T(4,128)(2,1)} %bitcast.35), calls=%async_computation.4 | async-start | bytes 327680 | tf_op jit(solution)/shard_map/all_to_all | solution.py:333
  117.2 18.5 %copy-start.15 = (f32[48,4]{0,1:T(4,128)S(1)}, f32[48,4]{0,1:T(4,128)}, u32[]{:S(2)}) copy-start(f32[48,4]{0,1:T(4,128)} %param.32) | copy-start | bytes 2308
  117.4 29.3 %copy-start.14 = (f32[128]{0:T(128)S(1)}, f32[128]{0:T(128)}, u32[]{:S(2)}) copy-start(f32[128]{0:T(128)} %param.43) | copy-start | bytes 1540

commit v6 on v5

--- a/solution.py
+++ b/solution.py
@@ -342,8 +342,33 @@
     return lax.dot_general(a, b, (dims, ((), ())), preferred_element_type=jnp.float32)
 
 
-def hidden_kernel(rows_pre, gains, pre_first, own_gain, local_weights, *refs):
-    pieces, (message, normed_cols, switch, normed, hidden, gate_up, sent) = refs[:-7], refs[-7:]
+def ordered_kernel(*refs):
+    pieces, gate_up = refs[:-1], refs[-1]
+    units = gate_up.shape[0] // 2
+    lane = lax.axis_index("tp_1")
+    for d, piece in enumerate(pieces):
+        span = piece.shape[1]
+        start = (lane + len(pieces) - d) % len(pieces) * span
+        for i in range(2):
+            gate_up[pl.ds(pl.multiple_of(i * units + start, span), span)] = piece[i]
+
+
+def ordered(pieces):
+    two, span, width = pieces[0].shape
+    whole = pl.BlockSpec(memory_space=pltpu.VMEM)
+    return pl.pallas_call(
+        ordered_kernel,
+        in_specs=[whole] * len(pieces),
+        out_specs=whole,
+        out_shape=pltpu.VMEM((two * span * len(pieces), width), pieces[0].dtype),
+        name="ordered",
+        compiler_params=pltpu.CompilerParams(vmem_limit_bytes=GRANT),
+    )(*near(*pieces))
+
+
+def hidden_kernel(
+    rows_pre, gains, pre_first, own_gain, local_weights, gate_up, message, normed_cols, switch, normed
+):
     parts, row_count, cols = rows_pre.shape
     own_rows = pre_first.shape[0]
     slots = row_count - own_rows
@@ -364,53 +389,39 @@
         normed_cols.dtype
     )
     units = gate_up.shape[0] // 2
-    lane = lax.axis_index("tp_1")
-    for d, piece in enumerate(pieces):
-        span = piece.shape[1]
-        start = (lane + len(pieces) - d) % len(pieces) * span
-        for i in range(2):
-            gate_up[pl.ds(pl.multiple_of(i * units + start, span), span)] = piece[i]
     both = f32_dot(normed[:slots], gate_up[...], ACROSS)
-    hidden[:slots] = (jax.nn.silu(both[:, :units]) * both[:, units:]).astype(hidden.dtype)
+    routed = (jax.nn.silu(both[:, :units]) * both[:, units:]).astype(message.dtype)
+    for t in range(message.shape[0]):
+        message[t, :slots] = routed
     local = f32_dot(normed[slots:], local_weights[...], ACROSS)
     cut = (local.shape[1] - RIDER) // 2
     mine = jax.nn.silu(local[:, :cut]) * local[:, cut : 2 * cut]
     mine = jnp.concatenate([mine, jnp.zeros((own_rows, units // 2 - cut), jnp.float32)], 1)
     half = own_rows // 2
-    hidden[slots:] = jnp.concatenate([mine[:half], mine[half:]], 1).astype(hidden.dtype)
-    copies = [
-        pltpu.make_async_copy(hidden, message.at[t], sent.at[t]) for t in range(message.shape[0])
-    ]
-    for c in copies:
-        c.start()
+    packed = jnp.concatenate([mine[:half], mine[half:]], 1).astype(message.dtype)
+    for t in range(message.shape[0]):
+        message[t, slots:] = packed
     switch[...] = jax.nn.sigmoid(local[:, 2 * cut : 2 * cut + 1])
-    for c in copies:
-        c.wait()
-
-
-def hidden_units(rows_pre, gains, pre_first, own_gain, local_weights, pieces):
+
+
+def hidden_units(rows_pre, gains, pre_first, own_gain, local_weights, gate_up):
     parts, row_count, cols = rows_pre.shape
-    units = sum(p.shape[1] for p in pieces)
+    units = gate_up.shape[0] // 2
     own_rows = pre_first.shape[0]
     whole = pl.BlockSpec(memory_space=pltpu.VMEM)
     return pl.pallas_call(
         hidden_kernel,
-        in_specs=[whole] * (5 + len(pieces)),
-        out_specs=[pl.BlockSpec(memory_space=pl.ANY), whole, whole],
+        in_specs=[whole] * 6,
+        out_specs=[whole] * 3,
         out_shape=[
             jax.ShapeDtypeStruct((parts, row_count - own_rows // 2, units), jnp.bfloat16),
             pltpu.VMEM((own_rows, cols), jnp.bfloat16),
             pltpu.VMEM((own_rows, 1), jnp.float32),
         ],
-        scratch_shapes=[
-            pltpu.VMEM((row_count, parts * cols), jnp.bfloat16),
-            pltpu.VMEM((row_count - own_rows // 2, units), jnp.bfloat16),
-            pltpu.VMEM((2 * units, parts * cols), jnp.bfloat16),
-            pltpu.SemaphoreType.DMA((parts,)),
-        ],
+        scratch_shapes=[pltpu.VMEM((row_count, parts * cols), jnp.bfloat16)],
         name="hidden_units",
         compiler_params=pltpu.CompilerParams(vmem_limit_bytes=GRANT),
-    )(*near(rows_pre, gains, pre_first, own_gain, local_weights, *pieces))
+    )(*near(rows_pre, gains, pre_first, own_gain, local_weights, gate_up))
 
 
 def on_device(
@@ -503,7 +514,7 @@
             pre_short, jnp.swapaxes(expert_gate, 1, 2), jnp.swapaxes(expert_up, 1, 2)
         )
     )
-    for d in range(1, class_count):
+    for d in sorted(range(1, class_count), key=lambda d: -min(d, class_count - d)):
         steps = [(i, (i + d) % class_count) for i in range(class_count)]
         pieces[d] = lax.ppermute(pieces[d], "tp_1", steps)
     arrived = swap(outgoing.reshape(-1, TILE, col_count), EP).reshape(-1, col_count)
@@ -548,7 +559,7 @@
         0,
     )
     hidden, normed_cols, switch = hidden_units(
-        rows_pre, first_gain.reshape(tp_count, col_count), pre_first, own_gain[None], local_weights, pieces
+        rows_pre, first_gain.reshape(tp_count, col_count), pre_first, own_gain[None], local_weights, ordered(pieces)
     )
 
     hidden_all = swap(hidden, TP)

time: 148 us -> 139 us (0.939)
  waiting for transfers between devices: 63 us -> 56 us
  local copies, waits for them, and re-layouts: 7.05 us -> 2.16 us
  starting transfers between devices: 50 us -> 52.1 us
    all_to_all x5, waiting for transfers between devices: 62.6 us -> 56 us  [swap(): return lax.all_to_all(parts, axis, 0, 0, tiled=True)]
    all_to_all x5, starting transfers between devices: 38.4 us -> 40.5 us  [swap(): return lax.all_to_all(parts, axis, 0, 0, tiled=True)]
    slice x2, local copies, waits for them, and re-layouts: 2.12 us -> 0.45 us  [on_device(): side_all[1]]
  transfers between devices with their start and end apart: 9 -> 9, of which waited for: 6 -> 5; matrix products, arithmetic and copies ran while one was open for 7% -> 5% of each run, Pallas kernels for 1% -> 2%
where the time goes in v6:
time: 139 us
  waiting for transfers between devices  56 us (40%)
  starting transfers between devices  52.1 us (37%)
  blocking collectives  10.7 us (8%)
  Pallas kernels  9.88 us (7%)
  other arithmetic  5.63 us (4%)
  local copies, waits for them, and re-layouts  2.16 us (2%)
    all_to_all x5, waiting for transfers between devices, swap(): return lax.all_to_all(parts, axis, 0, 0, tiled=True)  56 us
    all_to_all x5, starting transfers between devices, swap(): return lax.all_to_all(parts, axis, 0, 0, tiled=True)  40.5 us
    all_to_all x1, blocking collectives, swap(): return lax.all_to_all(parts, axis, 0, 0, tiled=True)  10.7 us
    ppermute x3, starting transfers between devices, on_device(): pieces[d] = lax.ppermute(pieces[d], 'tp_1', steps)  9.71 us
    add x1, other arithmetic, retain(): decays[None, :, None, None] * retention_state  3.09 us
  transfers between devices with their start and end apart: 9, of which 5 were waited for; matrix products, arithmetic and copies ran while one was open for 5% of the time, Pallas kernels for 2%

profile of v6, /device:TPU:2, one launch (start us, length us, event | category | flops | bytes accessed | tf_op | source)
XLA Modules:
  0.0 138.7 jit_solution(2404209069325071158)
XLA Ops:
  0.7 2.1 %project.1 = (f32[48,64]{1,0:T(8,128)S(1)}, f32[48,64]{1,0:T(8,128)S(1)}, f32[48,64]{1,0:T(8,128)S(1)}, f32[48,64]{1,0:T(8,128)S(1)}, f32[48]{0:T(128)S(1)}, /*index=5*/bf16[48,128]{1,0:T(8,128)(2,1)S(1)}) custom-call(bf16[48,2048]{1,0:T(8,128)(2,1)} %tokens.1, s32[48]{0:T(128)} %lengths.1, bf16[64,2048]{1,0:T(8,128)(2,1)} %bitcast.106, ...), custom_call_target="tpu_custom_call" | custom-call | tf_op jit(solution)/shard_map/project/pallas_call | solution.py:102
  2.8 0.2 fusion.32
  3.0 0.2 fusion.39
  3.2 0.3 fusion.66
  3.7 0.8 mixed_message.1
  4.5 9.2 %all-to-all-start = ((bf16[16,24,128]{2,1,0:T(8,128)(2,1)}), bf16[16,24,128]{2,1,0:T(8,128)(2,1)S(1)}, u32[]{:S(2)}, u32[]{:S(2)}) async-start(bf16[16,24,128]{2,1,0:T(8,128)(2,1)} %mixed_message.1), calls=%async_computation | async-start | bytes 196608 | tf_op jit(solution)/shard_map/all_to_all | solution.py:333
  13.7 0.1 copy.51
  13.8 0.1 eq.161
  13.9 0.2 convert_reduce_fusion
  14.2 0.1 reshape.473
  14.3 0.2 fusion.28
  14.7 0.3 fusion.10.table
  15.1 5.1 %all-to-all-done.folded_all = bf16[16,24,128]{2,1,0:T(8,128)(2,1)S(1)} async-done(((bf16[16,24,128]{2,1,0:T(8,128)(2,1)}), bf16[16,24,128]{2,1,0:T(8,128)(2,1)S(1)}, u32[]{:S(2)}, u32[]{:S(2)}) %all-to-all-start) | async-done | bytes 98336 | tf_op jit(solution)/shard_map/all_to_all | solution.py:333
  20.2 1.2 dispatch_rows.1
  21.4 13.7 %all-to-all-start.1 = ((bf16[224,4,128]{2,1,0:T(4,128)(2,1)}), bf16[224,4,128]{2,1,0:T(4,128)(2,1)S(1)}, u32[]{:S(2)}, u32[]{:S(2)}) async-start(bf16[224,4,128]{2,1,0:T(4,128)(2,1)} %bitcast.14), calls=%async_computation.1 | async-start | bytes 458752 | tf_op jit(solution)/shard_map/all_to_all | solution.py:333
  35.1 0.1 fusion.12.regroup
  35.3 1.4 expert_pieces.1
  36.6 2.6 %collective-permute-start.1 = (bf16[2,32,2048]{2,1,0:T(8,128)(2,1)S(1)}, bf16[2,32,2048]{2,1,0:T(8,128)(2,1)S(1)}, u32[]{:S(2)}, u32[]{:S(2)}) collective-permute-start(bf16[2,32,2048]{2,1,0:T(8,128)(2,1)S(1)} %get-tuple-element.34), channel_id=1, source_target_pairs={{0,1},{1,2},{2,3},{3,0},{4,5},{5,6},{6,7},{7,4},{8,9},{9,10},{10,1... | collective-permute-start | bytes 786440 | tf_op jit(solution)/shard_map/ppermute | solution.py:519
  39.2 4.8 %collective-permute-start.2 = (bf16[2,32,2048]{2,1,0:T(8,128)(2,1)S(1)}, bf16[2,32,2048]{2,1,0:T(8,128)(2,1)S(1)}, u32[]{:S(2)}, u32[]{:S(2)}) collective-permute-start(bf16[2,32,2048]{2,1,0:T(8,128)(2,1)S(1)} %get-tuple-element.35), channel_id=1, source_target_pairs={{0,2},{1,3},{2,0},{3,1},{4,6},{5,7},{6,4},{7,5},{8,10},{9,11},{10,... | collective-permute-start | bytes 786440 | tf_op jit(solution)/shard_map/ppermute | solution.py:519
  44.0 2.4 %collective-permute-start.3 = (bf16[2,32,2048]{2,1,0:T(8,128)(2,1)S(1)}, bf16[2,32,2048]{2,1,0:T(8,128)(2,1)S(1)}, u32[]{:S(2)}, u32[]{:S(2)}) collective-permute-start(bf16[2,32,2048]{2,1,0:T(8,128)(2,1)S(1)} %get-tuple-element.36), channel_id=1, source_target_pairs={{0,3},{1,0},{2,1},{3,2},{4,7},{5,4},{6,5},{7,6},{8,11},{9,8},{10,9... | collective-permute-start | bytes 786440 | tf_op jit(solution)/shard_map/ppermute | solution.py:519
  46.5 10.0 %all-to-all-done.1 = bf16[224,4,128]{2,1,0:T(4,128)(2,1)S(1)} async-done(((bf16[224,4,128]{2,1,0:T(4,128)(2,1)}), bf16[224,4,128]{2,1,0:T(4,128)(2,1)S(1)}, u32[]{:S(2)}, u32[]{:S(2)}) %all-to-all-start.1) | async-done | bytes 229408 | tf_op jit(solution)/shard_map/all_to_all | solution.py:333
  56.5 1.2 slot_message.1
  57.7 1.9 %collective-permute-start = (bf16[32,8,128]{2,1,0:T(8,128)(2,1)S(1)}, bf16[32,8,128]{2,1,0:T(8,128)(2,1)S(1)}, u32[]{:S(2)}, u32[]{:S(2)}) collective-permute-start(bf16[32,8,128]{2,1,0:T(8,128)(2,1)S(1)} %bitcast.99), channel_id=1, source_target_pairs={{0,16},{16,0},{1,17},{17,1},{2,18},{18,2},{3,19},{19,3},{4,20},{20... | collective-permute-start | bytes 196616 | tf_op jit(solution)/shard_map/ppermute | solution.py:537
  59.8 0.1 ordered.1.gate_up
  59.9 4.9 %all-to-all-start.2 = ((bf16[16,208,128]{2,1,0:T(8,128)(2,1)}), bf16[16,208,128]{2,1,0:T(8,128)(2,1)S(1)}, u32[]{:S(2)}, u32[]{:S(2)}) async-start(bf16[16,208,128]{2,1,0:T(8,128)(2,1)} %bitcast.16), calls=%async_computation.2 | async-start | bytes 1703936 | tf_op jit(solution)/shard_map/all_to_all | solution.py:333
  64.8 0.1 reshape.479
  65.0 0.4 fusion.65
  65.3 0.1 copy.56
  65.4 0.2 squeeze.6
  65.7 0.1 copy.57
  65.8 0.2 squeeze.7
  66.0 13.5 %all-to-all-done.2.rows_pre = bf16[16,208,128]{2,1,0:T(8,128)(2,1)S(1)} async-done(((bf16[16,208,128]{2,1,0:T(8,128)(2,1)}), bf16[16,208,128]{2,1,0:T(8,128)(2,1)S(1)}, u32[]{:S(2)}, u32[]{:S(2)}) %all-to-all-start.2) | async-done | bytes 852000 | tf_op jit(solution)/shard_map/all_to_all | solution.py:333
  79.5 1.9 %hidden_units.1 = (bf16[16,184,128]{2,1,0:T(8,128)(2,1)}, bf16[48,128]{1,0:T(8,128)(2,1)S(1)}, f32[48,1]{1,0:T(8,128)S(1)}) custom-call(bf16[16,208,128]{2,1,0:T(8,128)(2,1)S(1)} %all-to-all-done.2.rows_pre, f32[16,128]{1,0:T(8,128)S(1)} %bitcast.100, f32[48,128]{1,0:T(8,128)S(1)} %get-tuple-element.31.pre_first, ...), custom_call_target="tpu_custom_call" | custom-call | tf_op jit(solution)/shard_map/hidden_units/pallas_call | solution.py:412
  81.4 5.3 %all-to-all-start.3 = ((bf16[16,184,128]{2,1,0:T(8,128)(2,1)}), bf16[16,184,128]{2,1,0:T(8,128)(2,1)S(1)}, u32[]{:S(2)}, u32[]{:S(2)}) async-start(bf16[16,184,128]{2,1,0:T(8,128)(2,1)} %get-tuple-element.38), calls=%async_computation.3 | async-start | bytes 1507328 | tf_op jit(solution)/shard_map/all_to_all | solution.py:333
  86.8 3.1 %multiply_add_fusion = f32[48,1,64,64]{3,2,1,0:T(8,128)} fusion(f32[48,1,64,64]{3,2,1,0:T(8,128)} %param.23, f32[48,64]{1,0:T(8,128)S(1)} %get-tuple-element.25, f32[48,64]{1,0:T(8,128)S(1)} %maximum_multiply_fusion.1, f32[]{:T(128)S(6)} %sub.83), kind=kLoop, calls=%fused_computation.2 | loop fusion | flops 589824 | bytes 1597444 | tf_op jit(solution)/shard_map/add | solution.py:325
  89.9 0.1 reduce.5
  90.0 9.5 %all-to-all-done.3.hidden_all = bf16[16,184,128]{2,1,0:T(8,128)(2,1)S(1)} async-done(((bf16[16,184,128]{2,1,0:T(8,128)(2,1)}), bf16[16,184,128]{2,1,0:T(8,128)(2,1)S(1)}, u32[]{:S(2)}, u32[]{:S(2)}) %all-to-all-start.3) | async-done | bytes 753696 | tf_op jit(solution)/shard_map/all_to_all | solution.py:333
  99.5 1.2 return_rows.1
  100.7 7.5 %all-to-all-start.4 = ((bf16[160,4,128]{2,1,0:T(4,128)(2,1)}), bf16[160,4,128]{2,1,0:T(4,128)(2,1)S(1)}, u32[]{:S(2)}, u32[]{:S(2)}) async-start(bf16[160,4,128]{2,1,0:T(4,128)(2,1)} %bitcast.35), calls=%async_computation.4 | async-start | bytes 327680 | tf_op jit(solution)/shard_map/all_to_all | solution.py:333
  108.2 0.1 broadcast_in_dim.34
  108.3 0.2 fusion.15
  108.6 0.1 broadcast_in_dim.36
  108.7 0.2 fusion.13
  108.9 17.9 %all-to-all-done.4 = bf16[160,4,128]{2,1,0:T(4,128)(2,1)S(1)} async-done(((bf16[160,4,128]{2,1,0:T(4,128)(2,1)}), bf16[160,4,128]{2,1,0:T(4,128)(2,1)S(1)}, u32[]{:S(2)}, u32[]{:S(2)}) %all-to-all-start.4) | async-done | bytes 163872 | tf_op jit(solution)/shard_map/all_to_all | solution.py:333
  126.8 0.3 fusion.2
  127.1 0.2 fusion.63
  127.3 10.7 %all_to_all.30 = f32[16,2,48]{2,1,0:T(2,128)S(1)} all-to-all(f32[16,2,48]{2,1,0:T(2,128)S(1)} %broadcast_in_dim.37), channel_id=1, replica_groups=mesh['z'=16,'core'=2,'tp_0'=4,'tp_1'=4] {'tp_0','tp_1'}, dimensions={0} | all-to-all | bytes 12288 | tf_op jit(solution)/shard_map/all_to_all | solution.py:333
  138.0 0.7 multiply_convert_fusion
  (63 shorter events, 0.9 us)
Async XLA Ops:
  0.6 2.6 %copy-start.3 = (f32[48,1,64,64]{3,2,1,0:T(8,128)S(1)}, f32[48,1,64,64]{3,2,1,0:T(8,128)}, u32[]{:S(2)}) copy-start(f32[48,1,64,64]{3,2,1,0:T(8,128)} %param.23) | copy-start | bytes 2359300
  0.7 13.1 %copy-start.11 = (s32[48,4]{0,1:T(4,128)S(1)}, s32[48,4]{0,1:T(4,128)}, u32[]{:S(2)}) copy-start(s32[48,4]{0,1:T(4,128)} %param.31) | copy-start | bytes 2308
  2.8 11.7 %copy-start.8 = (bf16[64,16]{0,1:T(8,128)(2,1)S(1)}, bf16[64,16]{0,1:T(8,128)(2,1)}, u32[]{:S(2)}) copy-start(bf16[64,16]{0,1:T(8,128)(2,1)} %param.40) | copy-start | bytes 6148
  2.8 11.7 %copy-start.9 = (bf16[64,16]{0,1:T(8,128)(2,1)S(1)}, bf16[64,16]{0,1:T(8,128)(2,1)}, u32[]{:S(2)}) copy-start(bf16[64,16]{0,1:T(8,128)(2,1)} %param.39) | copy-start | bytes 6148
  2.8 17.4 %copy-start.1 = (bf16[1024,128]{1,0:T(8,128)(2,1)S(1)}, bf16[1024,128]{1,0:T(8,128)(2,1)}, u32[]{:S(2)}) copy-start(bf16[1024,128]{1,0:T(8,128)(2,1)} %out_weight.1) | copy-start | bytes 786436
  3.2 32.0 %copy-start.5 = (bf16[2048,32]{0,1:T(8,128)(2,1)S(1)}, bf16[2048,32]{0,1:T(8,128)(2,1)}, u32[]{:S(2)}) copy-start(bf16[2048,32]{0,1:T(8,128)(2,1)} %param.36) | copy-start | bytes 393220
  4.5 15.7 %all-to-all-start = ((bf16[16,24,128]{2,1,0:T(8,128)(2,1)}), bf16[16,24,128]{2,1,0:T(8,128)(2,1)S(1)}, u32[]{:S(2)}, u32[]{:S(2)}) async-start(bf16[16,24,128]{2,1,0:T(8,128)(2,1)} %mixed_message.1), calls=%async_computation | async-start | bytes 196608 | tf_op jit(solution)/shard_map/all_to_all | solution.py:333
  13.6 32.8 %copy-start.4 = (bf16[512,128]{1,0:T(8,128)(2,1)S(1)}, bf16[512,128]{1,0:T(8,128)(2,1)}, u32[]{:S(2)}) copy-start(bf16[512,128]{1,0:T(8,128)(2,1)} %param.38) | copy-start | bytes 393220
  20.2 39.5 %copy-start.2 = (f32[2048]{0:T(1024)S(1)}, f32[2048]{0:T(1024)}, u32[]{:S(2)}) copy-start(f32[2048]{0:T(1024)} %param.30) | copy-start | bytes 24580
  21.4 35.1 %all-to-all-start.1 = ((bf16[224,4,128]{2,1,0:T(4,128)(2,1)}), bf16[224,4,128]{2,1,0:T(4,128)(2,1)S(1)}, u32[]{:S(2)}, u32[]{:S(2)}) async-start(bf16[224,4,128]{2,1,0:T(4,128)(2,1)} %bitcast.14), calls=%async_computation.1 | async-start | bytes 458752 | tf_op jit(solution)/shard_map/all_to_all | solution.py:333
  36.6 23.1 %collective-permute-start.1 = (bf16[2,32,2048]{2,1,0:T(8,128)(2,1)S(1)}, bf16[2,32,2048]{2,1,0:T(8,128)(2,1)S(1)}, u32[]{:S(2)}, u32[]{:S(2)}) collective-permute-start(bf16[2,32,2048]{2,1,0:T(8,128)(2,1)S(1)} %get-tuple-element.34), channel_id=1, source_target_pairs={{0,1},{1,2},{2,3},{3,0},{4,5},{5,6},{6,7},{7,4},{8,9},{9,10},{10,1... | collective-permute-start | bytes 786440 | tf_op jit(solution)/shard_map/ppermute | solution.py:519
  39.2 20.5 %collective-permute-start.2 = (bf16[2,32,2048]{2,1,0:T(8,128)(2,1)S(1)}, bf16[2,32,2048]{2,1,0:T(8,128)(2,1)S(1)}, u32[]{:S(2)}, u32[]{:S(2)}) collective-permute-start(bf16[2,32,2048]{2,1,0:T(8,128)(2,1)S(1)} %get-tuple-element.35), channel_id=1, source_target_pairs={{0,2},{1,3},{2,0},{3,1},{4,6},{5,7},{6,4},{7,5},{8,10},{9,11},{10,... | collective-permute-start | bytes 786440 | tf_op jit(solution)/shard_map/ppermute | solution.py:519
  44.0 15.8 %collective-permute-start.3 = (bf16[2,32,2048]{2,1,0:T(8,128)(2,1)S(1)}, bf16[2,32,2048]{2,1,0:T(8,128)(2,1)S(1)}, u32[]{:S(2)}, u32[]{:S(2)}) collective-permute-start(bf16[2,32,2048]{2,1,0:T(8,128)(2,1)S(1)} %get-tuple-element.36), channel_id=1, source_target_pairs={{0,3},{1,0},{2,1},{3,2},{4,7},{5,4},{6,5},{7,6},{8,11},{9,8},{10,9... | collective-permute-start | bytes 786440 | tf_op jit(solution)/shard_map/ppermute | solution.py:519
  57.7 7.0 %collective-permute-start = (bf16[32,8,128]{2,1,0:T(8,128)(2,1)S(1)}, bf16[32,8,128]{2,1,0:T(8,128)(2,1)S(1)}, u32[]{:S(2)}, u32[]{:S(2)}) collective-permute-start(bf16[32,8,128]{2,1,0:T(8,128)(2,1)S(1)} %bitcast.99), channel_id=1, source_target_pairs={{0,16},{16,0},{1,17},{17,1},{2,18},{18,2},{3,19},{19,3},{4,20},{20... | collective-permute-start | bytes 196616 | tf_op jit(solution)/shard_map/ppermute | solution.py:537
  59.9 19.7 %all-to-all-start.2 = ((bf16[16,208,128]{2,1,0:T(8,128)(2,1)}), bf16[16,208,128]{2,1,0:T(8,128)(2,1)S(1)}, u32[]{:S(2)}, u32[]{:S(2)}) async-start(bf16[16,208,128]{2,1,0:T(8,128)(2,1)} %bitcast.16), calls=%async_computation.2 | async-start | bytes 1703936 | tf_op jit(solution)/shard_map/all_to_all | solution.py:333
  64.7 0.9 copy-start.6
  64.8 1.1 copy-start.10
  79.5 7.2 %copy-start.7 = (bf16[256,128]{1,0:T(8,128)(2,1)S(1)}, bf16[256,128]{1,0:T(8,128)(2,1)}, u32[]{:S(2)}) copy-start(bf16[256,128]{1,0:T(8,128)(2,1)} %param.41) | copy-start | bytes 196612
  81.4 18.1 %all-to-all-start.3 = ((bf16[16,184,128]{2,1,0:T(8,128)(2,1)}), bf16[16,184,128]{2,1,0:T(8,128)(2,1)S(1)}, u32[]{:S(2)}, u32[]{:S(2)}) async-start(bf16[16,184,128]{2,1,0:T(8,128)(2,1)} %get-tuple-element.38), calls=%async_computation.3 | async-start | bytes 1507328 | tf_op jit(solution)/shard_map/all_to_all | solution.py:333
  86.8 12.7 %copy-start = (bf16[4,512,128]{2,1,0:T(8,128)(2,1)S(1)}, bf16[4,512,128]{2,1,0:T(8,128)(2,1)}, u32[]{:S(2)}) copy-start(bf16[4,512,128]{2,1,0:T(8,128)(2,1)} %param.35) | copy-start | bytes 1572868
  100.7 26.1 %all-to-all-start.4 = ((bf16[160,4,128]{2,1,0:T(4,128)(2,1)}), bf16[160,4,128]{2,1,0:T(4,128)(2,1)S(1)}, u32[]{:S(2)}, u32[]{:S(2)}) async-start(bf16[160,4,128]{2,1,0:T(4,128)(2,1)} %bitcast.35), calls=%async_computation.4 | async-start | bytes 327680 | tf_op jit(solution)/shard_map/all_to_all | solution.py:333
  108.2 18.6 %copy-start.13 = (f32[48,4]{0,1:T(4,128)S(1)}, f32[48,4]{0,1:T(4,128)}, u32[]{:S(2)}) copy-start(f32[48,4]{0,1:T(4,128)} %param.32) | copy-start | bytes 2308
  108.3 29.7 %copy-start.12 = (f32[128]{0:T(128)S(1)}, f32[128]{0:T(128)}, u32[]{:S(2)}) copy-start(f32[128]{0:T(128)} %param.43) | copy-start | bytes 1540

commit v7 on v6

--- a/solution.py
+++ b/solution.py
@@ -120,7 +120,7 @@
 
 
 def dispatch_kernel(
-    folded_all, out_weight, table, side_piece, own_cols, outgoing, exact, short, lhs, rhs
+    folded_all, out_weight, table, side_piece, own_cols, outgoing, exact, short, lhs
 ):
     parts, half, lanes = folded_all.shape
     width = lanes // 2
@@ -130,11 +130,7 @@
         at = slice(t * lanes, (t + 1) * lanes)
         lhs[0, :, at] = jnp.where(lane < width, block, 0.0).astype(lhs.dtype)
         lhs[1, :, at] = jnp.where(lane < width, 0.0, block).astype(lhs.dtype)
-        for i in range(2):
-            rhs[t * lanes + i * width : t * lanes + (i + 1) * width] = out_weight[
-                t * width : (t + 1) * width
-            ]
-    mixing = jnp.concatenate([f32_dot(lhs[i], rhs[...], FLAT) for i in range(2)], 0)
+    mixing = jnp.concatenate([f32_dot(lhs[i], out_weight[...], FLAT) for i in range(2)], 0)
     pre_first = RESIDUAL_SCALE * own_cols[...].astype(jnp.float32) + mixing
     exact[...] = pre_first
     pre_short = pre_first.astype(short.dtype)
@@ -159,7 +155,6 @@
         ],
         scratch_shapes=[
             pltpu.VMEM((2, half, parts * lanes), bf16),
-            pltpu.VMEM((parts * lanes, cols), bf16),
         ],
         name="dispatch_rows",
         compiler_params=pltpu.CompilerParams(vmem_limit_bytes=GRANT),
@@ -504,7 +499,7 @@
     side_piece = jnp.concatenate([side_gate.T, side_up.T], 1)
     outgoing, pre_first, pre_short = dispatch_rows(
         folded_all,
-        out_weight,
+        jnp.repeat(out_weight.reshape(tp_count, -1, col_count), 2, 0).reshape(-1, col_count),
         table,
         side_piece,
         own_cols,

time: 139 us -> 140 us (level)
  no operation moved by 1% of the time
where the time goes in v7:
time: 140 us; the launch traced here: 139 us
  waiting for transfers between devices  56 us (40%)
  starting transfers between devices  52.3 us (37%)
  blocking collectives  10.7 us (8%)
  Pallas kernels  9.84 us (7%)
  other arithmetic  5.63 us (4%)
  local copies, waits for them, and re-layouts  2.28 us (2%)
    all_to_all x5, waiting for transfers between devices, swap(): return lax.all_to_all(parts, axis, 0, 0, tiled=True)  56 us
    all_to_all x5, starting transfers between devices, swap(): return lax.all_to_all(parts, axis, 0, 0, tiled=True)  40.6 us
    all_to_all x1, blocking collectives, swap(): return lax.all_to_all(parts, axis, 0, 0, tiled=True)  10.7 us
    ppermute x3, starting transfers between devices, on_device(): pieces[d] = lax.ppermute(pieces[d], 'tp_1', steps)  9.71 us
    add x1, other arithmetic, retain(): decays[None, :, None, None] * retention_state  3.09 us
  transfers between devices with their start and end apart: 9, of which 5 were waited for; matrix products, arithmetic and copies ran while one was open for 5% of the time, Pallas kernels for 2%

profile of v7, /device:TPU:2, one launch (start us, length us, event | category | flops | bytes accessed | tf_op | source)
XLA Modules:
  0.0 138.9 jit_solution(12848297760126894189)
XLA Ops:
  0.7 2.1 %project.1 = (f32[48,64]{1,0:T(8,128)S(1)}, f32[48,64]{1,0:T(8,128)S(1)}, f32[48,64]{1,0:T(8,128)S(1)}, f32[48,64]{1,0:T(8,128)S(1)}, f32[48]{0:T(128)S(1)}, /*index=5*/bf16[48,128]{1,0:T(8,128)(2,1)S(1)}) custom-call(bf16[48,2048]{1,0:T(8,128)(2,1)} %tokens.1, s32[48]{0:T(128)} %lengths.1, bf16[64,2048]{1,0:T(8,128)(2,1)} %bitcast.110, ...), custom_call_target="tpu_custom_call" | custom-call | tf_op jit(solution)/shard_map/project/pallas_call | solution.py:102
  2.8 0.2 fusion.32
  3.0 0.2 fusion.39
  3.2 0.3 fusion.66
  3.6 0.8 mixed_message.1
  4.5 9.2 %all-to-all-start = ((bf16[16,24,128]{2,1,0:T(8,128)(2,1)}), bf16[16,24,128]{2,1,0:T(8,128)(2,1)S(1)}, u32[]{:S(2)}, u32[]{:S(2)}) async-start(bf16[16,24,128]{2,1,0:T(8,128)(2,1)} %mixed_message.1), calls=%async_computation | async-start | bytes 196608 | tf_op jit(solution)/shard_map/all_to_all | solution.py:328
  13.7 0.1 copy.51
  13.8 0.1 eq.161
  13.9 0.2 convert_reduce_fusion
  14.1 0.1 reshape.477
  14.3 0.2 fusion.28
  14.7 0.3 fusion.10.table
  15.1 5.1 %all-to-all-done.folded_all = bf16[16,24,128]{2,1,0:T(8,128)(2,1)S(1)} async-done(((bf16[16,24,128]{2,1,0:T(8,128)(2,1)}), bf16[16,24,128]{2,1,0:T(8,128)(2,1)S(1)}, u32[]{:S(2)}, u32[]{:S(2)}) %all-to-all-start) | async-done | bytes 98336 | tf_op jit(solution)/shard_map/all_to_all | solution.py:328
  20.2 0.1 broadcast_in_dim.31
  20.3 1.2 dispatch_rows.1
  21.5 13.8 %all-to-all-start.1 = ((bf16[224,4,128]{2,1,0:T(4,128)(2,1)}), bf16[224,4,128]{2,1,0:T(4,128)(2,1)S(1)}, u32[]{:S(2)}, u32[]{:S(2)}) async-start(bf16[224,4,128]{2,1,0:T(4,128)(2,1)} %bitcast.16), calls=%async_computation.1 | async-start | bytes 458752 | tf_op jit(solution)/shard_map/all_to_all | solution.py:328
  35.3 0.1 fusion.12.regroup
  35.5 1.4 expert_pieces.1
  36.9 2.6 %collective-permute-start.1 = (bf16[2,32,2048]{2,1,0:T(8,128)(2,1)S(1)}, bf16[2,32,2048]{2,1,0:T(8,128)(2,1)S(1)}, u32[]{:S(2)}, u32[]{:S(2)}) collective-permute-start(bf16[2,32,2048]{2,1,0:T(8,128)(2,1)S(1)} %get-tuple-element.34), channel_id=1, source_target_pairs={{0,1},{1,2},{2,3},{3,0},{4,5},{5,6},{6,7},{7,4},{8,9},{9,10},{10,1... | collective-permute-start | bytes 786440 | tf_op jit(solution)/shard_map/ppermute | solution.py:514
  39.4 4.8 %collective-permute-start.2 = (bf16[2,32,2048]{2,1,0:T(8,128)(2,1)S(1)}, bf16[2,32,2048]{2,1,0:T(8,128)(2,1)S(1)}, u32[]{:S(2)}, u32[]{:S(2)}) collective-permute-start(bf16[2,32,2048]{2,1,0:T(8,128)(2,1)S(1)} %get-tuple-element.35), channel_id=1, source_target_pairs={{0,2},{1,3},{2,0},{3,1},{4,6},{5,7},{6,4},{7,5},{8,10},{9,11},{10,... | collective-permute-start | bytes 786440 | tf_op jit(solution)/shard_map/ppermute | solution.py:514
  44.2 2.4 %collective-permute-start.3 = (bf16[2,32,2048]{2,1,0:T(8,128)(2,1)S(1)}, bf16[2,32,2048]{2,1,0:T(8,128)(2,1)S(1)}, u32[]{:S(2)}, u32[]{:S(2)}) collective-permute-start(bf16[2,32,2048]{2,1,0:T(8,128)(2,1)S(1)} %get-tuple-element.36), channel_id=1, source_target_pairs={{0,3},{1,0},{2,1},{3,2},{4,7},{5,4},{6,5},{7,6},{8,11},{9,8},{10,9... | collective-permute-start | bytes 786440 | tf_op jit(solution)/shard_map/ppermute | solution.py:514
  46.7 10.0 %all-to-all-done.1 = bf16[224,4,128]{2,1,0:T(4,128)(2,1)S(1)} async-done(((bf16[224,4,128]{2,1,0:T(4,128)(2,1)}), bf16[224,4,128]{2,1,0:T(4,128)(2,1)S(1)}, u32[]{:S(2)}, u32[]{:S(2)}) %all-to-all-start.1) | async-done | bytes 229408 | tf_op jit(solution)/shard_map/all_to_all | solution.py:328
  56.7 1.2 slot_message.1
  57.9 1.9 %collective-permute-start = (bf16[32,8,128]{2,1,0:T(8,128)(2,1)S(1)}, bf16[32,8,128]{2,1,0:T(8,128)(2,1)S(1)}, u32[]{:S(2)}, u32[]{:S(2)}) collective-permute-start(bf16[32,8,128]{2,1,0:T(8,128)(2,1)S(1)} %bitcast.102), channel_id=1, source_target_pairs={{0,16},{16,0},{1,17},{17,1},{2,18},{18,2},{3,19},{19,3},{4,20},{20... | collective-permute-start | bytes 196616 | tf_op jit(solution)/shard_map/ppermute | solution.py:532
  60.1 4.9 %all-to-all-start.2 = ((bf16[16,208,128]{2,1,0:T(8,128)(2,1)}), bf16[16,208,128]{2,1,0:T(8,128)(2,1)S(1)}, u32[]{:S(2)}, u32[]{:S(2)}) async-start(bf16[16,208,128]{2,1,0:T(8,128)(2,1)} %bitcast.18), calls=%async_computation.2 | async-start | bytes 1703936 | tf_op jit(solution)/shard_map/all_to_all | solution.py:328
  65.0 0.1 reshape.483
  65.2 0.4 fusion.65
  65.6 0.1 copy.56
  65.6 0.2 squeeze.6
  65.9 0.1 copy.57
  66.0 0.2 squeeze.7
  66.2 13.5 %all-to-all-done.2.rows_pre = bf16[16,208,128]{2,1,0:T(8,128)(2,1)S(1)} async-done(((bf16[16,208,128]{2,1,0:T(8,128)(2,1)}), bf16[16,208,128]{2,1,0:T(8,128)(2,1)S(1)}, u32[]{:S(2)}, u32[]{:S(2)}) %all-to-all-start.2) | async-done | bytes 852000 | tf_op jit(solution)/shard_map/all_to_all | solution.py:328
  79.7 1.9 %hidden_units.1 = (bf16[16,184,128]{2,1,0:T(8,128)(2,1)}, bf16[48,128]{1,0:T(8,128)(2,1)S(1)}, f32[48,1]{1,0:T(8,128)S(1)}) custom-call(bf16[16,208,128]{2,1,0:T(8,128)(2,1)S(1)} %all-to-all-done.2.rows_pre, f32[16,128]{1,0:T(8,128)S(1)} %bitcast.103, f32[48,128]{1,0:T(8,128)S(1)} %get-tuple-element.31.pre_first, ...), custom_call_target="tpu_custom_call" | custom-call | tf_op jit(solution)/shard_map/hidden_units/pallas_call | solution.py:407
  81.7 5.3 %all-to-all-start.3 = ((bf16[16,184,128]{2,1,0:T(8,128)(2,1)}), bf16[16,184,128]{2,1,0:T(8,128)(2,1)S(1)}, u32[]{:S(2)}, u32[]{:S(2)}) async-start(bf16[16,184,128]{2,1,0:T(8,128)(2,1)} %get-tuple-element.38), calls=%async_computation.3 | async-start | bytes 1507328 | tf_op jit(solution)/shard_map/all_to_all | solution.py:328
  87.0 3.1 %multiply_add_fusion = f32[48,1,64,64]{3,2,1,0:T(8,128)} fusion(f32[48,1,64,64]{3,2,1,0:T(8,128)} %param.23, f32[48,64]{1,0:T(8,128)S(1)} %get-tuple-element.25, f32[48,64]{1,0:T(8,128)S(1)} %maximum_multiply_fusion.1, f32[]{:T(128)S(6)} %sub.83), kind=kLoop, calls=%fused_computation.2 | loop fusion | flops 589824 | bytes 1597444 | tf_op jit(solution)/shard_map/add | solution.py:320
  90.1 0.1 reduce.5
  90.3 9.5 %all-to-all-done.3.hidden_all = bf16[16,184,128]{2,1,0:T(8,128)(2,1)S(1)} async-done(((bf16[16,184,128]{2,1,0:T(8,128)(2,1)}), bf16[16,184,128]{2,1,0:T(8,128)(2,1)S(1)}, u32[]{:S(2)}, u32[]{:S(2)}) %all-to-all-start.3) | async-done | bytes 753696 | tf_op jit(solution)/shard_map/all_to_all | solution.py:328
  99.7 1.2 return_rows.1
  100.9 7.5 %all-to-all-start.4 = ((bf16[160,4,128]{2,1,0:T(4,128)(2,1)}), bf16[160,4,128]{2,1,0:T(4,128)(2,1)S(1)}, u32[]{:S(2)}, u32[]{:S(2)}) async-start(bf16[160,4,128]{2,1,0:T(4,128)(2,1)} %bitcast.37), calls=%async_computation.4 | async-start | bytes 327680 | tf_op jit(solution)/shard_map/all_to_all | solution.py:328
  108.4 0.1 broadcast_in_dim.37
  108.6 0.2 fusion.15
  108.8 0.1 broadcast_in_dim.39
  108.9 0.2 fusion.13
  109.1 17.9 %all-to-all-done.4 = bf16[160,4,128]{2,1,0:T(4,128)(2,1)S(1)} async-done(((bf16[160,4,128]{2,1,0:T(4,128)(2,1)}), bf16[160,4,128]{2,1,0:T(4,128)(2,1)S(1)}, u32[]{:S(2)}, u32[]{:S(2)}) %all-to-all-start.4) | async-done | bytes 163872 | tf_op jit(solution)/shard_map/all_to_all | solution.py:328
  127.0 0.3 fusion.2
  127.3 0.2 fusion.63
  127.5 10.7 %all_to_all.30 = f32[16,2,48]{2,1,0:T(2,128)S(1)} all-to-all(f32[16,2,48]{2,1,0:T(2,128)S(1)} %broadcast_in_dim.40), channel_id=1, replica_groups=mesh['z'=16,'core'=2,'tp_0'=4,'tp_1'=4] {'tp_0','tp_1'}, dimensions={0} | all-to-all | bytes 12288 | tf_op jit(solution)/shard_map/all_to_all | solution.py:328
  138.2 0.7 multiply_convert_fusion
  (64 shorter events, 1.0 us)
Async XLA Ops:
  0.6 2.6 %copy-start.2 = (f32[48,1,64,64]{3,2,1,0:T(8,128)S(1)}, f32[48,1,64,64]{3,2,1,0:T(8,128)}, u32[]{:S(2)}) copy-start(f32[48,1,64,64]{3,2,1,0:T(8,128)} %param.23) | copy-start | bytes 2359300
  0.7 13.0 %copy-start.11 = (s32[48,4]{0,1:T(4,128)S(1)}, s32[48,4]{0,1:T(4,128)}, u32[]{:S(2)}) copy-start(s32[48,4]{0,1:T(4,128)} %param.31) | copy-start | bytes 2308
  2.8 11.7 %copy-start.8 = (bf16[64,16]{0,1:T(8,128)(2,1)S(1)}, bf16[64,16]{0,1:T(8,128)(2,1)}, u32[]{:S(2)}) copy-start(bf16[64,16]{0,1:T(8,128)(2,1)} %param.40) | copy-start | bytes 6148
  2.8 11.7 %copy-start.9 = (bf16[64,16]{0,1:T(8,128)(2,1)S(1)}, bf16[64,16]{0,1:T(8,128)(2,1)}, u32[]{:S(2)}) copy-start(bf16[64,16]{0,1:T(8,128)(2,1)} %param.39) | copy-start | bytes 6148
  2.8 17.4 %copy-start.3 = (bf16[1024,128]{1,0:T(8,128)(2,1)S(1)}, bf16[1024,128]{1,0:T(8,128)(2,1)}, u32[]{:S(2)}) copy-start(bf16[1024,128]{1,0:T(8,128)(2,1)} %param.29) | copy-start | bytes 786436
  3.6 31.8 %copy-start.5 = (bf16[2048,32]{0,1:T(8,128)(2,1)S(1)}, bf16[2048,32]{0,1:T(8,128)(2,1)}, u32[]{:S(2)}) copy-start(bf16[2048,32]{0,1:T(8,128)(2,1)} %param.36) | copy-start | bytes 393220
  4.5 15.7 %all-to-all-start = ((bf16[16,24,128]{2,1,0:T(8,128)(2,1)}), bf16[16,24,128]{2,1,0:T(8,128)(2,1)S(1)}, u32[]{:S(2)}, u32[]{:S(2)}) async-start(bf16[16,24,128]{2,1,0:T(8,128)(2,1)} %mixed_message.1), calls=%async_computation | async-start | bytes 196608 | tf_op jit(solution)/shard_map/all_to_all | solution.py:328
  20.3 26.4 %copy-start.4 = (bf16[512,128]{1,0:T(8,128)(2,1)S(1)}, bf16[512,128]{1,0:T(8,128)(2,1)}, u32[]{:S(2)}) copy-start(bf16[512,128]{1,0:T(8,128)(2,1)} %param.38) | copy-start | bytes 393220
  21.5 38.4 %copy-start.1 = (f32[2048]{0:T(1024)S(1)}, f32[2048]{0:T(1024)}, u32[]{:S(2)}) copy-start(f32[2048]{0:T(1024)} %param.30) | copy-start | bytes 24580
  21.5 35.2 %all-to-all-start.1 = ((bf16[224,4,128]{2,1,0:T(4,128)(2,1)}), bf16[224,4,128]{2,1,0:T(4,128)(2,1)S(1)}, u32[]{:S(2)}, u32[]{:S(2)}) async-start(bf16[224,4,128]{2,1,0:T(4,128)(2,1)} %bitcast.16), calls=%async_computation.1 | async-start | bytes 458752 | tf_op jit(solution)/shard_map/all_to_all | solution.py:328
  36.9 23.1 %collective-permute-start.1 = (bf16[2,32,2048]{2,1,0:T(8,128)(2,1)S(1)}, bf16[2,32,2048]{2,1,0:T(8,128)(2,1)S(1)}, u32[]{:S(2)}, u32[]{:S(2)}) collective-permute-start(bf16[2,32,2048]{2,1,0:T(8,128)(2,1)S(1)} %get-tuple-element.34), channel_id=1, source_target_pairs={{0,1},{1,2},{2,3},{3,0},{4,5},{5,6},{6,7},{7,4},{8,9},{9,10},{10,1... | collective-permute-start | bytes 786440 | tf_op jit(solution)/shard_map/ppermute | solution.py:514
  39.4 20.5 %collective-permute-start.2 = (bf16[2,32,2048]{2,1,0:T(8,128)(2,1)S(1)}, bf16[2,32,2048]{2,1,0:T(8,128)(2,1)S(1)}, u32[]{:S(2)}, u32[]{:S(2)}) collective-permute-start(bf16[2,32,2048]{2,1,0:T(8,128)(2,1)S(1)} %get-tuple-element.35), channel_id=1, source_target_pairs={{0,2},{1,3},{2,0},{3,1},{4,6},{5,7},{6,4},{7,5},{8,10},{9,11},{10,... | collective-permute-start | bytes 786440 | tf_op jit(solution)/shard_map/ppermute | solution.py:514
  44.2 15.8 %collective-permute-start.3 = (bf16[2,32,2048]{2,1,0:T(8,128)(2,1)S(1)}, bf16[2,32,2048]{2,1,0:T(8,128)(2,1)S(1)}, u32[]{:S(2)}, u32[]{:S(2)}) collective-permute-start(bf16[2,32,2048]{2,1,0:T(8,128)(2,1)S(1)} %get-tuple-element.36), channel_id=1, source_target_pairs={{0,3},{1,0},{2,1},{3,2},{4,7},{5,4},{6,5},{7,6},{8,11},{9,8},{10,9... | collective-permute-start | bytes 786440 | tf_op jit(solution)/shard_map/ppermute | solution.py:514
  57.9 7.0 %collective-permute-start = (bf16[32,8,128]{2,1,0:T(8,128)(2,1)S(1)}, bf16[32,8,128]{2,1,0:T(8,128)(2,1)S(1)}, u32[]{:S(2)}, u32[]{:S(2)}) collective-permute-start(bf16[32,8,128]{2,1,0:T(8,128)(2,1)S(1)} %bitcast.102), channel_id=1, source_target_pairs={{0,16},{16,0},{1,17},{17,1},{2,18},{18,2},{3,19},{19,3},{4,20},{20... | collective-permute-start | bytes 196616 | tf_op jit(solution)/shard_map/ppermute | solution.py:532
  60.1 19.7 %all-to-all-start.2 = ((bf16[16,208,128]{2,1,0:T(8,128)(2,1)}), bf16[16,208,128]{2,1,0:T(8,128)(2,1)S(1)}, u32[]{:S(2)}, u32[]{:S(2)}) async-start(bf16[16,208,128]{2,1,0:T(8,128)(2,1)} %bitcast.18), calls=%async_computation.2 | async-start | bytes 1703936 | tf_op jit(solution)/shard_map/all_to_all | solution.py:328
  65.0 0.9 copy-start.6
  65.0 1.1 copy-start.10
  79.7 7.2 %copy-start.7 = (bf16[256,128]{1,0:T(8,128)(2,1)S(1)}, bf16[256,128]{1,0:T(8,128)(2,1)}, u32[]{:S(2)}) copy-start(bf16[256,128]{1,0:T(8,128)(2,1)} %param.41) | copy-start | bytes 196612
  81.7 18.1 %all-to-all-start.3 = ((bf16[16,184,128]{2,1,0:T(8,128)(2,1)}), bf16[16,184,128]{2,1,0:T(8,128)(2,1)S(1)}, u32[]{:S(2)}, u32[]{:S(2)}) async-start(bf16[16,184,128]{2,1,0:T(8,128)(2,1)} %get-tuple-element.38), calls=%async_computation.3 | async-start | bytes 1507328 | tf_op jit(solution)/shard_map/all_to_all | solution.py:328
  87.0 12.7 %copy-start = (bf16[4,512,128]{2,1,0:T(8,128)(2,1)S(1)}, bf16[4,512,128]{2,1,0:T(8,128)(2,1)}, u32[]{:S(2)}) copy-start(bf16[4,512,128]{2,1,0:T(8,128)(2,1)} %param.35) | copy-start | bytes 1572868
  100.9 26.1 %all-to-all-start.4 = ((bf16[160,4,128]{2,1,0:T(4,128)(2,1)}), bf16[160,4,128]{2,1,0:T(4,128)(2,1)S(1)}, u32[]{:S(2)}, u32[]{:S(2)}) async-start(bf16[160,4,128]{2,1,0:T(4,128)(2,1)} %bitcast.37), calls=%async_computation.4 | async-start | bytes 327680 | tf_op jit(solution)/shard_map/all_to_all | solution.py:328
  108.4 18.6 %copy-start.13 = (f32[48,4]{0,1:T(4,128)S(1)}, f32[48,4]{0,1:T(4,128)}, u32[]{:S(2)}) copy-start(f32[48,4]{0,1:T(4,128)} %param.32) | copy-start | bytes 2308
  108.5 29.7 %copy-start.12 = (f32[128]{0:T(128)S(1)}, f32[128]{0:T(128)}, u32[]{:S(2)}) copy-start(f32[128]{0:T(128)} %param.43) | copy-start | bytes 1540
